TPU v7x, 256 devices: a whole 4x4x8 slice. The times are simulated.
256 devices in a mesh: sp: 64 (over z, y, core), tp: 4 (over x).
Axes of the slice: x: 4, y: 4, z: 8, core: 2. Of those that a mesh axis runs over, the one named last changes fastest.
Arguments:
- queries_one: bfloat16 [16384, 512], P('sp', 'tp'), may hold values from -6 to 6
- queries_two: bfloat16 [16384, 512], P('sp', 'tp'), may hold values from -6 to 6
- keys_one: bfloat16 [16384, 512], P('sp', 'tp'), may hold values from -6 to 6
- keys_two: bfloat16 [16384, 512], P('sp', 'tp'), may hold values from -6 to 6
- values: bfloat16 [16384, 1024], P('sp', 'tp'), may hold values from -6 to 6
- mix_lambda: float32 [4], P('tp'), may hold values from 0.3 to 0.8
- head_gain: float32 [1024], P('tp'), may hold values from 0.1 to 1.9
- out_weight: bfloat16 [1024, 2048], P('tp'), may hold values from -0.1875 to 0.1875
- residual_in: bfloat16 [16384, 2048], P('sp', 'tp'), may hold values from -12 to 12
- norm_gain: float32 [2048], replicated, may hold values from 0.1 to 1.9
- gate_weight: bfloat16 [2048, 5632], P('sp', 'tp'), may hold values from -0.125 to 0.125
- up_weight: bfloat16 [2048, 5632], P('sp', 'tp'), may hold values from -0.125 to 0.125
- down_weight: bfloat16 [5632, 2048], P('tp', 'sp'), may hold values from -0.078125 to 0.078125
Outputs:
- layer_out: bfloat16 [16384, 2048], P('sp', 'tp')
All inputs are finite; a program needn't handle non-finite values.
Results may differ from a plain program's by a relative error of at most 0.012.
Values may be sent and summed in bfloat16 or wider, within the bound.
No kernel may reach another device: no remote copies, remote signals or barrier semaphores. Data moves between devices by JAX's collectives and lax.ppermute only.
A program may use at most 192 MiB of HBM per device.

v0:
```python
import functools
import math

import jax
import jax.numpy as jnp
from jax import lax
from jax.experimental import pallas as pl
from jax.experimental.pallas import tpu as pltpu
from jax.sharding import Mesh
from jax.sharding import PartitionSpec as P

HEAD = 128
EPS = 1e-06
NEG = -1e30
FLOOR = -1e20
SCALE2 = HEAD**-0.5 * math.log2(math.e)
STAT = 16


VMEM = pl.BlockSpec(memory_space=pltpu.VMEM)
SMEM = pl.BlockSpec(memory_space=pltpu.SMEM)


def shift(a, axis, count, by):
    return lax.ppermute(a, axis, [(i, (i + by) % count) for i in range(count)])


def dot_nt(a, b):
    return lax.dot_general(a, b, (((1,), (1,)), ((), ())), preferred_element_type=jnp.float32)


def dot_nn(a, b):
    return lax.dot_general(a, b, (((1,), (0,)), ((), ())), preferred_element_type=jnp.float32)


def eye(n):
    return lax.broadcasted_iota(jnp.int32, (n, n), 0) == lax.broadcasted_iota(jnp.int32, (n, n), 1)


def to_row(col):
    n = col.shape[0]
    return jnp.sum(jnp.where(eye(n), col, 0.0), axis=0, keepdims=True)


def to_col(row):
    n = row.shape[1]
    return jnp.sum(jnp.where(eye(n), row, 0.0), axis=1, keepdims=True)


def stat_rows(lse_cols):
    row = jnp.concatenate([to_row(c) for c in lse_cols], axis=1)
    high = row.astype(jnp.bfloat16)
    rest = row - high.astype(jnp.float32)
    mid = rest.astype(jnp.bfloat16)
    low = (rest - mid.astype(jnp.float32)).astype(jnp.bfloat16)
    index = lax.broadcasted_iota(jnp.int32, (STAT, row.shape[1]), 0)
    zero = jnp.zeros_like(row)
    picked = jnp.where(
        index == 0,
        high.astype(jnp.float32),
        jnp.where(index == 1, mid.astype(jnp.float32), jnp.where(index == 2, low.astype(jnp.float32), zero)),
    )
    return picked.astype(jnp.bfloat16)


def read_stats(block, m):
    rows = block.shape[0] - STAT
    half = block.shape[1] // 2
    stats = block[rows:, m * half : (m + 1) * half].astype(jnp.float32)
    return to_col(jnp.sum(stats, axis=0, keepdims=True))


def attention_kernel(steps, carried, where_ref, q_ref, other_q_ref, *rest):
    pieces, rest = rest[: len(steps)], rest[len(steps) :]
    before, (mine_ref, other_ref, s_ref) = rest[:-3], rest[-3:]
    z, y, c = where_ref[0], where_ref[1], where_ref[2]
    r = pl.program_id(0)
    yq = lax.rem(y - r + 4, 4)
    tok = q_ref.shape[1]
    rows = 2 * tok
    lanes = 128
    biases, starts, at = [], [], 0
    for ref, step in zip(pieces, steps):
        source = lax.rem(z + step + 8, 8)
        biases.append(jnp.where(source <= z, 0.0, NEG).astype(jnp.float32))
        starts.append(at)
        at += ref.shape[0]
    out = []
    lse = []
    for m in range(2):
        heads = slice(m * HEAD, (m + 1) * HEAD)
        q = jnp.concatenate([q_ref[0, :, heads], other_q_ref[0, :, heads]], axis=0)
        high = jnp.full((rows, lanes), FLOOR, jnp.float32)
        for n, ref in enumerate(pieces):
            keys = ref.shape[0]
            s = dot_nt(q, ref[:, heads])
            if steps[n] == 0:
                row = lax.broadcasted_iota(jnp.int32, (rows, keys), 0)
                col = lax.broadcasted_iota(jnp.int32, (rows, keys), 1)
                qpos = yq * rows + jnp.where(row < tok, row + c * tok, row - tok + (1 - c) * tok)
                s = jnp.where(y * rows + c * tok + col <= qpos, s, NEG)
            s_ref[:, starts[n] : starts[n] + keys] = s
            top = s[:, :lanes]
            for k in range(lanes, keys, lanes):
                top = jnp.maximum(top, s[:, k : k + lanes])
            high = jnp.maximum(high, top * SCALE2 + biases[n])
        high = jnp.max(high, axis=1, keepdims=True)
        total = jnp.zeros((rows, lanes), jnp.float32)
        acc = jnp.zeros((rows, 2 * HEAD), jnp.float32)
        for n, ref in enumerate(pieces):
            keys = ref.shape[0]
            p = jnp.exp2(s_ref[:, starts[n] : starts[n] + keys] * SCALE2 - (high - biases[n]))
            for k in range(0, keys, lanes):
                total = total + p[:, k : k + lanes]
            acc = acc + dot_nn(p.astype(jnp.bfloat16), ref[:, 2 * HEAD :])
        total = jnp.sum(total, axis=1, keepdims=True)
        if carried:
            stats = jnp.concatenate([read_stats(ref[0], m) for ref in before], axis=0)
            old = jnp.concatenate(
                [ref[0, :tok, m * 2 * HEAD : (m + 1) * 2 * HEAD] for ref in before], axis=0
            )
            now = jnp.where(total > 0.0, high + jnp.log2(jnp.maximum(total, 1e-30)), NEG)
            top = jnp.maximum(stats, now)
            w_old, w_now = jnp.exp2(stats - top), jnp.exp2(now - top)
            both = w_old + w_now
            scale_now = w_now / (jnp.maximum(total, 1e-30) * both)
            out.append((acc * scale_now + old.astype(jnp.float32) * (w_old / both)).astype(jnp.bfloat16))
            lse.append(top + jnp.log2(both))
        else:
            out.append((acc * (1.0 / jnp.maximum(total, 1e-30))).astype(jnp.bfloat16))
            lse.append(jnp.where(total > 0.0, high + jnp.log2(jnp.maximum(total, 1e-30)), NEG))
    for h, ref in enumerate((mine_ref, other_ref)):
        part = slice(h * tok, (h + 1) * tok)
        ref[0, :tok, : 2 * HEAD] = out[0][part]
        ref[0, :tok, 2 * HEAD :] = out[1][part]
        ref[0, tok:, :] = stat_rows([lse[0][part], lse[1][part]])


def attention(where, q, other_q, pieces, steps, before):
    count, tok, _ = q.shape
    rows = 2 * tok
    keys = sum(p.shape[0] for p in pieces)
    width = pieces[0].shape[1]
    block = jax.ShapeDtypeStruct((count, tok + STAT, width), jnp.bfloat16)
    flops = 2 * 2 * count * rows * keys * 3 * HEAD
    spec = pl.BlockSpec((1, tok + STAT, width), lambda r: (r, 0, 0))
    return pl.pallas_call(
        functools.partial(attention_kernel, steps, bool(before)),
        grid=(count,),
        out_shape=(block, block),
        in_specs=[SMEM]
        + [pl.BlockSpec((1, tok, 2 * HEAD), lambda r: (r, 0, 0))] * 2
        + [pl.BlockSpec(p.shape, lambda r: (0, 0)) for p in pieces]
        + [spec] * len(before),
        out_specs=[spec, spec],
        scratch_shapes=[pltpu.VMEM((rows, keys), jnp.float32)],
        compiler_params=pltpu.CompilerParams(vmem_limit_bytes=32 * 1024 * 1024),
        cost_estimate=pl.CostEstimate(
            flops=flops, bytes_accessed=4 * 1024 * 1024, transcendentals=2 * count * rows * keys
        ),
    )(where, q, other_q, *pieces, *before)


def merged(blocks):
    tok = blocks[0].shape[0] - STAT
    stats = [[read_stats(b, m) for m in range(2)] for b in blocks]
    outs, lses = [], []
    for m in range(2):
        top = stats[0][m]
        for s in stats[1:]:
            top = jnp.maximum(top, s[m])
        weights = [jnp.exp2(s[m] - top) for s in stats]
        total = sum(weights[1:], weights[0])
        acc = None
        for w, b in zip(weights, blocks):
            term = w * b[:tok, m * 2 * HEAD : (m + 1) * 2 * HEAD].astype(jnp.float32)
            acc = term if acc is None else acc + term
        outs.append(acc / total)
        lses.append(top + jnp.log2(total))
    return outs, lses


def merge_kernel(a_ref, b_ref, *out_refs):
    for r, ref in enumerate(out_refs):
        tok = ref.shape[0] - STAT
        outs, lses = merged([a_ref[r], b_ref[r]])
        ref[:tok, : 2 * HEAD] = outs[0].astype(jnp.bfloat16)
        ref[:tok, 2 * HEAD :] = outs[1].astype(jnp.bfloat16)
        ref[tok:, :] = stat_rows(lses)


def merge_cores(a, b):
    count, rows, width = a.shape
    return pl.pallas_call(
        merge_kernel,
        out_shape=(jax.ShapeDtypeStruct((rows, width), jnp.bfloat16),) * count,
        in_specs=[VMEM, VMEM],
        out_specs=(VMEM,) * count,
        cost_estimate=pl.CostEstimate(flops=4_000_000_000, bytes_accessed=3 * a.size * 2, transcendentals=0),
        name="merge_cores",
    )(a, b)


def finish_kernel(lam_ref, gain_ref, *refs):
    blocks, out_ref = [ref[...] for ref in refs[:-1]], refs[-1]
    outs, _ = merged(blocks)
    mixed = outs[0] - lam_ref[0] * outs[1]
    mean = jnp.mean(mixed * mixed, axis=1, keepdims=True)
    out_ref[...] = (mixed * lax.rsqrt(mean + EPS) * gain_ref[...] * 0.8).astype(jnp.bfloat16)


def finish(lam, gain, blocks):
    tok = blocks[0].shape[0] - STAT
    return pl.pallas_call(
        finish_kernel,
        out_shape=jax.ShapeDtypeStruct((tok, 2 * HEAD), jnp.bfloat16),
        in_specs=[SMEM] + [VMEM] * (1 + len(blocks)),
        out_specs=VMEM,
        cost_estimate=pl.CostEstimate(flops=4_000_000_000, bytes_accessed=2_000_000, transcendentals=0),
        name="finish_heads",
    )(lam, gain.reshape(1, -1), *blocks)


def project_kernel(where_ref, gain_ref, *refs):
    att, (ow_ref, res_ref), extra = refs[:4], refs[4:6], refs[6:10]
    own_ref, normed_ref, sum_ref = refs[10:]
    x = where_ref[3]
    tok, block = res_ref.shape
    width = ow_ref.shape[1]
    half = tok // 2
    left, low, high, right = extra

    def at(s):
        return pl.ds(pl.multiple_of(lax.rem(x - s + 4, 4) * block, block), block)

    sum_ref[:, at(0)] = res_ref[...].astype(jnp.float32)
    sum_ref[:, at(1)] = left[:, width:].astype(jnp.float32)
    sum_ref[:half, at(2)] = low[:, width:].astype(jnp.float32)
    sum_ref[half:, at(2)] = high[:, width:].astype(jnp.float32)
    sum_ref[:, at(3)] = right[:, width:].astype(jnp.float32)
    square = jnp.zeros((tok, 1), jnp.float32)
    for k in range(0, width, block):
        cols = slice(k, k + block)
        acc = sum_ref[:, cols]
        parts = (
            dot_nn(att[0][...], ow_ref[:, cols]),
            dot_nn(att[1][...], left[:, cols]),
            dot_nn(att[2][:, :half], low[:, cols]) + dot_nn(att[2][:, half:], high[:, cols]),
            dot_nn(att[3][...], right[:, cols]),
        )
        total = None
        for part in parts:
            part = part.astype(jnp.bfloat16).astype(jnp.float32)
            total = part if total is None else total + part
        resid = (acc + total).astype(jnp.bfloat16).astype(jnp.float32)
        sum_ref[:, cols] = resid
        square = square + jnp.sum(resid * resid, axis=1, keepdims=True)
    scale = lax.rsqrt(square * (1.0 / width) + EPS)
    own_ref[...] = sum_ref[:, at(0)].astype(jnp.bfloat16)
    normed_ref[...] = (sum_ref[...] * scale * gain_ref[...]).astype(jnp.bfloat16)


def project(where, gain, att, ow, res, extra):
    tok, block = res.shape
    width = ow.shape[1]
    return pl.pallas_call(
        project_kernel,
        out_shape=(
            jax.ShapeDtypeStruct((tok, block), jnp.bfloat16),
            jax.ShapeDtypeStruct((tok, width), jnp.bfloat16),
        ),
        in_specs=[SMEM] + [VMEM] * 11,
        out_specs=(VMEM, VMEM),
        scratch_shapes=[pltpu.VMEM((tok, width), jnp.float32)],
        compiler_params=pltpu.CompilerParams(vmem_limit_bytes=32 * 1024 * 1024),
        cost_estimate=pl.CostEstimate(flops=2_000_000_000, bytes_accessed=8_000_000, transcendentals=0),
        name="project_norm",
    )(where, gain.reshape(1, -1), *att, ow, res, *extra)


def mixer_kernel(where_ref, normed_ref, full_ref, lo_ref, hi_ref, one_ref, three_ref, here_ref, w_ref, d_ref, h_ref, sems):
    count, _, width = w_ref.shape
    _, block, units = d_ref.shape
    lane = width // 2
    half = lo_ref.shape[0]

    def copies(j):
        at = pl.multiple_of(j * lane, lane)
        return [
            pltpu.make_async_copy(
                full_ref.at[:, pl.ds(at + n * units, lane)],
                w_ref.at[j, :, pl.ds(n * lane, lane)],
                sems.at[n, j],
            )
            for n in range(2)
        ]

    def down_copy(n, s):
        row = pl.multiple_of(lax.rem(where_ref[3] + s, 4) * block, block)
        return pltpu.make_async_copy(
            full_ref.at[pl.ds(row, block), pl.ds(2 * units, units)], d_ref.at[n], sems.at[0, count + n]
        )

    @pl.loop(0, count)
    def _(j):
        for c in copies(j):
            c.start()

    ahead = (2, 1, 3, 0)
    for n, s in enumerate(ahead):
        down_copy(n, s).start()

    @pl.loop(0, count)
    def _(j):
        for c in copies(j):
            c.wait()
        both = dot_nn(normed_ref[...], w_ref[j])
        gate, up = both[:, :lane], both[:, lane:]
        cols = pl.ds(pl.multiple_of(j * lane, lane), lane)
        h_ref[:, cols] = (gate / (1.0 + jnp.exp(-gate)) * up).astype(jnp.bfloat16)

    for n, s in enumerate(ahead):
        down_copy(n, s).wait()
    two = dot_nt(h_ref[...], d_ref[0]).astype(jnp.bfloat16)
    lo_ref[...] = two[:half]
    hi_ref[...] = two[half:]
    for n, ref in enumerate((one_ref, three_ref, here_ref)):
        ref[...] = dot_nt(h_ref[...], d_ref[n + 1]).astype(jnp.bfloat16)


def mixer(where, normed, full, block):
    tok, width = normed.shape
    units = full.shape[1] // 3
    lane = 128
    count = units // lane
    whole = jax.ShapeDtypeStruct((tok, block), jnp.bfloat16)
    part = jax.ShapeDtypeStruct((tok // 2, block), jnp.bfloat16)
    return pl.pallas_call(
        mixer_kernel,
        out_shape=(part, part, whole, whole, whole),
        in_specs=[SMEM, VMEM, pl.BlockSpec(memory_space=pl.ANY)],
        out_specs=(VMEM,) * 5,
        scratch_shapes=[
            pltpu.VMEM((count, width, 2 * lane), jnp.bfloat16),
            pltpu.VMEM((4, block, units), jnp.bfloat16),
            pltpu.VMEM((tok, units), jnp.bfloat16),
            pltpu.SemaphoreType.DMA((2, count + 4)),
        ],
        compiler_params=pltpu.CompilerParams(vmem_limit_bytes=40 * 1024 * 1024),
        cost_estimate=pl.CostEstimate(
            flops=2 * tok * width * units * 3, bytes_accessed=18_000_000, transcendentals=tok * units
        ),
        name="mixer",
    )(where, normed, full)


def both_ways(a, axis, count):
    half = a.shape[0] // 2
    left = shift(a, axis, count, 1)
    right = shift(a, axis, count, -1)
    low = shift(left[:half], axis, count, 1)
    high = shift(right[half:], axis, count, -1)
    return [left, low, high, right]


def per_device(q1, q2, k1, k2, v, lam, hgain, ow, res, ngain, gw, uw, dw):
    z, y, c, x = (lax.axis_index(n).astype(jnp.int32) for n in ("z", "y", "c", "x"))
    where = jnp.stack([z, y, c, x])

    both = jnp.concatenate([gw, uw, dw.T], axis=1)
    full = lax.all_gather(both, ("z", "y", "c"), axis=0, tiled=True)

    q = jnp.concatenate([q1, q2], axis=1)
    seen = [q]
    for s in range(1, 4):
        seen.append(shift(q, "y", 4, s))
    queries = jnp.stack(seen)
    others = shift(queries, "c", 2, 1)

    kv = jnp.concatenate([k1, k2, v], axis=1)
    tok = kv.shape[0]
    up, down_ring = [kv], [kv]
    for _ in range(3):
        up.append(shift(up[-1], "z", 8, 1))
        down_ring.append(shift(down_ring[-1], "z", 8, -1))
    half_up = shift(up[3][: tok // 2], "z", 8, 1)
    half_down = shift(down_ring[3][tok // 2 :], "z", 8, -1)

    extra = both_ways(jnp.concatenate([ow, res], axis=1), "x", 4)

    part = attention(where, queries, others, [kv, up[1], down_ring[1], up[2], down_ring[2]], (0, -1, 1, -2, 2), ())
    mine, other = attention(where, queries, others, [up[3], down_ring[3], half_up, half_down], (-3, 3, 4, 4), part)
    theirs = shift(other, "c", 2, 1)
    blocks = merge_cores(mine, theirs)
    arrived = [blocks[0]] + [shift(blocks[s], "y", 4, -s) for s in range(1, 4)]
    attended = finish(lam, hgain, arrived)
    att = [attended] + [shift(attended, "x", 4, s) for s in range(1, 4)]
    own, normed = project(where, ngain, att, ow, res, extra)

    width = res.shape[1]
    lo, hi, one, three, here = mixer(where, normed, full, width)
    half = tok // 2

    def wide(a):
        return a.astype(jnp.float32)

    from_left = shift(lo, "x", 4, 1)
    from_right = shift(hi, "x", 4, -1)
    left_hi = shift(one[half:], "x", 4, 1)
    right_lo = shift(three[:half], "x", 4, -1)
    left_lo = shift((wide(one[:half]) + wide(from_left)).astype(jnp.bfloat16), "x", 4, 1)
    right_hi = shift((wide(three[half:]) + wide(from_right)).astype(jnp.bfloat16), "x", 4, -1)
    near = wide(own) + wide(here)
    first = near[:half] + wide(right_lo) + wide(left_lo)
    second = near[half:] + wide(left_hi) + wide(right_hi)
    return jnp.concatenate([first, second], axis=0).astype(jnp.bfloat16)


def solution(mesh):
    fine = Mesh(mesh.devices.reshape(8, 4, 2, 4), ("z", "y", "c", "x"))
    sp = ("z", "y", "c")
    in_specs = (P(sp, "x"),) * 5 + (
        P("x"),
        P("x"),
        P("x", None),
        P(sp, "x"),
        P(),
        P(sp, "x"),
        P(sp, "x"),
        P("x", sp),
    )

    return jax.shard_map(per_device, mesh=fine, in_specs=in_specs, out_specs=P(sp, "x"), check_vma=False)
```

profile of v0, /device:TPU:1, one launch (start us, length us, event | category | flops | bytes accessed | tf_op | source)
XLA Modules:
  0.0 168.9 jit_solution(10736885205760315668)
XLA Ops:
  6.5 1.7 %pad_maximum_fusion.1 = bf16[32,4224]{1,0:T(8,128)(2,1)} fusion(bf16[32,1408]{1,0:T(8,128)(2,1)} %bitcast.16, bf16[32,1408]{1,0:T(8,128)(2,1)} %param.24, bf16[32,1408]{1,0:T(8,128)(2,1)} %param.23), kind=kLoop, calls=%fused_computation.2 | loop fusion | flops 811008 | bytes 540672 | tf_op jit(solution)/shard_map/concatenate | solution.py:370
  10.9 2.5 %collective-permute-start.4 = (bf16[256,512]{1,0:T(8,128)(2,1)S(1)}, bf16[256,512]{1,0:T(8,128)(2,1)S(1)}, u32[]{:S(2)}, u32[]{:S(2)}) collective-permute-start(bf16[256,512]{1,0:T(8,128)(2,1)S(1)} %constant_dynamic-update-slice_fusion.2.rest_0_), channel_id=1, source_target_pairs={{0,32},{32,64},{64,96},{96,128},{128,160},{160,192},{192,224},{224... | collective-permute-start | bytes 786440 | tf_op jit(solution)/shard_map/ppermute | solution.py:25
  13.5 4.0 %collective-permute-start.7 = (bf16[256,512]{1,0:T(8,128)(2,1)S(1)}, bf16[256,512]{1,0:T(8,128)(2,1)S(1)}, u32[]{:S(2)}, u32[]{:S(2)}) collective-permute-start(bf16[256,512]{1,0:T(8,128)(2,1)S(1)} %constant_dynamic-update-slice_fusion.2.rest_0_), channel_id=1, source_target_pairs={{0,224},{32,0},{64,32},{96,64},{128,96},{160,128},{192,160},{224,1... | collective-permute-start | bytes 786440 | tf_op jit(solution)/shard_map/ppermute | solution.py:25
  17.6 1.4 collective-permute-start
  18.9 2.6 %collective-permute-start.1 = (bf16[256,256]{1,0:T(8,128)(2,1)S(1)}, bf16[256,256]{1,0:T(8,128)(2,1)S(1)}, u32[]{:S(2)}, u32[]{:S(2)}) collective-permute-start(bf16[256,256]{1,0:T(8,128)(2,1)S(1)} %constant_dynamic-update-slice_fusion), channel_id=1, source_target_pairs={{0,16},{8,24},{16,0},{24,8},{1,17},{9,25},{17,1},{25,9},{2,18},{10... | collective-permute-start | bytes 393224 | tf_op jit(solution)/shard_map/ppermute | solution.py:25
  23.4 2.7 %collective-permute-start.8 = (bf16[256,512]{1,0:T(8,128)(2,1)S(1)}, bf16[256,512]{1,0:T(8,128)(2,1)S(1)}, u32[]{:S(2)}, u32[]{:S(2)}) collective-permute-start(bf16[256,512]{1,0:T(8,128)(2,1)S(1)} %collective-permute-done.7.rest_2_), channel_id=1, source_target_pairs={{0,224},{32,0},{64,32},{96,64},{128,96},{160,128},{192,160},{224,1... | collective-permute-start | bytes 786440 | tf_op jit(solution)/shard_map/ppermute | solution.py:25
  27.1 1.9 %collective-permute-start.3 = (bf16[4,256,256]{2,1,0:T(8,128)(2,1)S(1)}, bf16[4,256,256]{2,1,0:T(8,128)(2,1)S(1)}, u32[]{:S(2)}, u32[]{:S(2)}) collective-permute-start(bf16[4,256,256]{2,1,0:T(8,128)(2,1)S(1)} %pad_maximum_fusion.q_ref), channel_id=1, source_target_pairs={{0,4},{4,0},{1,5},{5,1},{2,6},{6,2},{3,7},{7,3},{8,12},{12,8},{9,1... | collective-permute-start | bytes 1572872 | tf_op jit(solution)/shard_map/ppermute | solution.py:25
  29.0 2.4 %collective-permute-done.5.rest_3_ = bf16[256,512]{1,0:T(8,128)(2,1)S(1)} collective-permute-done((bf16[256,512]{1,0:T(8,128)(2,1)S(1)}, bf16[256,512]{1,0:T(8,128)(2,1)S(1)}, u32[]{:S(2)}, u32[]{:S(2)}) %collective-permute-start.5) | collective-permute-done | bytes 262176 | tf_op jit(solution)/shard_map/ppermute | solution.py:25
  32.4 3.4 %collective-permute-start.9 = (bf16[256,512]{1,0:T(8,128)(2,1)S(1)}, bf16[256,512]{1,0:T(8,128)(2,1)S(1)}, u32[]{:S(2)}, u32[]{:S(2)}) collective-permute-start(bf16[256,512]{1,0:T(8,128)(2,1)S(1)} %collective-permute-done.8.rest_4_), channel_id=1, source_target_pairs={{0,224},{32,0},{64,32},{96,64},{128,96},{160,128},{192,160},{224,1... | collective-permute-start | bytes 786440 | tf_op jit(solution)/shard_map/ppermute | solution.py:25
  35.9 5.6 %collective-permute-done.6.rest_0_ = bf16[256,512]{1,0:T(8,128)(2,1)S(1)} collective-permute-done((bf16[256,512]{1,0:T(8,128)(2,1)S(1)}, bf16[256,512]{1,0:T(8,128)(2,1)S(1)}, u32[]{:S(2)}, u32[]{:S(2)}) %collective-permute-start.6) | collective-permute-done | bytes 262176 | tf_op jit(solution)/shard_map/ppermute | solution.py:25
  42.3 3.6 %collective-permute-start.11 = (bf16[128,512]{1,0:T(8,128)(2,1)S(1)}, bf16[128,512]{1,0:T(8,128)(2,1)S(1)}, u32[]{:S(2)}, u32[]{:S(2)}) collective-permute-start(bf16[128,512]{1,0:T(8,128)(2,1)S(1)} %slice.41), channel_id=1, source_target_pairs={{0,224},{32,0},{64,32},{96,64},{128,96},{160,128},{192,160},{224,1... | collective-permute-start | bytes 393224 | tf_op jit(solution)/shard_map/ppermute | solution.py:25
  45.9 12.1 %shard_map.127 = (bf16[4,272,512]{2,1,0:T(8,128)(2,1)S(1)}, bf16[4,272,512]{2,1,0:T(8,128)(2,1)S(1)}) custom-call(s32[4]{0:T(128)S(1)} %pad_add_fusion.where_ref, bf16[4,256,256]{2,1,0:T(8,128)(2,1)S(1)} %pad_maximum_fusion.q_ref, bf16[4,256,256]{2,1,0:T(8,128)(2,1)S(1)} %collective-permute-done.3.other_q_ref, ...), custom_call_target="tpu_custom_call" | custom-call | flops 4026531840 | bytes 4194304 | tf_op jit(solution)/shard_map/pallas_call | solution.py:147
  58.0 8.6 %shard_map.128 = (bf16[4,272,512]{2,1,0:T(8,128)(2,1)S(1)}, bf16[4,272,512]{2,1,0:T(8,128)(2,1)S(1)}) custom-call(s32[4]{0:T(128)S(1)} %pad_add_fusion.where_ref, bf16[4,256,256]{2,1,0:T(8,128)(2,1)S(1)} %pad_maximum_fusion.q_ref, bf16[4,256,256]{2,1,0:T(8,128)(2,1)S(1)} %collective-permute-done.3.other_q_ref, ...), custom_call_target="tpu_custom_call" | custom-call | flops 2415919104 | bytes 4194304 | tf_op jit(solution)/shard_map/pallas_call | solution.py:147
  66.7 4.2 %collective-permute-start.12 = (bf16[4,272,512]{2,1,0:T(8,128)(2,1)S(1)}, bf16[4,272,512]{2,1,0:T(8,128)(2,1)S(1)}, u32[]{:S(2)}, u32[]{:S(2)}) collective-permute-start(bf16[4,272,512]{2,1,0:T(8,128)(2,1)S(1)} %get-tuple-element.23), channel_id=1, source_target_pairs={{0,4},{4,0},{1,5},{5,1},{2,6},{6,2},{3,7},{7,3},{8,12},{12,8},{9,1... | collective-permute-start | bytes 3342344 | tf_op jit(solution)/shard_map/ppermute | solution.py:25
  73.9 1.5 collective-permute-start.21
  76.4 3.8 %merge_cores.1 = (bf16[272,512]{1,0:T(8,128)(2,1)}, bf16[272,512]{1,0:T(8,128)(2,1)}, bf16[272,512]{1,0:T(8,128)(2,1)}, bf16[272,512]{1,0:T(8,128)(2,1)}) custom-call(bf16[4,272,512]{2,1,0:T(8,128)(2,1)} %copy-done.9, bf16[4,272,512]{2,1,0:T(8,128)(2,1)} %copy-done.12), custom_call_target="tpu_custom_call" | custom-call | flops 4000000000 | bytes 3342336 | tf_op jit(solution)/shard_map/merge_cores/pallas_call | solution.py:194
  80.1 3.4 %collective-permute-start.13 = (bf16[272,512]{1,0:T(8,128)(2,1)}, bf16[272,512]{1,0:T(8,128)(2,1)S(1)}, u32[]{:S(2)}, u32[]{:S(2)}) collective-permute-start(bf16[272,512]{1,0:T(8,128)(2,1)} %get-tuple-element.25), channel_id=1, source_target_pairs={{0,24},{8,0},{16,8},{24,16},{1,25},{9,1},{17,9},{25,17},{2,26},{10... | collective-permute-start | bytes 835592 | tf_op jit(solution)/shard_map/ppermute | solution.py:25
  84.9 19.6 %collective-permute-done.19.refs_6_ = bf16[256,2560]{1,0:T(8,128)(2,1)S(1)} collective-permute-done((bf16[256,2560]{1,0:T(8,128)(2,1)}, bf16[256,2560]{1,0:T(8,128)(2,1)S(1)}, u32[]{:S(2)}, u32[]{:S(2)}) %collective-permute-start.19) | collective-permute-done | bytes 1310752 | tf_op jit(solution)/shard_map/ppermute | solution.py:25
  105.4 2.0 %slice.43 = bf16[128,2560]{1,0:T(8,128)(2,1)} slice(bf16[256,2560]{1,0:T(8,128)(2,1)} %collective-permute-done.21.refs_9_), slice={[128:256], [0:2560]} | slice | bytes 1310720 | tf_op jit(solution)/shard_map/slice | solution.py:362
  107.3 2.7 %collective-permute-start.22 = (bf16[128,2560]{1,0:T(8,128)(2,1)}, bf16[128,2560]{1,0:T(8,128)(2,1)}, u32[]{:S(2)}, u32[]{:S(2)}) collective-permute-start(bf16[128,2560]{1,0:T(8,128)(2,1)} %slice.43), channel_id=1, source_target_pairs={{0,3},{1,0},{2,1},{3,2},{4,7},{5,4},{6,5},{7,6},{8,11},{9,8},{10,9... | collective-permute-start | bytes 1966088 | tf_op jit(solution)/shard_map/ppermute | solution.py:25
  111.6 2.7 %finish_heads.1.refs_0_ = bf16[256,256]{1,0:T(8,128)(2,1)} custom-call(f32[1]{0:T(128)S(6)} %copy.18.lam_ref, f32[1,256]{1,0:T(1,128)} %bitcast.17, bf16[272,512]{1,0:T(8,128)(2,1)} %get-tuple-element.24.refs_0_, bf16[272,512]{1,0:T(8,128)(2,1)} %copy-done.13, bf16[272,512]{1,0:T(8,128)(2,1)} %copy-done.14, bf16[272,512]{1,0:T(8,128)(2,1)} %copy-done.15), custom_call_target="tpu_custom_call" | custom-call | flops 4000000000 | bytes 2000000 | tf_op jit(solution)/shard_map/finish_heads/pallas_call | solution.py:214
  115.5 1.5 collective-permute-start.18
  117.0 5.4 %collective-permute-done.20.refs_7_ = bf16[128,2560]{1,0:T(8,128)(2,1)S(1)} collective-permute-done((bf16[128,2560]{1,0:T(8,128)(2,1)}, bf16[128,2560]{1,0:T(8,128)(2,1)S(1)}, u32[]{:S(2)}, u32[]{:S(2)}) %collective-permute-start.20) | collective-permute-done | bytes 655392 | tf_op jit(solution)/shard_map/ppermute | solution.py:25
  125.5 2.2 %collective-permute-done.17.refs_2_ = bf16[256,256]{1,0:T(8,128)(2,1)S(1)} collective-permute-done((bf16[256,256]{1,0:T(8,128)(2,1)}, bf16[256,256]{1,0:T(8,128)(2,1)S(1)}, u32[]{:S(2)}, u32[]{:S(2)}) %collective-permute-start.17) | collective-permute-done | bytes 131104 | tf_op jit(solution)/shard_map/ppermute | solution.py:25
  127.7 1.2 collective-permute-done.18.refs_3_
  131.8 3.7 %project_norm.1 = (bf16[256,512]{1,0:T(8,128)(2,1)S(1)}, bf16[256,2048]{1,0:T(8,128)(2,1)S(1)}) custom-call(s32[4]{0:T(128)S(1)} %pad_add_fusion.where_ref, f32[1,2048]{1,0:T(1,128)S(1)} %bitcast.11, bf16[256,256]{1,0:T(8,128)(2,1)S(1)} %copy-done.7, bf16[256,256]{1,0:T(8,128)(2,1)S(1)} %collective-permute-done.16.refs_1_, ...), custom_call_target="tpu_custom_call" | custom-call | flops 2000000000 | bytes 8000000 | tf_op jit(solution)/shard_map/project_norm/pallas_call | solution.py:266
  136.2 9.0 %mixer.1 = (bf16[128,512]{1,0:T(8,128)(2,1)S(1)}, bf16[128,512]{1,0:T(8,128)(2,1)S(1)}, bf16[256,512]{1,0:T(8,128)(2,1)S(1)}, bf16[256,512]{1,0:T(8,128)(2,1)S(1)}, bf16[256,512]{1,0:T(8,128)(2,1)S(1)}) custom-call(s32[4]{0:T(128)S(1)} %pad_add_fusion.where_ref, bf16[256,2048]{1,0:T(8,128)(2,1)S(1)} %get-tuple-element.29.normed_ref, ...), custom_call_target="tpu_custom_call" | custom-call | flops 4429185024 | bytes 18000000 | tf_op jit(solution)/shard_map/mixer/pallas_call | solution.py:338
  145.3 3.6 %collective-permute-start.27 = (bf16[128,512]{1,0:T(8,128)(2,1)S(1)}, bf16[128,512]{1,0:T(8,128)(2,1)S(1)}, u32[]{:S(2)}, u32[]{:S(2)}) collective-permute-start(bf16[128,512]{1,0:T(8,128)(2,1)S(1)} %get-tuple-element.34), channel_id=1, source_target_pairs={{0,3},{1,0},{2,1},{3,2},{4,7},{5,4},{6,5},{7,6},{8,11},{9,8},{10,9... | collective-permute-start | bytes 393224 | tf_op jit(solution)/shard_map/ppermute | solution.py:25
  148.9 2.8 %collective-permute-start.23 = (bf16[128,512]{1,0:T(8,128)(2,1)S(1)}, bf16[128,512]{1,0:T(8,128)(2,1)S(1)}, u32[]{:S(2)}, u32[]{:S(2)}) collective-permute-start(bf16[128,512]{1,0:T(8,128)(2,1)S(1)} %slice.35), channel_id=1, source_target_pairs={{0,3},{1,0},{2,1},{3,2},{4,7},{5,4},{6,5},{7,6},{8,11},{9,8},{10,9... | collective-permute-start | bytes 393224 | tf_op jit(solution)/shard_map/ppermute | solution.py:25
  151.9 2.7 %collective-permute-start.28 = (bf16[128,512]{1,0:T(8,128)(2,1)S(1)}, bf16[128,512]{1,0:T(8,128)(2,1)S(1)}, u32[]{:S(2)}, u32[]{:S(2)}) collective-permute-start(bf16[128,512]{1,0:T(8,128)(2,1)S(1)} %add_convert_fusion), channel_id=1, source_target_pairs={{0,3},{1,0},{2,1},{3,2},{4,7},{5,4},{6,5},{7,6},{8,11},{9,8},{10,9... | collective-permute-start | bytes 393224 | tf_op jit(solution)/shard_map/ppermute | solution.py:25
  154.8 3.1 %collective-permute-done.26 = bf16[128,512]{1,0:T(8,128)(2,1)S(1)} collective-permute-done((bf16[128,512]{1,0:T(8,128)(2,1)S(1)}, bf16[128,512]{1,0:T(8,128)(2,1)S(1)}, u32[]{:S(2)}, u32[]{:S(2)}) %collective-permute-start.26) | collective-permute-done | bytes 131104 | tf_op jit(solution)/shard_map/ppermute | solution.py:25
  157.9 3.3 %collective-permute-done.25 = bf16[128,512]{1,0:T(8,128)(2,1)S(1)} collective-permute-done((bf16[128,512]{1,0:T(8,128)(2,1)S(1)}, bf16[128,512]{1,0:T(8,128)(2,1)S(1)}, u32[]{:S(2)}, u32[]{:S(2)}) %collective-permute-start.25) | collective-permute-done | bytes 131104 | tf_op jit(solution)/shard_map/ppermute | solution.py:25
  (88 shorter events, 23.7 us)
Async XLA Ops:
  6.5 129.7 %all-gather.2.cloned.1.call-start = ((), (), s32[]{:S(2)}) async-start(), calls=%async_computation | async-start | bytes 17571840 | tf_op jit(solution)/shard_map/all_gather | solution.py:371
  10.9 12.5 %collective-permute-start.4 = (bf16[256,512]{1,0:T(8,128)(2,1)S(1)}, bf16[256,512]{1,0:T(8,128)(2,1)S(1)}, u32[]{:S(2)}, u32[]{:S(2)}) collective-permute-start(bf16[256,512]{1,0:T(8,128)(2,1)S(1)} %constant_dynamic-update-slice_fusion.2.rest_0_), channel_id=1, source_target_pairs={{0,32},{32,64},{64,96},{96,128},{128,160},{160,192},{192,224},{224... | collective-permute-start | bytes 786440 | tf_op jit(solution)/shard_map/ppermute | solution.py:25
  13.5 10.0 %collective-permute-start.7 = (bf16[256,512]{1,0:T(8,128)(2,1)S(1)}, bf16[256,512]{1,0:T(8,128)(2,1)S(1)}, u32[]{:S(2)}, u32[]{:S(2)}) collective-permute-start(bf16[256,512]{1,0:T(8,128)(2,1)S(1)} %constant_dynamic-update-slice_fusion.2.rest_0_), channel_id=1, source_target_pairs={{0,224},{32,0},{64,32},{96,64},{128,96},{160,128},{192,160},{224,1... | collective-permute-start | bytes 786440 | tf_op jit(solution)/shard_map/ppermute | solution.py:25
  17.6 8.6 %collective-permute-start = (bf16[256,256]{1,0:T(8,128)(2,1)S(1)}, bf16[256,256]{1,0:T(8,128)(2,1)S(1)}, u32[]{:S(2)}, u32[]{:S(2)}) collective-permute-start(bf16[256,256]{1,0:T(8,128)(2,1)S(1)} %constant_dynamic-update-slice_fusion), channel_id=1, source_target_pairs={{0,8},{8,16},{16,24},{24,0},{1,9},{9,17},{17,25},{25,1},{2,10},{10... | collective-permute-start | bytes 393224 | tf_op jit(solution)/shard_map/ppermute | solution.py:25
  18.9 7.8 %collective-permute-start.1 = (bf16[256,256]{1,0:T(8,128)(2,1)S(1)}, bf16[256,256]{1,0:T(8,128)(2,1)S(1)}, u32[]{:S(2)}, u32[]{:S(2)}) collective-permute-start(bf16[256,256]{1,0:T(8,128)(2,1)S(1)} %constant_dynamic-update-slice_fusion), channel_id=1, source_target_pairs={{0,16},{8,24},{16,0},{24,8},{1,17},{9,25},{17,1},{25,9},{2,18},{10... | collective-permute-start | bytes 393224 | tf_op jit(solution)/shard_map/ppermute | solution.py:25
  21.5 5.5 %collective-permute-start.2 = (bf16[256,256]{1,0:T(8,128)(2,1)S(1)}, bf16[256,256]{1,0:T(8,128)(2,1)S(1)}, u32[]{:S(2)}, u32[]{:S(2)}) collective-permute-start(bf16[256,256]{1,0:T(8,128)(2,1)S(1)} %constant_dynamic-update-slice_fusion), channel_id=1, source_target_pairs={{0,24},{8,0},{16,8},{24,16},{1,25},{9,1},{17,9},{25,17},{2,26},{10... | collective-permute-start | bytes 393224 | tf_op jit(solution)/shard_map/ppermute | solution.py:25
  23.4 7.9 %collective-permute-start.5 = (bf16[256,512]{1,0:T(8,128)(2,1)S(1)}, bf16[256,512]{1,0:T(8,128)(2,1)S(1)}, u32[]{:S(2)}, u32[]{:S(2)}) collective-permute-start(bf16[256,512]{1,0:T(8,128)(2,1)S(1)} %collective-permute-done.4.rest_1_), channel_id=1, source_target_pairs={{0,32},{32,64},{64,96},{96,128},{128,160},{160,192},{192,224},{224... | collective-permute-start | bytes 786440 | tf_op jit(solution)/shard_map/ppermute | solution.py:25
  23.4 9.0 %collective-permute-start.8 = (bf16[256,512]{1,0:T(8,128)(2,1)S(1)}, bf16[256,512]{1,0:T(8,128)(2,1)S(1)}, u32[]{:S(2)}, u32[]{:S(2)}) collective-permute-start(bf16[256,512]{1,0:T(8,128)(2,1)S(1)} %collective-permute-done.7.rest_2_), channel_id=1, source_target_pairs={{0,224},{32,0},{64,32},{96,64},{128,96},{160,128},{192,160},{224,1... | collective-permute-start | bytes 786440 | tf_op jit(solution)/shard_map/ppermute | solution.py:25
  27.1 18.8 %collective-permute-start.3 = (bf16[4,256,256]{2,1,0:T(8,128)(2,1)S(1)}, bf16[4,256,256]{2,1,0:T(8,128)(2,1)S(1)}, u32[]{:S(2)}, u32[]{:S(2)}) collective-permute-start(bf16[4,256,256]{2,1,0:T(8,128)(2,1)S(1)} %pad_maximum_fusion.q_ref), channel_id=1, source_target_pairs={{0,4},{4,0},{1,5},{5,1},{2,6},{6,2},{3,7},{7,3},{8,12},{12,8},{9,1... | collective-permute-start | bytes 1572872 | tf_op jit(solution)/shard_map/ppermute | solution.py:25
  31.3 10.1 %collective-permute-start.6 = (bf16[256,512]{1,0:T(8,128)(2,1)S(1)}, bf16[256,512]{1,0:T(8,128)(2,1)S(1)}, u32[]{:S(2)}, u32[]{:S(2)}) collective-permute-start(bf16[256,512]{1,0:T(8,128)(2,1)S(1)} %collective-permute-done.5.rest_3_), channel_id=1, source_target_pairs={{0,32},{32,64},{64,96},{96,128},{128,160},{160,192},{192,224},{224... | collective-permute-start | bytes 786440 | tf_op jit(solution)/shard_map/ppermute | solution.py:25
  32.4 9.8 %collective-permute-start.9 = (bf16[256,512]{1,0:T(8,128)(2,1)S(1)}, bf16[256,512]{1,0:T(8,128)(2,1)S(1)}, u32[]{:S(2)}, u32[]{:S(2)}) collective-permute-start(bf16[256,512]{1,0:T(8,128)(2,1)S(1)} %collective-permute-done.8.rest_4_), channel_id=1, source_target_pairs={{0,224},{32,0},{64,32},{96,64},{128,96},{160,128},{192,160},{224,1... | collective-permute-start | bytes 786440 | tf_op jit(solution)/shard_map/ppermute | solution.py:25
  41.5 16.5 %collective-permute-start.10 = (bf16[128,512]{1,0:T(8,128)(2,1)S(1)}, bf16[128,512]{1,0:T(8,128)(2,1)S(1)}, u32[]{:S(2)}, u32[]{:S(2)}) collective-permute-start(bf16[128,512]{1,0:T(8,128)(2,1)S(1)} %slice.40), channel_id=1, source_target_pairs={{0,32},{32,64},{64,96},{96,128},{128,160},{160,192},{192,224},{224... | collective-permute-start | bytes 393224 | tf_op jit(solution)/shard_map/ppermute | solution.py:25
  42.3 15.7 %collective-permute-start.11 = (bf16[128,512]{1,0:T(8,128)(2,1)S(1)}, bf16[128,512]{1,0:T(8,128)(2,1)S(1)}, u32[]{:S(2)}, u32[]{:S(2)}) collective-permute-start(bf16[128,512]{1,0:T(8,128)(2,1)S(1)} %slice.41), channel_id=1, source_target_pairs={{0,224},{32,0},{64,32},{96,64},{128,96},{160,128},{192,160},{224,1... | collective-permute-start | bytes 393224 | tf_op jit(solution)/shard_map/ppermute | solution.py:25
  58.0 12.9 %copy-start = (bf16[256,2048]{1,0:T(8,128)(2,1)S(1)}, bf16[256,2048]{1,0:T(8,128)(2,1)}, u32[]{:S(2)}) copy-start(bf16[256,2048]{1,0:T(8,128)(2,1)} %refs_4_.1) | copy-start | bytes 3145732
  66.7 8.7 %collective-permute-start.12 = (bf16[4,272,512]{2,1,0:T(8,128)(2,1)S(1)}, bf16[4,272,512]{2,1,0:T(8,128)(2,1)S(1)}, u32[]{:S(2)}, u32[]{:S(2)}) collective-permute-start(bf16[4,272,512]{2,1,0:T(8,128)(2,1)S(1)} %get-tuple-element.23), channel_id=1, source_target_pairs={{0,4},{4,0},{1,5},{5,1},{2,6},{6,2},{3,7},{7,3},{8,12},{12,8},{9,1... | collective-permute-start | bytes 3342344 | tf_op jit(solution)/shard_map/ppermute | solution.py:25
  72.7 31.8 %collective-permute-start.19 = (bf16[256,2560]{1,0:T(8,128)(2,1)}, bf16[256,2560]{1,0:T(8,128)(2,1)S(1)}, u32[]{:S(2)}, u32[]{:S(2)}) collective-permute-start(bf16[256,2560]{1,0:T(8,128)(2,1)} %constant_dynamic-update-slice_fusion.5), channel_id=1, source_target_pairs={{0,1},{1,2},{2,3},{3,0},{4,5},{5,6},{6,7},{7,4},{8,9},{9,10},{10,1... | collective-permute-start | bytes 3932168 | tf_op jit(solution)/shard_map/ppermute | solution.py:25
  73.9 31.5 %collective-permute-start.21 = (bf16[256,2560]{1,0:T(8,128)(2,1)}, bf16[256,2560]{1,0:T(8,128)(2,1)}, u32[]{:S(2)}, u32[]{:S(2)}) collective-permute-start(bf16[256,2560]{1,0:T(8,128)(2,1)} %constant_dynamic-update-slice_fusion.5), channel_id=1, source_target_pairs={{0,3},{1,0},{2,1},{3,2},{4,7},{5,4},{6,5},{7,6},{8,11},{9,8},{10,9... | collective-permute-start | bytes 3932168 | tf_op jit(solution)/shard_map/ppermute | solution.py:25
  80.1 30.6 %collective-permute-start.13 = (bf16[272,512]{1,0:T(8,128)(2,1)}, bf16[272,512]{1,0:T(8,128)(2,1)S(1)}, u32[]{:S(2)}, u32[]{:S(2)}) collective-permute-start(bf16[272,512]{1,0:T(8,128)(2,1)} %get-tuple-element.25), channel_id=1, source_target_pairs={{0,24},{8,0},{16,8},{24,16},{1,25},{9,1},{17,9},{25,17},{2,26},{10... | collective-permute-start | bytes 835592 | tf_op jit(solution)/shard_map/ppermute | solution.py:25
  83.5 27.2 %collective-permute-start.14 = (bf16[272,512]{1,0:T(8,128)(2,1)}, bf16[272,512]{1,0:T(8,128)(2,1)S(1)}, u32[]{:S(2)}, u32[]{:S(2)}) collective-permute-start(bf16[272,512]{1,0:T(8,128)(2,1)} %get-tuple-element.26), channel_id=1, source_target_pairs={{0,16},{8,24},{16,0},{24,8},{1,17},{9,25},{17,1},{25,9},{2,18},{10... | collective-permute-start | bytes 835592 | tf_op jit(solution)/shard_map/ppermute | solution.py:25
  84.3 26.4 %collective-permute-start.15 = (bf16[272,512]{1,0:T(8,128)(2,1)}, bf16[272,512]{1,0:T(8,128)(2,1)S(1)}, u32[]{:S(2)}, u32[]{:S(2)}) collective-permute-start(bf16[272,512]{1,0:T(8,128)(2,1)} %get-tuple-element.27), channel_id=1, source_target_pairs={{0,8},{8,16},{16,24},{24,0},{1,9},{9,17},{17,25},{25,1},{2,10},{10... | collective-permute-start | bytes 835592 | tf_op jit(solution)/shard_map/ppermute | solution.py:25
  105.4 17.0 %collective-permute-start.20 = (bf16[128,2560]{1,0:T(8,128)(2,1)}, bf16[128,2560]{1,0:T(8,128)(2,1)S(1)}, u32[]{:S(2)}, u32[]{:S(2)}) collective-permute-start(bf16[128,2560]{1,0:T(8,128)(2,1)} %slice.42), channel_id=1, source_target_pairs={{0,1},{1,2},{2,3},{3,0},{4,5},{5,6},{6,7},{7,4},{8,9},{9,10},{10,1... | collective-permute-start | bytes 1966088 | tf_op jit(solution)/shard_map/ppermute | solution.py:25
  107.3 17.1 %collective-permute-start.22 = (bf16[128,2560]{1,0:T(8,128)(2,1)}, bf16[128,2560]{1,0:T(8,128)(2,1)}, u32[]{:S(2)}, u32[]{:S(2)}) collective-permute-start(bf16[128,2560]{1,0:T(8,128)(2,1)} %slice.43), channel_id=1, source_target_pairs={{0,3},{1,0},{2,1},{3,2},{4,7},{5,4},{6,5},{7,6},{8,11},{9,8},{10,9... | collective-permute-start | bytes 1966088 | tf_op jit(solution)/shard_map/ppermute | solution.py:25
  111.6 17.3 %copy-start.8 = (f32[2048]{0:T(1024)S(1)}, f32[2048]{0:T(1024)}, u32[]{:S(2)}) copy-start(f32[2048]{0:T(1024)} %param.22) | copy-start | bytes 24580
  114.3 11.1 %collective-permute-start.16 = (bf16[256,256]{1,0:T(8,128)(2,1)}, bf16[256,256]{1,0:T(8,128)(2,1)S(1)}, u32[]{:S(2)}, u32[]{:S(2)}) collective-permute-start(bf16[256,256]{1,0:T(8,128)(2,1)} %finish_heads.1.refs_0_), channel_id=1, source_target_pairs={{0,1},{1,2},{2,3},{3,0},{4,5},{5,6},{6,7},{7,4},{8,9},{9,10},{10,1... | collective-permute-start | bytes 393224 | tf_op jit(solution)/shard_map/ppermute | solution.py:25
  114.3 13.3 %collective-permute-start.17 = (bf16[256,256]{1,0:T(8,128)(2,1)}, bf16[256,256]{1,0:T(8,128)(2,1)S(1)}, u32[]{:S(2)}, u32[]{:S(2)}) collective-permute-start(bf16[256,256]{1,0:T(8,128)(2,1)} %finish_heads.1.refs_0_), channel_id=1, source_target_pairs={{0,2},{1,3},{2,0},{3,1},{4,6},{5,7},{6,4},{7,5},{8,10},{9,11},{10,... | collective-permute-start | bytes 393224 | tf_op jit(solution)/shard_map/ppermute | solution.py:25
  115.5 13.3 %collective-permute-start.18 = (bf16[256,256]{1,0:T(8,128)(2,1)}, bf16[256,256]{1,0:T(8,128)(2,1)S(1)}, u32[]{:S(2)}, u32[]{:S(2)}) collective-permute-start(bf16[256,256]{1,0:T(8,128)(2,1)} %finish_heads.1.refs_0_), channel_id=1, source_target_pairs={{0,3},{1,0},{2,1},{3,2},{4,7},{5,4},{6,5},{7,6},{8,11},{9,8},{10,9... | collective-permute-start | bytes 393224 | tf_op jit(solution)/shard_map/ppermute | solution.py:25
  145.3 6.5 %collective-permute-start.27 = (bf16[128,512]{1,0:T(8,128)(2,1)S(1)}, bf16[128,512]{1,0:T(8,128)(2,1)S(1)}, u32[]{:S(2)}, u32[]{:S(2)}) collective-permute-start(bf16[128,512]{1,0:T(8,128)(2,1)S(1)} %get-tuple-element.34), channel_id=1, source_target_pairs={{0,3},{1,0},{2,1},{3,2},{4,7},{5,4},{6,5},{7,6},{8,11},{9,8},{10,9... | collective-permute-start | bytes 393224 | tf_op jit(solution)/shard_map/ppermute | solution.py:25
  148.9 5.7 %collective-permute-start.24 = (bf16[128,512]{1,0:T(8,128)(2,1)S(1)}, bf16[128,512]{1,0:T(8,128)(2,1)S(1)}, u32[]{:S(2)}, u32[]{:S(2)}) collective-permute-start(bf16[128,512]{1,0:T(8,128)(2,1)S(1)} %get-tuple-element.33), channel_id=1, source_target_pairs={{0,1},{1,2},{2,3},{3,0},{4,5},{5,6},{6,7},{7,4},{8,9},{9,10},{10,1... | collective-permute-start | bytes 393224 | tf_op jit(solution)/shard_map/ppermute | solution.py:25
  148.9 5.9 %collective-permute-start.23 = (bf16[128,512]{1,0:T(8,128)(2,1)S(1)}, bf16[128,512]{1,0:T(8,128)(2,1)S(1)}, u32[]{:S(2)}, u32[]{:S(2)}) collective-permute-start(bf16[128,512]{1,0:T(8,128)(2,1)S(1)} %slice.35), channel_id=1, source_target_pairs={{0,3},{1,0},{2,1},{3,2},{4,7},{5,4},{6,5},{7,6},{8,11},{9,8},{10,9... | collective-permute-start | bytes 393224 | tf_op jit(solution)/shard_map/ppermute | solution.py:25
  151.7 6.2 %collective-permute-start.26 = (bf16[128,512]{1,0:T(8,128)(2,1)S(1)}, bf16[128,512]{1,0:T(8,128)(2,1)S(1)}, u32[]{:S(2)}, u32[]{:S(2)}) collective-permute-start(bf16[128,512]{1,0:T(8,128)(2,1)S(1)} %slice.38), channel_id=1, source_target_pairs={{0,1},{1,2},{2,3},{3,0},{4,5},{5,6},{6,7},{7,4},{8,9},{9,10},{10,1... | collective-permute-start | bytes 393224 | tf_op jit(solution)/shard_map/ppermute | solution.py:25
  151.9 6.0 %collective-permute-start.28 = (bf16[128,512]{1,0:T(8,128)(2,1)S(1)}, bf16[128,512]{1,0:T(8,128)(2,1)S(1)}, u32[]{:S(2)}, u32[]{:S(2)}) collective-permute-start(bf16[128,512]{1,0:T(8,128)(2,1)S(1)} %add_convert_fusion), channel_id=1, source_target_pairs={{0,3},{1,0},{2,1},{3,2},{4,7},{5,4},{6,5},{7,6},{8,11},{9,8},{10,9... | collective-permute-start | bytes 393224 | tf_op jit(solution)/shard_map/ppermute | solution.py:25
  154.6 6.6 %collective-permute-start.25 = (bf16[128,512]{1,0:T(8,128)(2,1)S(1)}, bf16[128,512]{1,0:T(8,128)(2,1)S(1)}, u32[]{:S(2)}, u32[]{:S(2)}) collective-permute-start(bf16[128,512]{1,0:T(8,128)(2,1)S(1)} %add_convert_fusion.1), channel_id=1, source_target_pairs={{0,1},{1,2},{2,3},{3,0},{4,5},{5,6},{6,7},{7,4},{8,9},{9,10},{10,1... | collective-permute-start | bytes 393224 | tf_op jit(solution)/shard_map/ppermute | solution.py:25
  (14 other events, 50.7 us)
Sparse Core Ops, SparseCore 0:
  10.1 117.9 all-gather.1
where the time goes:
time: 172 us; the launch traced here: 169 us
  starting transfers between devices  49.6 us (29%)
  waiting for transfers between devices  48.5 us (28%)
  Pallas kernels  39.9 us (23%)
  between operations  14.3 us (8%)
  local copies, waits for them, and re-layouts  13.7 us (8%)
  other arithmetic  2.85 us (2%)
    ppermute x29, starting transfers between devices, shift(): return lax.ppermute(a, axis, [(i, (i + by) % count) for i in range(count)])  49.6 us
    ppermute x29, waiting for transfers between devices, shift(): return lax.ppermute(a, axis, [(i, (i + by) % count) for i in range(count)])  48.5 us
    pallas_call x2, Pallas kernels, attention(): pl.pallas_call(functools.partial(attention_kernel, steps, bool(before)),...  20.7 us
    unnamed x36, local copies, waits for them, and re-layouts  9.18 us
    pallas_call x1, Pallas kernels, mixer(): pl.pallas_call(mixer_kernel, out_shape=(part, part, whole, whole, whole),...  9.03 us
    pallas_call x1, Pallas kernels, merge_cores(): pl.pallas_call(merge_kernel, out_shape=(jax.ShapeDtypeStruct((rows, width...  3.75 us
    pallas_call x1, Pallas kernels, project(): pl.pallas_call(project_kernel, out_shape=(jax.ShapeDtypeStruct((tok, bloc...  3.71 us
  transfers between devices with their start and end apart: 30, of which 15 were waited for; matrix products, arithmetic and copies ran while one was open for 5% of the time, Pallas kernels for 18%

commit v1 on v0

--- a/solution.py
+++ b/solution.py
@@ -154,7 +154,7 @@
         + [spec] * len(before),
         out_specs=[spec, spec],
         scratch_shapes=[pltpu.VMEM((rows, keys), jnp.float32)],
-        compiler_params=pltpu.CompilerParams(vmem_limit_bytes=32 * 1024 * 1024),
+        compiler_params=pltpu.CompilerParams(vmem_limit_bytes=20 * 1024 * 1024),
         cost_estimate=pl.CostEstimate(
             flops=flops, bytes_accessed=4 * 1024 * 1024, transcendentals=2 * count * rows * keys
         ),
@@ -196,6 +196,7 @@
         out_shape=(jax.ShapeDtypeStruct((rows, width), jnp.bfloat16),) * count,
         in_specs=[VMEM, VMEM],
         out_specs=(VMEM,) * count,
+        compiler_params=pltpu.CompilerParams(vmem_limit_bytes=10 * 1024 * 1024),
         cost_estimate=pl.CostEstimate(flops=4_000_000_000, bytes_accessed=3 * a.size * 2, transcendentals=0),
         name="merge_cores",
     )(a, b)
@@ -216,38 +217,37 @@
         out_shape=jax.ShapeDtypeStruct((tok, 2 * HEAD), jnp.bfloat16),
         in_specs=[SMEM] + [VMEM] * (1 + len(blocks)),
         out_specs=VMEM,
+        compiler_params=pltpu.CompilerParams(vmem_limit_bytes=8 * 1024 * 1024),
         cost_estimate=pl.CostEstimate(flops=4_000_000_000, bytes_accessed=2_000_000, transcendentals=0),
         name="finish_heads",
     )(lam, gain.reshape(1, -1), *blocks)
 
 
 def project_kernel(where_ref, gain_ref, *refs):
-    att, (ow_ref, res_ref), extra = refs[:4], refs[4:6], refs[6:10]
-    own_ref, normed_ref, sum_ref = refs[10:]
+    att, (ow_ref, res_ref), extra = refs[:4], refs[4:6], refs[6:12]
+    own_ref, normed_ref, sum_ref = refs[12:]
     x = where_ref[3]
     tok, block = res_ref.shape
     width = ow_ref.shape[1]
     half = tok // 2
-    left, low, high, right = extra
 
     def at(s):
         return pl.ds(pl.multiple_of(lax.rem(x - s + 4, 4) * block, block), block)
 
     sum_ref[:, at(0)] = res_ref[...].astype(jnp.float32)
-    sum_ref[:, at(1)] = left[:, width:].astype(jnp.float32)
-    sum_ref[:half, at(2)] = low[:, width:].astype(jnp.float32)
-    sum_ref[half:, at(2)] = high[:, width:].astype(jnp.float32)
-    sum_ref[:, at(3)] = right[:, width:].astype(jnp.float32)
+    for s in range(3):
+        sum_ref[:half, at(s + 1)] = extra[2 * s][:, width:].astype(jnp.float32)
+        sum_ref[half:, at(s + 1)] = extra[2 * s + 1][:, width:].astype(jnp.float32)
     square = jnp.zeros((tok, 1), jnp.float32)
     for k in range(0, width, block):
         cols = slice(k, k + block)
         acc = sum_ref[:, cols]
-        parts = (
-            dot_nn(att[0][...], ow_ref[:, cols]),
-            dot_nn(att[1][...], left[:, cols]),
-            dot_nn(att[2][:, :half], low[:, cols]) + dot_nn(att[2][:, half:], high[:, cols]),
-            dot_nn(att[3][...], right[:, cols]),
-        )
+        parts = [dot_nn(att[0][...], ow_ref[:, cols])]
+        for s in range(3):
+            low, high = extra[2 * s], extra[2 * s + 1]
+            parts.append(
+                dot_nn(att[s + 1][:, :half], low[:, cols]) + dot_nn(att[s + 1][:, half:], high[:, cols])
+            )
         total = None
         for part in parts:
             part = part.astype(jnp.bfloat16).astype(jnp.float32)
@@ -269,20 +269,22 @@
             jax.ShapeDtypeStruct((tok, block), jnp.bfloat16),
             jax.ShapeDtypeStruct((tok, width), jnp.bfloat16),
         ),
-        in_specs=[SMEM] + [VMEM] * 11,
+        in_specs=[SMEM] + [VMEM] * 13,
         out_specs=(VMEM, VMEM),
         scratch_shapes=[pltpu.VMEM((tok, width), jnp.float32)],
-        compiler_params=pltpu.CompilerParams(vmem_limit_bytes=32 * 1024 * 1024),
+        compiler_params=pltpu.CompilerParams(vmem_limit_bytes=16 * 1024 * 1024),
         cost_estimate=pl.CostEstimate(flops=2_000_000_000, bytes_accessed=8_000_000, transcendentals=0),
         name="project_norm",
     )(where, gain.reshape(1, -1), *att, ow, res, *extra)
 
 
-def mixer_kernel(where_ref, normed_ref, full_ref, lo_ref, hi_ref, one_ref, three_ref, here_ref, w_ref, d_ref, h_ref, sems):
+def mixer_kernel(
+    where_ref, normed_ref, full_ref, plus_ref, minus_ref, one_ref, three_ref, here_ref, w_ref, d_ref, h_ref, sems
+):
     count, _, width = w_ref.shape
     _, block, units = d_ref.shape
     lane = width // 2
-    half = lo_ref.shape[0]
+    half = one_ref.shape[0]
 
     def copies(j):
         at = pl.multiple_of(j * lane, lane)
@@ -321,11 +323,14 @@
 
     for n, s in enumerate(ahead):
         down_copy(n, s).wait()
-    two = dot_nt(h_ref[...], d_ref[0]).astype(jnp.bfloat16)
-    lo_ref[...] = two[:half]
-    hi_ref[...] = two[half:]
-    for n, ref in enumerate((one_ref, three_ref, here_ref)):
-        ref[...] = dot_nt(h_ref[...], d_ref[n + 1]).astype(jnp.bfloat16)
+    two, one, three, here = (dot_nt(h_ref[...], d_ref[n]).astype(jnp.bfloat16) for n in range(4))
+    plus_ref[:half] = two[:half]
+    plus_ref[half:] = one[half:]
+    minus_ref[:half] = two[half:]
+    minus_ref[half:] = three[:half]
+    one_ref[...] = one[:half]
+    three_ref[...] = three[half:]
+    here_ref[...] = here
 
 
 def mixer(where, normed, full, block):
@@ -337,7 +342,7 @@
     part = jax.ShapeDtypeStruct((tok // 2, block), jnp.bfloat16)
     return pl.pallas_call(
         mixer_kernel,
-        out_shape=(part, part, whole, whole, whole),
+        out_shape=(whole, whole, part, part, whole),
         in_specs=[SMEM, VMEM, pl.BlockSpec(memory_space=pl.ANY)],
         out_specs=(VMEM,) * 5,
         scratch_shapes=[
@@ -346,7 +351,7 @@
             pltpu.VMEM((tok, units), jnp.bfloat16),
             pltpu.SemaphoreType.DMA((2, count + 4)),
         ],
-        compiler_params=pltpu.CompilerParams(vmem_limit_bytes=40 * 1024 * 1024),
+        compiler_params=pltpu.CompilerParams(vmem_limit_bytes=48 * 1024 * 1024),
         cost_estimate=pl.CostEstimate(
             flops=2 * tok * width * units * 3, bytes_accessed=18_000_000, transcendentals=tok * units
         ),
@@ -354,13 +359,13 @@
     )(where, normed, full)
 
 
-def both_ways(a, axis, count):
-    half = a.shape[0] // 2
-    left = shift(a, axis, count, 1)
-    right = shift(a, axis, count, -1)
-    low = shift(left[:half], axis, count, 1)
-    high = shift(right[half:], axis, count, -1)
-    return [left, low, high, right]
+def both_ways(halves, axis, count):
+    first, second = halves
+    left = [shift(h, axis, count, 1) for h in halves]
+    right = [shift(h, axis, count, -1) for h in (second, first)]
+    low = shift(left[0], axis, count, 1)
+    high = shift(right[0], axis, count, -1)
+    return [left[0], left[1], low, high, right[1], right[0]]
 
 
 def per_device(q1, q2, k1, k2, v, lam, hgain, ow, res, ngain, gw, uw, dw):
@@ -386,7 +391,10 @@
     half_up = shift(up[3][: tok // 2], "z", 8, 1)
     half_down = shift(down_ring[3][tok // 2 :], "z", 8, -1)
 
-    extra = both_ways(jnp.concatenate([ow, res], axis=1), "x", 4)
+    half = tok // 2
+    extra = both_ways(
+        [jnp.concatenate([ow[h : h + half], res[h : h + half]], axis=1) for h in (0, half)], "x", 4
+    )
 
     part = attention(where, queries, others, [kv, up[1], down_ring[1], up[2], down_ring[2]], (0, -1, 1, -2, 2), ())
     mine, other = attention(where, queries, others, [up[3], down_ring[3], half_up, half_down], (-3, 3, 4, 4), part)
@@ -398,21 +406,18 @@
     own, normed = project(where, ngain, att, ow, res, extra)
 
     width = res.shape[1]
-    lo, hi, one, three, here = mixer(where, normed, full, width)
-    half = tok // 2
+    plus, minus, one_lo, three_hi, here = mixer(where, normed, full, width)
 
     def wide(a):
         return a.astype(jnp.float32)
 
-    from_left = shift(lo, "x", 4, 1)
-    from_right = shift(hi, "x", 4, -1)
-    left_hi = shift(one[half:], "x", 4, 1)
-    right_lo = shift(three[:half], "x", 4, -1)
-    left_lo = shift((wide(one[:half]) + wide(from_left)).astype(jnp.bfloat16), "x", 4, 1)
-    right_hi = shift((wide(three[half:]) + wide(from_right)).astype(jnp.bfloat16), "x", 4, -1)
+    plus = shift(plus, "x", 4, 1)
+    minus = shift(minus, "x", 4, -1)
+    left_lo = shift((wide(one_lo) + wide(plus[:half])).astype(jnp.bfloat16), "x", 4, 1)
+    right_hi = shift((wide(three_hi) + wide(minus[:half])).astype(jnp.bfloat16), "x", 4, -1)
     near = wide(own) + wide(here)
-    first = near[:half] + wide(right_lo) + wide(left_lo)
-    second = near[half:] + wide(left_hi) + wide(right_hi)
+    first = near[:half] + wide(minus[half:]) + wide(left_lo)
+    second = near[half:] + wide(plus[half:]) + wide(right_hi)
     return jnp.concatenate([first, second], axis=0).astype(jnp.bfloat16)
 
 

time: 172 us -> 164 us (0.953)
  local copies, waits for them, and re-layouts: 13.7 us -> 2.8 us
  starting transfers between devices: 49.6 us -> 54.7 us
  Pallas kernels: 39.9 us -> 34.9 us
  waiting for transfers between devices: 48.5 us -> 51.6 us
    unnamed x36 -> x15, local copies, waits for them, and re-layouts: 9.18 us -> 1.75 us
    ppermute x29, starting transfers between devices: 49.6 us -> 54.7 us  [shift(): return lax.ppermute(a, axis, [(i, (i + by) % count) for i in range(count)])]
    slice x4 -> x2, local copies, waits for them, and re-layouts: 2.85 us -> 0.1 us  [the longest x1 0.08 us: per_device(): ow[h:h + half]]
    pallas_call x1, Pallas kernels: 3.75 us -> 1.2 us  [merge_cores(): pl.pallas_call(merge_kernel, out_shape=(jax.ShapeDtypeStruct((rows, width...]
    all_gather x1, waiting for transfers between devices: 0.01 us -> 2.24 us  [per_device(): full = lax.all_gather(both, ('z', 'y', 'c'), axis=0, tiled=True)]
    pallas_call x1, Pallas kernels: 2.72 us -> 0.78 us  [finish(): pl.pallas_call(finish_kernel, out_shape=jax.ShapeDtypeStruct((tok, 2 * HE...]
  transfers between devices with their start and end apart: 30 -> 30, of which waited for: 15 -> 18; matrix products, arithmetic and copies ran while one was open for 5% -> 2% of each run, Pallas kernels for 18% -> 16%
where the time goes in v1:
time: 164 us; the launch traced here: 161 us
  starting transfers between devices  54.7 us (33%)
  waiting for transfers between devices  51.6 us (31%)
  Pallas kernels  34.9 us (21%)
  between operations  14.3 us (9%)
  other arithmetic  2.95 us (2%)
  local copies, waits for them, and re-layouts  2.8 us (2%)
    ppermute x29, starting transfers between devices, shift(): return lax.ppermute(a, axis, [(i, (i + by) % count) for i in range(count)])  54.7 us
    ppermute x29, waiting for transfers between devices, shift(): return lax.ppermute(a, axis, [(i, (i + by) % count) for i in range(count)])  49.4 us
    pallas_call x2, Pallas kernels, attention(): pl.pallas_call(functools.partial(attention_kernel, steps, bool(before)),...  20.6 us
    pallas_call x1, Pallas kernels, mixer(): pl.pallas_call(mixer_kernel, out_shape=(whole, whole, part, part, whole),...  9.02 us
  transfers between devices with their start and end apart: 30, of which 18 were waited for; matrix products, arithmetic and copies ran while one was open for 2% of the time, Pallas kernels for 16%

profile of v1, /device:TPU:1, one launch (start us, length us, event | category | flops | bytes accessed | tf_op | source)
XLA Modules:
  0.0 161.2 jit_solution(4317130255580256385)
XLA Ops:
  6.5 1.8 %pad_maximum_fusion.3 = bf16[32,4224]{1,0:T(8,128)(2,1)} fusion(bf16[32,1408]{1,0:T(8,128)(2,1)} %bitcast.17, bf16[32,1408]{1,0:T(8,128)(2,1)} %param.24, bf16[32,1408]{1,0:T(8,128)(2,1)} %param.23), kind=kLoop, calls=%fused_computation.4 | loop fusion | flops 811008 | bytes 540672 | tf_op jit(solution)/shard_map/concatenate | solution.py:375
  11.0 2.5 %collective-permute-start.4 = (bf16[256,512]{1,0:T(8,128)(2,1)S(1)}, bf16[256,512]{1,0:T(8,128)(2,1)S(1)}, u32[]{:S(2)}, u32[]{:S(2)}) collective-permute-start(bf16[256,512]{1,0:T(8,128)(2,1)S(1)} %constant_dynamic-update-slice_fusion.2.rest_0_), channel_id=1, source_target_pairs={{0,32},{32,64},{64,96},{96,128},{128,160},{160,192},{192,224},{224... | collective-permute-start | bytes 786440 | tf_op jit(solution)/shard_map/ppermute | solution.py:25
  13.5 4.0 %collective-permute-start.7 = (bf16[256,512]{1,0:T(8,128)(2,1)S(1)}, bf16[256,512]{1,0:T(8,128)(2,1)S(1)}, u32[]{:S(2)}, u32[]{:S(2)}) collective-permute-start(bf16[256,512]{1,0:T(8,128)(2,1)S(1)} %constant_dynamic-update-slice_fusion.2.rest_0_), channel_id=1, source_target_pairs={{0,224},{32,0},{64,32},{96,64},{128,96},{160,128},{192,160},{224,1... | collective-permute-start | bytes 786440 | tf_op jit(solution)/shard_map/ppermute | solution.py:25
  18.9 2.6 %collective-permute-start.1 = (bf16[256,256]{1,0:T(8,128)(2,1)S(1)}, bf16[256,256]{1,0:T(8,128)(2,1)S(1)}, u32[]{:S(2)}, u32[]{:S(2)}) collective-permute-start(bf16[256,256]{1,0:T(8,128)(2,1)S(1)} %constant_dynamic-update-slice_fusion), channel_id=1, source_target_pairs={{0,16},{8,24},{16,0},{24,8},{1,17},{9,25},{17,1},{25,9},{2,18},{10... | collective-permute-start | bytes 393224 | tf_op jit(solution)/shard_map/ppermute | solution.py:25
  23.4 2.7 %collective-permute-start.8 = (bf16[256,512]{1,0:T(8,128)(2,1)S(1)}, bf16[256,512]{1,0:T(8,128)(2,1)S(1)}, u32[]{:S(2)}, u32[]{:S(2)}) collective-permute-start(bf16[256,512]{1,0:T(8,128)(2,1)S(1)} %collective-permute-done.7.rest_2_), channel_id=1, source_target_pairs={{0,224},{32,0},{64,32},{96,64},{128,96},{160,128},{192,160},{224,1... | collective-permute-start | bytes 786440 | tf_op jit(solution)/shard_map/ppermute | solution.py:25
  27.1 1.9 %collective-permute-start.3 = (bf16[4,256,256]{2,1,0:T(8,128)(2,1)S(1)}, bf16[4,256,256]{2,1,0:T(8,128)(2,1)S(1)}, u32[]{:S(2)}, u32[]{:S(2)}) collective-permute-start(bf16[4,256,256]{2,1,0:T(8,128)(2,1)S(1)} %pad_maximum_fusion.2.q_ref), channel_id=1, source_target_pairs={{0,4},{4,0},{1,5},{5,1},{2,6},{6,2},{3,7},{7,3},{8,12},{12,8},{9,1... | collective-permute-start | bytes 1572872 | tf_op jit(solution)/shard_map/ppermute | solution.py:25
  29.0 2.4 %collective-permute-done.5.rest_3_ = bf16[256,512]{1,0:T(8,128)(2,1)S(1)} collective-permute-done((bf16[256,512]{1,0:T(8,128)(2,1)S(1)}, bf16[256,512]{1,0:T(8,128)(2,1)S(1)}, u32[]{:S(2)}, u32[]{:S(2)}) %collective-permute-start.5) | collective-permute-done | bytes 262176 | tf_op jit(solution)/shard_map/ppermute | solution.py:25
  32.5 3.4 %collective-permute-start.9 = (bf16[256,512]{1,0:T(8,128)(2,1)S(1)}, bf16[256,512]{1,0:T(8,128)(2,1)S(1)}, u32[]{:S(2)}, u32[]{:S(2)}) collective-permute-start(bf16[256,512]{1,0:T(8,128)(2,1)S(1)} %collective-permute-done.8.rest_4_), channel_id=1, source_target_pairs={{0,224},{32,0},{64,32},{96,64},{128,96},{160,128},{192,160},{224,1... | collective-permute-start | bytes 786440 | tf_op jit(solution)/shard_map/ppermute | solution.py:25
  36.0 5.7 %collective-permute-done.6.rest_0_ = bf16[256,512]{1,0:T(8,128)(2,1)S(1)} collective-permute-done((bf16[256,512]{1,0:T(8,128)(2,1)S(1)}, bf16[256,512]{1,0:T(8,128)(2,1)S(1)}, u32[]{:S(2)}, u32[]{:S(2)}) %collective-permute-start.6) | collective-permute-done | bytes 262176 | tf_op jit(solution)/shard_map/ppermute | solution.py:25
  42.2 3.6 %collective-permute-start.11 = (bf16[128,512]{1,0:T(8,128)(2,1)S(1)}, bf16[128,512]{1,0:T(8,128)(2,1)S(1)}, u32[]{:S(2)}, u32[]{:S(2)}) collective-permute-start(bf16[128,512]{1,0:T(8,128)(2,1)S(1)} %slice.49), channel_id=1, source_target_pairs={{0,224},{32,0},{64,32},{96,64},{128,96},{160,128},{192,160},{224,1... | collective-permute-start | bytes 393224 | tf_op jit(solution)/shard_map/ppermute | solution.py:25
  45.9 12.0 %shard_map.127 = (bf16[4,272,512]{2,1,0:T(8,128)(2,1)S(1)}, bf16[4,272,512]{2,1,0:T(8,128)(2,1)S(1)}) custom-call(s32[4]{0:T(128)S(1)} %pad_add_fusion.where_ref, bf16[4,256,256]{2,1,0:T(8,128)(2,1)S(1)} %pad_maximum_fusion.2.q_ref, bf16[4,256,256]{2,1,0:T(8,128)(2,1)S(1)} %collective-permute-done.3.other_q_ref, ...), custom_call_target="tpu_custom_call" | custom-call | flops 4026531840 | bytes 4194304 | tf_op jit(solution)/shard_map/pallas_call | solution.py:147
  58.0 8.6 %shard_map.128 = (bf16[4,272,512]{2,1,0:T(8,128)(2,1)S(1)}, bf16[4,272,512]{2,1,0:T(8,128)(2,1)S(1)}) custom-call(s32[4]{0:T(128)S(1)} %pad_add_fusion.where_ref, bf16[4,256,256]{2,1,0:T(8,128)(2,1)S(1)} %pad_maximum_fusion.2.q_ref, bf16[4,256,256]{2,1,0:T(8,128)(2,1)S(1)} %collective-permute-done.3.other_q_ref, ...), custom_call_target="tpu_custom_call" | custom-call | flops 2415919104 | bytes 4194304 | tf_op jit(solution)/shard_map/pallas_call | solution.py:147
  66.6 4.2 %collective-permute-start.12 = (bf16[4,272,512]{2,1,0:T(8,128)(2,1)S(1)}, bf16[4,272,512]{2,1,0:T(8,128)(2,1)S(1)}, u32[]{:S(2)}, u32[]{:S(2)}) collective-permute-start(bf16[4,272,512]{2,1,0:T(8,128)(2,1)S(1)} %get-tuple-element.23), channel_id=1, source_target_pairs={{0,4},{4,0},{1,5},{5,1},{2,6},{6,2},{3,7},{7,3},{8,12},{12,8},{9,1... | collective-permute-start | bytes 3342344 | tf_op jit(solution)/shard_map/ppermute | solution.py:25
  72.3 1.5 collective-permute-start.22
  75.1 3.6 %collective-permute-start.13 = (bf16[272,512]{1,0:T(8,128)(2,1)S(1)}, bf16[272,512]{1,0:T(8,128)(2,1)S(1)}, u32[]{:S(2)}, u32[]{:S(2)}) collective-permute-start(bf16[272,512]{1,0:T(8,128)(2,1)S(1)} %get-tuple-element.25), channel_id=1, source_target_pairs={{0,24},{8,0},{16,8},{24,16},{1,25},{9,1},{17,9},{25,17},{2,26},{10... | collective-permute-start | bytes 835592 | tf_op jit(solution)/shard_map/ppermute | solution.py:25
  80.6 7.2 %collective-permute-done.19.refs_6_ = bf16[128,2560]{1,0:T(8,128)(2,1)S(1)} collective-permute-done((bf16[128,2560]{1,0:T(8,128)(2,1)S(1)}, bf16[128,2560]{1,0:T(8,128)(2,1)S(1)}, u32[]{:S(2)}, u32[]{:S(2)}) %collective-permute-start.19) | collective-permute-done | bytes 655392 | tf_op jit(solution)/shard_map/ppermute | solution.py:25
  89.1 2.3 %collective-permute-start.15 = (bf16[272,512]{1,0:T(8,128)(2,1)S(1)}, bf16[272,512]{1,0:T(8,128)(2,1)S(1)}, u32[]{:S(2)}, u32[]{:S(2)}) collective-permute-start(bf16[272,512]{1,0:T(8,128)(2,1)S(1)} %get-tuple-element.27), channel_id=1, source_target_pairs={{0,8},{8,16},{16,24},{24,0},{1,9},{9,17},{17,25},{25,1},{2,10},{10... | collective-permute-start | bytes 835592 | tf_op jit(solution)/shard_map/ppermute | solution.py:25
  91.4 1.6 collective-permute-start.21
  94.4 3.2 %collective-permute-start.23 = (bf16[128,2560]{1,0:T(8,128)(2,1)S(1)}, bf16[128,2560]{1,0:T(8,128)(2,1)S(1)}, u32[]{:S(2)}, u32[]{:S(2)}) collective-permute-start(bf16[128,2560]{1,0:T(8,128)(2,1)S(1)} %collective-permute-done.22.refs_11_), channel_id=1, source_target_pairs={{0,3},{1,0},{2,1},{3,2},{4,7},{5,4},{6,5},{7,6},{8,11},{9,8},{10,9... | collective-permute-start | bytes 1966088 | tf_op jit(solution)/shard_map/ppermute | solution.py:25
  98.3 7.9 %collective-permute-done.15.refs_3_ = bf16[272,512]{1,0:T(8,128)(2,1)S(1)} collective-permute-done((bf16[272,512]{1,0:T(8,128)(2,1)S(1)}, bf16[272,512]{1,0:T(8,128)(2,1)S(1)}, u32[]{:S(2)}, u32[]{:S(2)}) %collective-permute-start.15) | collective-permute-done | bytes 278560 | tf_op jit(solution)/shard_map/ppermute | solution.py:25
  108.1 2.6 %collective-permute-start.17 = (bf16[256,256]{1,0:T(8,128)(2,1)S(1)}, bf16[256,256]{1,0:T(8,128)(2,1)S(1)}, u32[]{:S(2)}, u32[]{:S(2)}) collective-permute-start(bf16[256,256]{1,0:T(8,128)(2,1)S(1)} %finish_heads.1.refs_0_), channel_id=1, source_target_pairs={{0,2},{1,3},{2,0},{3,1},{4,6},{5,7},{6,4},{7,5},{8,10},{9,11},{10,... | collective-permute-start | bytes 393224 | tf_op jit(solution)/shard_map/ppermute | solution.py:25
  111.5 4.5 %collective-permute-done.21.refs_8_ = bf16[128,2560]{1,0:T(8,128)(2,1)S(1)} collective-permute-done((bf16[128,2560]{1,0:T(8,128)(2,1)S(1)}, bf16[128,2560]{1,0:T(8,128)(2,1)S(1)}, u32[]{:S(2)}, u32[]{:S(2)}) %collective-permute-start.21) | collective-permute-done | bytes 655392 | tf_op jit(solution)/shard_map/ppermute | solution.py:25
  116.0 2.8 %collective-permute-done.16.refs_1_ = bf16[256,256]{1,0:T(8,128)(2,1)S(1)} collective-permute-done((bf16[256,256]{1,0:T(8,128)(2,1)S(1)}, bf16[256,256]{1,0:T(8,128)(2,1)S(1)}, u32[]{:S(2)}, u32[]{:S(2)}) %collective-permute-start.16) | collective-permute-done | bytes 131104 | tf_op jit(solution)/shard_map/ppermute | solution.py:25
  118.8 3.6 %collective-permute-done.17.refs_2_ = bf16[256,256]{1,0:T(8,128)(2,1)S(1)} collective-permute-done((bf16[256,256]{1,0:T(8,128)(2,1)S(1)}, bf16[256,256]{1,0:T(8,128)(2,1)S(1)}, u32[]{:S(2)}, u32[]{:S(2)}) %collective-permute-start.17) | collective-permute-done | bytes 131104 | tf_op jit(solution)/shard_map/ppermute | solution.py:25
  122.4 3.2 %project_norm.1 = (bf16[256,512]{1,0:T(8,128)(2,1)S(1)}, bf16[256,2048]{1,0:T(8,128)(2,1)S(1)}) custom-call(s32[4]{0:T(128)S(1)} %pad_add_fusion.where_ref, f32[1,2048]{1,0:T(1,128)S(1)} %bitcast.11, bf16[256,256]{1,0:T(8,128)(2,1)S(1)} %finish_heads.1.refs_0_, bf16[256,256]{1,0:T(8,128)(2,1)S(1)} %collective-permute-done.16.refs_1_, ...), custom_call_target="tpu_custom_call" | custom-call | flops 2000000000 | bytes 8000000 | tf_op jit(solution)/shard_map/project_norm/pallas_call | solution.py:266
  125.7 2.2 %all-gather.2.cloned.1.call-done.full_ref = bf16[2048,4224]{1,0:T(8,128)(2,1)} async-done(((bf16[32,4224]{1,0:T(8,128)(2,1)}), bf16[2048,4224]{1,0:T(8,128)(2,1)}) %all-gather.2.cloned.1.call-update) | async-done | bytes 17301520 | tf_op jit(solution)/shard_map/all_gather | solution.py:376
  127.9 9.0 %mixer.1 = (bf16[256,512]{1,0:T(8,128)(2,1)S(1)}, bf16[256,512]{1,0:T(8,128)(2,1)S(1)}, bf16[128,512]{1,0:T(8,128)(2,1)S(1)}, bf16[128,512]{1,0:T(8,128)(2,1)S(1)}, bf16[256,512]{1,0:T(8,128)(2,1)S(1)}) custom-call(s32[4]{0:T(128)S(1)} %pad_add_fusion.where_ref, bf16[256,2048]{1,0:T(8,128)(2,1)S(1)} %get-tuple-element.29.normed_ref, ...), custom_call_target="tpu_custom_call" | custom-call | flops 4429185024 | bytes 18000000 | tf_op jit(solution)/shard_map/mixer/pallas_call | solution.py:343
  137.0 2.5 %collective-permute-start.25 = (bf16[256,512]{1,0:T(8,128)(2,1)S(1)}, bf16[256,512]{1,0:T(8,128)(2,1)S(1)}, u32[]{:S(2)}, u32[]{:S(2)}) collective-permute-start(bf16[256,512]{1,0:T(8,128)(2,1)S(1)} %get-tuple-element.31), channel_id=1, source_target_pairs={{0,3},{1,0},{2,1},{3,2},{4,7},{5,4},{6,5},{7,6},{8,11},{9,8},{10,9... | collective-permute-start | bytes 786440 | tf_op jit(solution)/shard_map/ppermute | solution.py:25
  139.4 5.4 %collective-permute-done.25 = bf16[256,512]{1,0:T(8,128)(2,1)S(1)} collective-permute-done((bf16[256,512]{1,0:T(8,128)(2,1)S(1)}, bf16[256,512]{1,0:T(8,128)(2,1)S(1)}, u32[]{:S(2)}, u32[]{:S(2)}) %collective-permute-start.25) | collective-permute-done | bytes 262176 | tf_op jit(solution)/shard_map/ppermute | solution.py:25
  144.9 3.5 %collective-permute-start.28 = (bf16[128,512]{1,0:T(8,128)(2,1)S(1)}, bf16[128,512]{1,0:T(8,128)(2,1)S(1)}, u32[]{:S(2)}, u32[]{:S(2)}) collective-permute-start(bf16[128,512]{1,0:T(8,128)(2,1)S(1)} %add_convert_fusion), channel_id=1, source_target_pairs={{0,3},{1,0},{2,1},{3,2},{4,7},{5,4},{6,5},{7,6},{8,11},{9,8},{10,9... | collective-permute-start | bytes 393224 | tf_op jit(solution)/shard_map/ppermute | solution.py:25
  148.6 1.7 %collective-permute-done.28 = bf16[128,512]{1,0:T(8,128)(2,1)S(1)} collective-permute-done((bf16[128,512]{1,0:T(8,128)(2,1)S(1)}, bf16[128,512]{1,0:T(8,128)(2,1)S(1)}, u32[]{:S(2)}, u32[]{:S(2)}) %collective-permute-start.28) | collective-permute-done | bytes 131104 | tf_op jit(solution)/shard_map/ppermute | solution.py:25
  150.3 3.2 %collective-permute-done.27 = bf16[128,512]{1,0:T(8,128)(2,1)S(1)} collective-permute-done((bf16[128,512]{1,0:T(8,128)(2,1)S(1)}, bf16[128,512]{1,0:T(8,128)(2,1)S(1)}, u32[]{:S(2)}, u32[]{:S(2)}) %collective-permute-start.27) | collective-permute-done | bytes 131104 | tf_op jit(solution)/shard_map/ppermute | solution.py:25
  (66 shorter events, 19.8 us)
Async XLA Ops:
  6.5 121.4 %all-gather.2.cloned.1.call-start = ((), (), s32[]{:S(2)}) async-start(), calls=%async_computation | async-start | bytes 17571840 | tf_op jit(solution)/shard_map/all_gather | solution.py:376
  11.0 12.5 %collective-permute-start.4 = (bf16[256,512]{1,0:T(8,128)(2,1)S(1)}, bf16[256,512]{1,0:T(8,128)(2,1)S(1)}, u32[]{:S(2)}, u32[]{:S(2)}) collective-permute-start(bf16[256,512]{1,0:T(8,128)(2,1)S(1)} %constant_dynamic-update-slice_fusion.2.rest_0_), channel_id=1, source_target_pairs={{0,32},{32,64},{64,96},{96,128},{128,160},{160,192},{192,224},{224... | collective-permute-start | bytes 786440 | tf_op jit(solution)/shard_map/ppermute | solution.py:25
  13.5 10.0 %collective-permute-start.7 = (bf16[256,512]{1,0:T(8,128)(2,1)S(1)}, bf16[256,512]{1,0:T(8,128)(2,1)S(1)}, u32[]{:S(2)}, u32[]{:S(2)}) collective-permute-start(bf16[256,512]{1,0:T(8,128)(2,1)S(1)} %constant_dynamic-update-slice_fusion.2.rest_0_), channel_id=1, source_target_pairs={{0,224},{32,0},{64,32},{96,64},{128,96},{160,128},{192,160},{224,1... | collective-permute-start | bytes 786440 | tf_op jit(solution)/shard_map/ppermute | solution.py:25
  17.6 8.6 %collective-permute-start = (bf16[256,256]{1,0:T(8,128)(2,1)S(1)}, bf16[256,256]{1,0:T(8,128)(2,1)S(1)}, u32[]{:S(2)}, u32[]{:S(2)}) collective-permute-start(bf16[256,256]{1,0:T(8,128)(2,1)S(1)} %constant_dynamic-update-slice_fusion), channel_id=1, source_target_pairs={{0,8},{8,16},{16,24},{24,0},{1,9},{9,17},{17,25},{25,1},{2,10},{10... | collective-permute-start | bytes 393224 | tf_op jit(solution)/shard_map/ppermute | solution.py:25
  18.9 7.8 %collective-permute-start.1 = (bf16[256,256]{1,0:T(8,128)(2,1)S(1)}, bf16[256,256]{1,0:T(8,128)(2,1)S(1)}, u32[]{:S(2)}, u32[]{:S(2)}) collective-permute-start(bf16[256,256]{1,0:T(8,128)(2,1)S(1)} %constant_dynamic-update-slice_fusion), channel_id=1, source_target_pairs={{0,16},{8,24},{16,0},{24,8},{1,17},{9,25},{17,1},{25,9},{2,18},{10... | collective-permute-start | bytes 393224 | tf_op jit(solution)/shard_map/ppermute | solution.py:25
  21.6 5.5 %collective-permute-start.2 = (bf16[256,256]{1,0:T(8,128)(2,1)S(1)}, bf16[256,256]{1,0:T(8,128)(2,1)S(1)}, u32[]{:S(2)}, u32[]{:S(2)}) collective-permute-start(bf16[256,256]{1,0:T(8,128)(2,1)S(1)} %constant_dynamic-update-slice_fusion), channel_id=1, source_target_pairs={{0,24},{8,0},{16,8},{24,16},{1,25},{9,1},{17,9},{25,17},{2,26},{10... | collective-permute-start | bytes 393224 | tf_op jit(solution)/shard_map/ppermute | solution.py:25
  23.4 7.9 %collective-permute-start.5 = (bf16[256,512]{1,0:T(8,128)(2,1)S(1)}, bf16[256,512]{1,0:T(8,128)(2,1)S(1)}, u32[]{:S(2)}, u32[]{:S(2)}) collective-permute-start(bf16[256,512]{1,0:T(8,128)(2,1)S(1)} %collective-permute-done.4.rest_1_), channel_id=1, source_target_pairs={{0,32},{32,64},{64,96},{96,128},{128,160},{160,192},{192,224},{224... | collective-permute-start | bytes 786440 | tf_op jit(solution)/shard_map/ppermute | solution.py:25
  23.4 9.0 %collective-permute-start.8 = (bf16[256,512]{1,0:T(8,128)(2,1)S(1)}, bf16[256,512]{1,0:T(8,128)(2,1)S(1)}, u32[]{:S(2)}, u32[]{:S(2)}) collective-permute-start(bf16[256,512]{1,0:T(8,128)(2,1)S(1)} %collective-permute-done.7.rest_2_), channel_id=1, source_target_pairs={{0,224},{32,0},{64,32},{96,64},{128,96},{160,128},{192,160},{224,1... | collective-permute-start | bytes 786440 | tf_op jit(solution)/shard_map/ppermute | solution.py:25
  27.1 18.8 %collective-permute-start.3 = (bf16[4,256,256]{2,1,0:T(8,128)(2,1)S(1)}, bf16[4,256,256]{2,1,0:T(8,128)(2,1)S(1)}, u32[]{:S(2)}, u32[]{:S(2)}) collective-permute-start(bf16[4,256,256]{2,1,0:T(8,128)(2,1)S(1)} %pad_maximum_fusion.2.q_ref), channel_id=1, source_target_pairs={{0,4},{4,0},{1,5},{5,1},{2,6},{6,2},{3,7},{7,3},{8,12},{12,8},{9,1... | collective-permute-start | bytes 1572872 | tf_op jit(solution)/shard_map/ppermute | solution.py:25
  31.4 10.3 %collective-permute-start.6 = (bf16[256,512]{1,0:T(8,128)(2,1)S(1)}, bf16[256,512]{1,0:T(8,128)(2,1)S(1)}, u32[]{:S(2)}, u32[]{:S(2)}) collective-permute-start(bf16[256,512]{1,0:T(8,128)(2,1)S(1)} %collective-permute-done.5.rest_3_), channel_id=1, source_target_pairs={{0,32},{32,64},{64,96},{96,128},{128,160},{160,192},{192,224},{224... | collective-permute-start | bytes 786440 | tf_op jit(solution)/shard_map/ppermute | solution.py:25
  32.5 9.8 %collective-permute-start.9 = (bf16[256,512]{1,0:T(8,128)(2,1)S(1)}, bf16[256,512]{1,0:T(8,128)(2,1)S(1)}, u32[]{:S(2)}, u32[]{:S(2)}) collective-permute-start(bf16[256,512]{1,0:T(8,128)(2,1)S(1)} %collective-permute-done.8.rest_4_), channel_id=1, source_target_pairs={{0,224},{32,0},{64,32},{96,64},{128,96},{160,128},{192,160},{224,1... | collective-permute-start | bytes 786440 | tf_op jit(solution)/shard_map/ppermute | solution.py:25
  41.6 16.3 %collective-permute-start.10 = (bf16[128,512]{1,0:T(8,128)(2,1)S(1)}, bf16[128,512]{1,0:T(8,128)(2,1)S(1)}, u32[]{:S(2)}, u32[]{:S(2)}) collective-permute-start(bf16[128,512]{1,0:T(8,128)(2,1)S(1)} %slice.48), channel_id=1, source_target_pairs={{0,32},{32,64},{64,96},{96,128},{128,160},{160,192},{192,224},{224... | collective-permute-start | bytes 393224 | tf_op jit(solution)/shard_map/ppermute | solution.py:25
  42.2 15.7 %collective-permute-start.11 = (bf16[128,512]{1,0:T(8,128)(2,1)S(1)}, bf16[128,512]{1,0:T(8,128)(2,1)S(1)}, u32[]{:S(2)}, u32[]{:S(2)}) collective-permute-start(bf16[128,512]{1,0:T(8,128)(2,1)S(1)} %slice.49), channel_id=1, source_target_pairs={{0,224},{32,0},{64,32},{96,64},{128,96},{160,128},{192,160},{224,1... | collective-permute-start | bytes 393224 | tf_op jit(solution)/shard_map/ppermute | solution.py:25
  66.6 7.4 %collective-permute-start.12 = (bf16[4,272,512]{2,1,0:T(8,128)(2,1)S(1)}, bf16[4,272,512]{2,1,0:T(8,128)(2,1)S(1)}, u32[]{:S(2)}, u32[]{:S(2)}) collective-permute-start(bf16[4,272,512]{2,1,0:T(8,128)(2,1)S(1)} %get-tuple-element.23), channel_id=1, source_target_pairs={{0,4},{4,0},{1,5},{5,1},{2,6},{6,2},{3,7},{7,3},{8,12},{12,8},{9,1... | collective-permute-start | bytes 3342344 | tf_op jit(solution)/shard_map/ppermute | solution.py:25
  71.0 16.9 %collective-permute-start.19 = (bf16[128,2560]{1,0:T(8,128)(2,1)S(1)}, bf16[128,2560]{1,0:T(8,128)(2,1)S(1)}, u32[]{:S(2)}, u32[]{:S(2)}) collective-permute-start(bf16[128,2560]{1,0:T(8,128)(2,1)S(1)} %pad_maximum_fusion), channel_id=1, source_target_pairs={{0,1},{1,2},{2,3},{3,0},{4,5},{5,6},{6,7},{7,4},{8,9},{9,10},{10,1... | collective-permute-start | bytes 1966088 | tf_op jit(solution)/shard_map/ppermute | solution.py:25
  72.3 16.8 %collective-permute-start.22 = (bf16[128,2560]{1,0:T(8,128)(2,1)S(1)}, bf16[128,2560]{1,0:T(8,128)(2,1)S(1)}, u32[]{:S(2)}, u32[]{:S(2)}) collective-permute-start(bf16[128,2560]{1,0:T(8,128)(2,1)S(1)} %pad_maximum_fusion.1), channel_id=1, source_target_pairs={{0,3},{1,0},{2,1},{3,2},{4,7},{5,4},{6,5},{7,6},{8,11},{9,8},{10,9... | collective-permute-start | bytes 1966088 | tf_op jit(solution)/shard_map/ppermute | solution.py:25
  73.9 32.3 %copy-start.3 = (f32[256]{0:T(256)S(1)}, f32[256]{0:T(256)}, u32[]{:S(2)}) copy-start(f32[256]{0:T(256)} %param.19) | copy-start | bytes 3076
  75.1 16.3 %collective-permute-start.13 = (bf16[272,512]{1,0:T(8,128)(2,1)S(1)}, bf16[272,512]{1,0:T(8,128)(2,1)S(1)}, u32[]{:S(2)}, u32[]{:S(2)}) collective-permute-start(bf16[272,512]{1,0:T(8,128)(2,1)S(1)} %get-tuple-element.25), channel_id=1, source_target_pairs={{0,24},{8,0},{16,8},{24,16},{1,25},{9,1},{17,9},{25,17},{2,26},{10... | collective-permute-start | bytes 835592 | tf_op jit(solution)/shard_map/ppermute | solution.py:25
  78.7 15.7 %collective-permute-start.14 = (bf16[272,512]{1,0:T(8,128)(2,1)S(1)}, bf16[272,512]{1,0:T(8,128)(2,1)S(1)}, u32[]{:S(2)}, u32[]{:S(2)}) collective-permute-start(bf16[272,512]{1,0:T(8,128)(2,1)S(1)} %get-tuple-element.26), channel_id=1, source_target_pairs={{0,16},{8,24},{16,0},{24,8},{1,17},{9,25},{17,1},{25,9},{2,18},{10... | collective-permute-start | bytes 835592 | tf_op jit(solution)/shard_map/ppermute | solution.py:25
  79.5 28.6 %collective-permute-start.20 = (bf16[128,2560]{1,0:T(8,128)(2,1)S(1)}, bf16[128,2560]{1,0:T(8,128)(2,1)S(1)}, u32[]{:S(2)}, u32[]{:S(2)}) collective-permute-start(bf16[128,2560]{1,0:T(8,128)(2,1)S(1)} %pad_maximum_fusion.1), channel_id=1, source_target_pairs={{0,1},{1,2},{2,3},{3,0},{4,5},{5,6},{6,7},{7,4},{8,9},{9,10},{10,1... | collective-permute-start | bytes 1966088 | tf_op jit(solution)/shard_map/ppermute | solution.py:25
  87.9 22.8 %collective-permute-start.24 = (bf16[128,2560]{1,0:T(8,128)(2,1)S(1)}, bf16[128,2560]{1,0:T(8,128)(2,1)S(1)}, u32[]{:S(2)}, u32[]{:S(2)}) collective-permute-start(bf16[128,2560]{1,0:T(8,128)(2,1)S(1)} %pad_maximum_fusion), channel_id=1, source_target_pairs={{0,3},{1,0},{2,1},{3,2},{4,7},{5,4},{6,5},{7,6},{8,11},{9,8},{10,9... | collective-permute-start | bytes 1966088 | tf_op jit(solution)/shard_map/ppermute | solution.py:25
  89.1 17.1 %collective-permute-start.15 = (bf16[272,512]{1,0:T(8,128)(2,1)S(1)}, bf16[272,512]{1,0:T(8,128)(2,1)S(1)}, u32[]{:S(2)}, u32[]{:S(2)}) collective-permute-start(bf16[272,512]{1,0:T(8,128)(2,1)S(1)} %get-tuple-element.27), channel_id=1, source_target_pairs={{0,8},{8,16},{16,24},{24,0},{1,9},{9,17},{17,25},{25,1},{2,10},{10... | collective-permute-start | bytes 835592 | tf_op jit(solution)/shard_map/ppermute | solution.py:25
  91.4 24.5 %collective-permute-start.21 = (bf16[128,2560]{1,0:T(8,128)(2,1)S(1)}, bf16[128,2560]{1,0:T(8,128)(2,1)S(1)}, u32[]{:S(2)}, u32[]{:S(2)}) collective-permute-start(bf16[128,2560]{1,0:T(8,128)(2,1)S(1)} %collective-permute-done.19.refs_6_), channel_id=1, source_target_pairs={{0,1},{1,2},{2,3},{3,0},{4,5},{5,6},{6,7},{7,4},{8,9},{9,10},{10,1... | collective-permute-start | bytes 1966088 | tf_op jit(solution)/shard_map/ppermute | solution.py:25
  94.4 21.6 %collective-permute-start.23 = (bf16[128,2560]{1,0:T(8,128)(2,1)S(1)}, bf16[128,2560]{1,0:T(8,128)(2,1)S(1)}, u32[]{:S(2)}, u32[]{:S(2)}) collective-permute-start(bf16[128,2560]{1,0:T(8,128)(2,1)S(1)} %collective-permute-done.22.refs_11_), channel_id=1, source_target_pairs={{0,3},{1,0},{2,1},{3,2},{4,7},{5,4},{6,5},{7,6},{8,11},{9,8},{10,9... | collective-permute-start | bytes 1966088 | tf_op jit(solution)/shard_map/ppermute | solution.py:25
  106.2 16.2 %copy-start.2 = (f32[2048]{0:T(1024)S(1)}, f32[2048]{0:T(1024)}, u32[]{:S(2)}) copy-start(f32[2048]{0:T(1024)} %param.22) | copy-start | bytes 24580
  107.0 11.8 %collective-permute-start.16 = (bf16[256,256]{1,0:T(8,128)(2,1)S(1)}, bf16[256,256]{1,0:T(8,128)(2,1)S(1)}, u32[]{:S(2)}, u32[]{:S(2)}) collective-permute-start(bf16[256,256]{1,0:T(8,128)(2,1)S(1)} %finish_heads.1.refs_0_), channel_id=1, source_target_pairs={{0,1},{1,2},{2,3},{3,0},{4,5},{5,6},{6,7},{7,4},{8,9},{9,10},{10,1... | collective-permute-start | bytes 393224 | tf_op jit(solution)/shard_map/ppermute | solution.py:25
  108.1 14.4 %collective-permute-start.17 = (bf16[256,256]{1,0:T(8,128)(2,1)S(1)}, bf16[256,256]{1,0:T(8,128)(2,1)S(1)}, u32[]{:S(2)}, u32[]{:S(2)}) collective-permute-start(bf16[256,256]{1,0:T(8,128)(2,1)S(1)} %finish_heads.1.refs_0_), channel_id=1, source_target_pairs={{0,2},{1,3},{2,0},{3,1},{4,6},{5,7},{6,4},{7,5},{8,10},{9,11},{10,... | collective-permute-start | bytes 393224 | tf_op jit(solution)/shard_map/ppermute | solution.py:25
  110.7 11.8 %collective-permute-start.18 = (bf16[256,256]{1,0:T(8,128)(2,1)S(1)}, bf16[256,256]{1,0:T(8,128)(2,1)S(1)}, u32[]{:S(2)}, u32[]{:S(2)}) collective-permute-start(bf16[256,256]{1,0:T(8,128)(2,1)S(1)} %finish_heads.1.refs_0_), channel_id=1, source_target_pairs={{0,3},{1,0},{2,1},{3,2},{4,7},{5,4},{6,5},{7,6},{8,11},{9,8},{10,9... | collective-permute-start | bytes 393224 | tf_op jit(solution)/shard_map/ppermute | solution.py:25
  137.0 7.9 %collective-permute-start.25 = (bf16[256,512]{1,0:T(8,128)(2,1)S(1)}, bf16[256,512]{1,0:T(8,128)(2,1)S(1)}, u32[]{:S(2)}, u32[]{:S(2)}) collective-permute-start(bf16[256,512]{1,0:T(8,128)(2,1)S(1)} %get-tuple-element.31), channel_id=1, source_target_pairs={{0,3},{1,0},{2,1},{3,2},{4,7},{5,4},{6,5},{7,6},{8,11},{9,8},{10,9... | collective-permute-start | bytes 786440 | tf_op jit(solution)/shard_map/ppermute | solution.py:25
  139.4 8.9 %collective-permute-start.26 = (bf16[256,512]{1,0:T(8,128)(2,1)S(1)}, bf16[256,512]{1,0:T(8,128)(2,1)S(1)}, u32[]{:S(2)}, u32[]{:S(2)}) collective-permute-start(bf16[256,512]{1,0:T(8,128)(2,1)S(1)} %get-tuple-element.33), channel_id=1, source_target_pairs={{0,1},{1,2},{2,3},{3,0},{4,5},{5,6},{6,7},{7,4},{8,9},{9,10},{10,1... | collective-permute-start | bytes 786440 | tf_op jit(solution)/shard_map/ppermute | solution.py:25
  144.9 5.4 %collective-permute-start.28 = (bf16[128,512]{1,0:T(8,128)(2,1)S(1)}, bf16[128,512]{1,0:T(8,128)(2,1)S(1)}, u32[]{:S(2)}, u32[]{:S(2)}) collective-permute-start(bf16[128,512]{1,0:T(8,128)(2,1)S(1)} %add_convert_fusion), channel_id=1, source_target_pairs={{0,3},{1,0},{2,1},{3,2},{4,7},{5,4},{6,5},{7,6},{8,11},{9,8},{10,9... | collective-permute-start | bytes 393224 | tf_op jit(solution)/shard_map/ppermute | solution.py:25
  148.4 5.1 %collective-permute-start.27 = (bf16[128,512]{1,0:T(8,128)(2,1)S(1)}, bf16[128,512]{1,0:T(8,128)(2,1)S(1)}, u32[]{:S(2)}, u32[]{:S(2)}) collective-permute-start(bf16[128,512]{1,0:T(8,128)(2,1)S(1)} %add_convert_fusion.1), channel_id=1, source_target_pairs={{0,1},{1,2},{2,3},{3,0},{4,5},{5,6},{6,7},{7,4},{8,9},{9,10},{10,1... | collective-permute-start | bytes 393224 | tf_op jit(solution)/shard_map/ppermute | solution.py:25
  (4 other events, 39.1 us)
Sparse Core Ops, SparseCore 0:
  10.1 117.8 all-gather.1

commit v2 on v1

--- a/solution.py
+++ b/solution.py
@@ -15,6 +15,7 @@
 FLOOR = -1e20
 SCALE2 = HEAD**-0.5 * math.log2(math.e)
 STAT = 16
+AHEAD = 4
 
 
 VMEM = pl.BlockSpec(memory_space=pltpu.VMEM)
@@ -278,13 +279,11 @@
     )(where, gain.reshape(1, -1), *att, ow, res, *extra)
 
 
-def mixer_kernel(
-    where_ref, normed_ref, full_ref, plus_ref, minus_ref, one_ref, three_ref, here_ref, w_ref, d_ref, h_ref, sems
-):
+def mixer_kernel(where_ref, normed_ref, full_ref, lo_ref, hi_ref, one_ref, three_ref, here_ref, w_ref, d_ref, h_ref, sems):
     count, _, width = w_ref.shape
     _, block, units = d_ref.shape
     lane = width // 2
-    half = one_ref.shape[0]
+    half = lo_ref.shape[0]
 
     def copies(j):
         at = pl.multiple_of(j * lane, lane)
@@ -297,40 +296,42 @@
             for n in range(2)
         ]
 
-    def down_copy(n, s):
-        row = pl.multiple_of(lax.rem(where_ref[3] + s, 4) * block, block)
+    def down_copy(n):
+        row = pl.multiple_of(lax.rem(where_ref[3] + n, 4) * block, block)
         return pltpu.make_async_copy(
             full_ref.at[pl.ds(row, block), pl.ds(2 * units, units)], d_ref.at[n], sems.at[0, count + n]
         )
 
-    @pl.loop(0, count)
-    def _(j):
+    for j in range(AHEAD):
         for c in copies(j):
             c.start()
-
-    ahead = (2, 1, 3, 0)
-    for n, s in enumerate(ahead):
-        down_copy(n, s).start()
 
     @pl.loop(0, count)
     def _(j):
         for c in copies(j):
             c.wait()
+
+        @pl.when(j + AHEAD < count)
+        def _():
+            for c in copies(j + AHEAD):
+                c.start()
+
+        @pl.when(j + AHEAD >= count)
+        def _():
+            down_copy(j + AHEAD - count).start()
+
         both = dot_nn(normed_ref[...], w_ref[j])
         gate, up = both[:, :lane], both[:, lane:]
         cols = pl.ds(pl.multiple_of(j * lane, lane), lane)
         h_ref[:, cols] = (gate / (1.0 + jnp.exp(-gate)) * up).astype(jnp.bfloat16)
 
-    for n, s in enumerate(ahead):
-        down_copy(n, s).wait()
-    two, one, three, here = (dot_nt(h_ref[...], d_ref[n]).astype(jnp.bfloat16) for n in range(4))
-    plus_ref[:half] = two[:half]
-    plus_ref[half:] = one[half:]
-    minus_ref[:half] = two[half:]
-    minus_ref[half:] = three[:half]
-    one_ref[...] = one[:half]
-    three_ref[...] = three[half:]
-    here_ref[...] = here
+    for n in range(4):
+        down_copy(n).wait()
+    two = dot_nt(h_ref[...], d_ref[2]).astype(jnp.bfloat16)
+    lo_ref[...] = two[:half]
+    hi_ref[...] = two[half:]
+    for n, ref in ((1, one_ref), (3, three_ref), (0, here_ref)):
+        ref[...] = dot_nt(h_ref[...], d_ref[n]).astype(jnp.bfloat16)
 
 
 def mixer(where, normed, full, block):
@@ -342,7 +343,7 @@
     part = jax.ShapeDtypeStruct((tok // 2, block), jnp.bfloat16)
     return pl.pallas_call(
         mixer_kernel,
-        out_shape=(whole, whole, part, part, whole),
+        out_shape=(part, part, whole, whole, whole),
         in_specs=[SMEM, VMEM, pl.BlockSpec(memory_space=pl.ANY)],
         out_specs=(VMEM,) * 5,
         scratch_shapes=[
@@ -406,18 +407,20 @@
     own, normed = project(where, ngain, att, ow, res, extra)
 
     width = res.shape[1]
-    plus, minus, one_lo, three_hi, here = mixer(where, normed, full, width)
+    lo, hi, one, three, here = mixer(where, normed, full, width)
 
     def wide(a):
         return a.astype(jnp.float32)
 
-    plus = shift(plus, "x", 4, 1)
-    minus = shift(minus, "x", 4, -1)
-    left_lo = shift((wide(one_lo) + wide(plus[:half])).astype(jnp.bfloat16), "x", 4, 1)
-    right_hi = shift((wide(three_hi) + wide(minus[:half])).astype(jnp.bfloat16), "x", 4, -1)
+    from_left = shift(lo, "x", 4, 1)
+    from_right = shift(hi, "x", 4, -1)
+    left_hi = shift(one[half:], "x", 4, 1)
+    right_lo = shift(three[:half], "x", 4, -1)
+    left_lo = shift((wide(one[:half]) + wide(from_left)).astype(jnp.bfloat16), "x", 4, 1)
+    right_hi = shift((wide(three[half:]) + wide(from_right)).astype(jnp.bfloat16), "x", 4, -1)
     near = wide(own) + wide(here)
-    first = near[:half] + wide(minus[half:]) + wide(left_lo)
-    second = near[half:] + wide(plus[half:]) + wide(right_hi)
+    first = near[:half] + wide(right_lo) + wide(left_lo)
+    second = near[half:] + wide(left_hi) + wide(right_hi)
     return jnp.concatenate([first, second], axis=0).astype(jnp.bfloat16)
 
 

time: 164 us -> 164 us (level)
  the two profiles are of different devices: /device:TPU:1 before, /device:TPU:8 now
where the time goes in v2:
time: 164 us
  waiting for transfers between devices  56.9 us (35%)
  starting transfers between devices  50.2 us (31%)
  Pallas kernels  36.1 us (22%)
  between operations  14.4 us (9%)
  local copies, waits for them, and re-layouts  3.57 us (2%)
  other arithmetic  2.96 us (2%)
    ppermute x31, waiting for transfers between devices, shift(): return lax.ppermute(a, axis, [(i, (i + by) % count) for i in range(count)])  56.9 us
    ppermute x31, starting transfers between devices, shift(): return lax.ppermute(a, axis, [(i, (i + by) % count) for i in range(count)])  50.2 us
    pallas_call x2, Pallas kernels, attention(): pl.pallas_call(functools.partial(attention_kernel, steps, bool(before)),...  20.6 us
    pallas_call x1, Pallas kernels, mixer(): pl.pallas_call(mixer_kernel, out_shape=(part, part, whole, whole, whole),...  10.3 us
  transfers between devices with their start and end apart: 32, of which 14 were waited for; matrix products, arithmetic and copies ran while one was open for 2% of the time, Pallas kernels for 16%

profile of v2, /device:TPU:8, one launch (start us, length us, event | category | flops | bytes accessed | tf_op | source)
XLA Modules:
  0.0 164.2 jit_solution(2087244661422280473)
XLA Ops:
  6.5 1.8 %pad_maximum_fusion.3 = bf16[32,4224]{1,0:T(8,128)(2,1)} fusion(bf16[32,1408]{1,0:T(8,128)(2,1)} %bitcast.17, bf16[32,1408]{1,0:T(8,128)(2,1)} %param.24, bf16[32,1408]{1,0:T(8,128)(2,1)} %param.23), kind=kLoop, calls=%fused_computation.4 | loop fusion | flops 811008 | bytes 540672 | tf_op jit(solution)/shard_map/concatenate | solution.py:376
  11.0 2.0 %collective-permute-start.4 = (bf16[256,512]{1,0:T(8,128)(2,1)S(1)}, bf16[256,512]{1,0:T(8,128)(2,1)S(1)}, u32[]{:S(2)}, u32[]{:S(2)}) collective-permute-start(bf16[256,512]{1,0:T(8,128)(2,1)S(1)} %constant_dynamic-update-slice_fusion.2.rest_0_), channel_id=1, source_target_pairs={{0,32},{32,64},{64,96},{96,128},{128,160},{160,192},{192,224},{224... | collective-permute-start | bytes 786440 | tf_op jit(solution)/shard_map/ppermute | solution.py:26
  13.0 4.0 %collective-permute-start.7 = (bf16[256,512]{1,0:T(8,128)(2,1)S(1)}, bf16[256,512]{1,0:T(8,128)(2,1)S(1)}, u32[]{:S(2)}, u32[]{:S(2)}) collective-permute-start(bf16[256,512]{1,0:T(8,128)(2,1)S(1)} %constant_dynamic-update-slice_fusion.2.rest_0_), channel_id=1, source_target_pairs={{0,224},{32,0},{64,32},{96,64},{128,96},{160,128},{192,160},{224,1... | collective-permute-start | bytes 786440 | tf_op jit(solution)/shard_map/ppermute | solution.py:26
  17.0 1.7 %collective-permute-start = (bf16[256,256]{1,0:T(8,128)(2,1)S(1)}, bf16[256,256]{1,0:T(8,128)(2,1)S(1)}, u32[]{:S(2)}, u32[]{:S(2)}) collective-permute-start(bf16[256,256]{1,0:T(8,128)(2,1)S(1)} %constant_dynamic-update-slice_fusion), channel_id=1, source_target_pairs={{0,8},{8,16},{16,24},{24,0},{1,9},{9,17},{17,25},{25,1},{2,10},{10... | collective-permute-start | bytes 393224 | tf_op jit(solution)/shard_map/ppermute | solution.py:26
  19.6 2.4 %collective-permute-start.2 = (bf16[256,256]{1,0:T(8,128)(2,1)S(1)}, bf16[256,256]{1,0:T(8,128)(2,1)S(1)}, u32[]{:S(2)}, u32[]{:S(2)}) collective-permute-start(bf16[256,256]{1,0:T(8,128)(2,1)S(1)} %constant_dynamic-update-slice_fusion), channel_id=1, source_target_pairs={{0,24},{8,0},{16,8},{24,16},{1,25},{9,1},{17,9},{25,17},{2,26},{10... | collective-permute-start | bytes 393224 | tf_op jit(solution)/shard_map/ppermute | solution.py:26
  23.2 3.2 %collective-permute-start.8 = (bf16[256,512]{1,0:T(8,128)(2,1)S(1)}, bf16[256,512]{1,0:T(8,128)(2,1)S(1)}, u32[]{:S(2)}, u32[]{:S(2)}) collective-permute-start(bf16[256,512]{1,0:T(8,128)(2,1)S(1)} %collective-permute-done.7.rest_2_), channel_id=1, source_target_pairs={{0,224},{32,0},{64,32},{96,64},{128,96},{160,128},{192,160},{224,1... | collective-permute-start | bytes 786440 | tf_op jit(solution)/shard_map/ppermute | solution.py:26
  27.2 6.3 %collective-permute-done.5.rest_3_ = bf16[256,512]{1,0:T(8,128)(2,1)S(1)} collective-permute-done((bf16[256,512]{1,0:T(8,128)(2,1)S(1)}, bf16[256,512]{1,0:T(8,128)(2,1)S(1)}, u32[]{:S(2)}, u32[]{:S(2)}) %collective-permute-start.5) | collective-permute-done | bytes 262176 | tf_op jit(solution)/shard_map/ppermute | solution.py:26
  33.9 3.8 %collective-permute-start.9 = (bf16[256,512]{1,0:T(8,128)(2,1)S(1)}, bf16[256,512]{1,0:T(8,128)(2,1)S(1)}, u32[]{:S(2)}, u32[]{:S(2)}) collective-permute-start(bf16[256,512]{1,0:T(8,128)(2,1)S(1)} %collective-permute-done.8.rest_4_), channel_id=1, source_target_pairs={{0,224},{32,0},{64,32},{96,64},{128,96},{160,128},{192,160},{224,1... | collective-permute-start | bytes 786440 | tf_op jit(solution)/shard_map/ppermute | solution.py:26
  37.7 6.7 %collective-permute-done.6.rest_0_ = bf16[256,512]{1,0:T(8,128)(2,1)S(1)} collective-permute-done((bf16[256,512]{1,0:T(8,128)(2,1)S(1)}, bf16[256,512]{1,0:T(8,128)(2,1)S(1)}, u32[]{:S(2)}, u32[]{:S(2)}) %collective-permute-start.6) | collective-permute-done | bytes 262176 | tf_op jit(solution)/shard_map/ppermute | solution.py:26
  45.1 4.0 %collective-permute-start.11 = (bf16[128,512]{1,0:T(8,128)(2,1)S(1)}, bf16[128,512]{1,0:T(8,128)(2,1)S(1)}, u32[]{:S(2)}, u32[]{:S(2)}) collective-permute-start(bf16[128,512]{1,0:T(8,128)(2,1)S(1)} %slice.49), channel_id=1, source_target_pairs={{0,224},{32,0},{64,32},{96,64},{128,96},{160,128},{192,160},{224,1... | collective-permute-start | bytes 393224 | tf_op jit(solution)/shard_map/ppermute | solution.py:26
  49.2 12.0 %shard_map.127 = (bf16[4,272,512]{2,1,0:T(8,128)(2,1)S(1)}, bf16[4,272,512]{2,1,0:T(8,128)(2,1)S(1)}) custom-call(s32[4]{0:T(128)S(1)} %pad_add_fusion.where_ref, bf16[4,256,256]{2,1,0:T(8,128)(2,1)S(1)} %pad_maximum_fusion.2.q_ref, bf16[4,256,256]{2,1,0:T(8,128)(2,1)S(1)} %collective-permute-done.3.other_q_ref, ...), custom_call_target="tpu_custom_call" | custom-call | flops 4026531840 | bytes 4194304 | tf_op jit(solution)/shard_map/pallas_call | solution.py:148
  61.2 8.6 %shard_map.128 = (bf16[4,272,512]{2,1,0:T(8,128)(2,1)S(1)}, bf16[4,272,512]{2,1,0:T(8,128)(2,1)S(1)}) custom-call(s32[4]{0:T(128)S(1)} %pad_add_fusion.where_ref, bf16[4,256,256]{2,1,0:T(8,128)(2,1)S(1)} %pad_maximum_fusion.2.q_ref, bf16[4,256,256]{2,1,0:T(8,128)(2,1)S(1)} %collective-permute-done.3.other_q_ref, ...), custom_call_target="tpu_custom_call" | custom-call | flops 2415919104 | bytes 4194304 | tf_op jit(solution)/shard_map/pallas_call | solution.py:148
  70.9 1.8 %collective-permute-start.19 = (bf16[128,2560]{1,0:T(8,128)(2,1)S(1)}, bf16[128,2560]{1,0:T(8,128)(2,1)S(1)}, u32[]{:S(2)}, u32[]{:S(2)}) collective-permute-start(bf16[128,2560]{1,0:T(8,128)(2,1)S(1)} %pad_maximum_fusion), channel_id=1, source_target_pairs={{0,1},{1,2},{2,3},{3,0},{4,5},{5,6},{6,7},{7,4},{8,9},{9,10},{10,1... | collective-permute-start | bytes 1966088 | tf_op jit(solution)/shard_map/ppermute | solution.py:26
  72.7 1.6 collective-permute-start.22
  74.3 1.2 merge_cores.1
  75.6 3.3 %collective-permute-start.14 = (bf16[272,512]{1,0:T(8,128)(2,1)S(1)}, bf16[272,512]{1,0:T(8,128)(2,1)S(1)}, u32[]{:S(2)}, u32[]{:S(2)}) collective-permute-start(bf16[272,512]{1,0:T(8,128)(2,1)S(1)} %get-tuple-element.26), channel_id=1, source_target_pairs={{0,16},{8,24},{16,0},{24,8},{1,17},{9,25},{17,1},{25,9},{2,18},{10... | collective-permute-start | bytes 835592 | tf_op jit(solution)/shard_map/ppermute | solution.py:26
  79.6 10.2 %collective-permute-done.19.refs_6_ = bf16[128,2560]{1,0:T(8,128)(2,1)S(1)} collective-permute-done((bf16[128,2560]{1,0:T(8,128)(2,1)S(1)}, bf16[128,2560]{1,0:T(8,128)(2,1)S(1)}, u32[]{:S(2)}, u32[]{:S(2)}) %collective-permute-start.19) | collective-permute-done | bytes 655392 | tf_op jit(solution)/shard_map/ppermute | solution.py:26
  89.8 1.9 %collective-permute-start.24 = (bf16[128,2560]{1,0:T(8,128)(2,1)S(1)}, bf16[128,2560]{1,0:T(8,128)(2,1)S(1)}, u32[]{:S(2)}, u32[]{:S(2)}) collective-permute-start(bf16[128,2560]{1,0:T(8,128)(2,1)S(1)} %pad_maximum_fusion), channel_id=1, source_target_pairs={{0,3},{1,0},{2,1},{3,2},{4,7},{5,4},{6,5},{7,6},{8,11},{9,8},{10,9... | collective-permute-start | bytes 1966088 | tf_op jit(solution)/shard_map/ppermute | solution.py:26
  91.6 1.7 %collective-permute-start.15 = (bf16[272,512]{1,0:T(8,128)(2,1)S(1)}, bf16[272,512]{1,0:T(8,128)(2,1)S(1)}, u32[]{:S(2)}, u32[]{:S(2)}) collective-permute-start(bf16[272,512]{1,0:T(8,128)(2,1)S(1)} %get-tuple-element.27), channel_id=1, source_target_pairs={{0,8},{8,16},{16,24},{24,0},{1,9},{9,17},{17,25},{25,1},{2,10},{10... | collective-permute-start | bytes 835592 | tf_op jit(solution)/shard_map/ppermute | solution.py:26
  93.7 10.2 %collective-permute-done.14.refs_2_ = bf16[272,512]{1,0:T(8,128)(2,1)S(1)} collective-permute-done((bf16[272,512]{1,0:T(8,128)(2,1)S(1)}, bf16[272,512]{1,0:T(8,128)(2,1)S(1)}, u32[]{:S(2)}, u32[]{:S(2)}) %collective-permute-start.14) | collective-permute-done | bytes 278560 | tf_op jit(solution)/shard_map/ppermute | solution.py:26
  103.9 2.3 %collective-permute-start.23 = (bf16[128,2560]{1,0:T(8,128)(2,1)S(1)}, bf16[128,2560]{1,0:T(8,128)(2,1)S(1)}, u32[]{:S(2)}, u32[]{:S(2)}) collective-permute-start(bf16[128,2560]{1,0:T(8,128)(2,1)S(1)} %collective-permute-done.22.refs_11_), channel_id=1, source_target_pairs={{0,3},{1,0},{2,1},{3,2},{4,7},{5,4},{6,5},{7,6},{8,11},{9,8},{10,9... | collective-permute-start | bytes 1966088 | tf_op jit(solution)/shard_map/ppermute | solution.py:26
  107.8 2.2 %collective-permute-start.17 = (bf16[256,256]{1,0:T(8,128)(2,1)S(1)}, bf16[256,256]{1,0:T(8,128)(2,1)S(1)}, u32[]{:S(2)}, u32[]{:S(2)}) collective-permute-start(bf16[256,256]{1,0:T(8,128)(2,1)S(1)} %finish_heads.1.refs_0_), channel_id=1, source_target_pairs={{0,2},{1,3},{2,0},{3,1},{4,6},{5,7},{6,4},{7,5},{8,10},{9,11},{10,... | collective-permute-start | bytes 393224 | tf_op jit(solution)/shard_map/ppermute | solution.py:26
  111.1 6.8 %collective-permute-done.21.refs_8_ = bf16[128,2560]{1,0:T(8,128)(2,1)S(1)} collective-permute-done((bf16[128,2560]{1,0:T(8,128)(2,1)S(1)}, bf16[128,2560]{1,0:T(8,128)(2,1)S(1)}, u32[]{:S(2)}, u32[]{:S(2)}) %collective-permute-start.21) | collective-permute-done | bytes 655392 | tf_op jit(solution)/shard_map/ppermute | solution.py:26
  117.9 6.3 %collective-permute-done.23.refs_9_ = bf16[128,2560]{1,0:T(8,128)(2,1)S(1)} collective-permute-done((bf16[128,2560]{1,0:T(8,128)(2,1)S(1)}, bf16[128,2560]{1,0:T(8,128)(2,1)S(1)}, u32[]{:S(2)}, u32[]{:S(2)}) %collective-permute-start.23) | collective-permute-done | bytes 655392 | tf_op jit(solution)/shard_map/ppermute | solution.py:26
  124.2 1.5 collective-permute-done.18.refs_3_
  125.6 3.2 %project_norm.1 = (bf16[256,512]{1,0:T(8,128)(2,1)S(1)}, bf16[256,2048]{1,0:T(8,128)(2,1)S(1)}) custom-call(s32[4]{0:T(128)S(1)} %pad_add_fusion.where_ref, f32[1,2048]{1,0:T(1,128)S(1)} %bitcast.11, bf16[256,256]{1,0:T(8,128)(2,1)S(1)} %finish_heads.1.refs_0_, bf16[256,256]{1,0:T(8,128)(2,1)S(1)} %collective-permute-done.16.refs_1_, ...), custom_call_target="tpu_custom_call" | custom-call | flops 2000000000 | bytes 8000000 | tf_op jit(solution)/shard_map/project_norm/pallas_call | solution.py:267
  128.9 10.3 %mixer.1 = (bf16[128,512]{1,0:T(8,128)(2,1)S(1)}, bf16[128,512]{1,0:T(8,128)(2,1)S(1)}, bf16[256,512]{1,0:T(8,128)(2,1)S(1)}, bf16[256,512]{1,0:T(8,128)(2,1)S(1)}, bf16[256,512]{1,0:T(8,128)(2,1)S(1)}) custom-call(s32[4]{0:T(128)S(1)} %pad_add_fusion.where_ref, bf16[256,2048]{1,0:T(8,128)(2,1)S(1)} %get-tuple-element.29.normed_ref, ...), custom_call_target="tpu_custom_call" | custom-call | flops 4429185024 | bytes 18000000 | tf_op jit(solution)/shard_map/mixer/pallas_call | solution.py:344
  139.2 3.8 %collective-permute-start.29 = (bf16[128,512]{1,0:T(8,128)(2,1)S(1)}, bf16[128,512]{1,0:T(8,128)(2,1)S(1)}, u32[]{:S(2)}, u32[]{:S(2)}) collective-permute-start(bf16[128,512]{1,0:T(8,128)(2,1)S(1)} %get-tuple-element.34), channel_id=1, source_target_pairs={{0,3},{1,0},{2,1},{3,2},{4,7},{5,4},{6,5},{7,6},{8,11},{9,8},{10,9... | collective-permute-start | bytes 393224 | tf_op jit(solution)/shard_map/ppermute | solution.py:26
  143.0 3.3 %collective-permute-start.25 = (bf16[128,512]{1,0:T(8,128)(2,1)S(1)}, bf16[128,512]{1,0:T(8,128)(2,1)S(1)}, u32[]{:S(2)}, u32[]{:S(2)}) collective-permute-start(bf16[128,512]{1,0:T(8,128)(2,1)S(1)} %slice.43), channel_id=1, source_target_pairs={{0,3},{1,0},{2,1},{3,2},{4,7},{5,4},{6,5},{7,6},{8,11},{9,8},{10,9... | collective-permute-start | bytes 393224 | tf_op jit(solution)/shard_map/ppermute | solution.py:26
  146.5 3.6 %collective-permute-start.30 = (bf16[128,512]{1,0:T(8,128)(2,1)S(1)}, bf16[128,512]{1,0:T(8,128)(2,1)S(1)}, u32[]{:S(2)}, u32[]{:S(2)}) collective-permute-start(bf16[128,512]{1,0:T(8,128)(2,1)S(1)} %add_convert_fusion), channel_id=1, source_target_pairs={{0,3},{1,0},{2,1},{3,2},{4,7},{5,4},{6,5},{7,6},{8,11},{9,8},{10,9... | collective-permute-start | bytes 393224 | tf_op jit(solution)/shard_map/ppermute | solution.py:26
  150.4 3.5 %collective-permute-done.28 = bf16[128,512]{1,0:T(8,128)(2,1)S(1)} collective-permute-done((bf16[128,512]{1,0:T(8,128)(2,1)S(1)}, bf16[128,512]{1,0:T(8,128)(2,1)S(1)}, u32[]{:S(2)}, u32[]{:S(2)}) %collective-permute-start.28) | collective-permute-done | bytes 131104 | tf_op jit(solution)/shard_map/ppermute | solution.py:26
  153.9 2.6 %collective-permute-done.27 = bf16[128,512]{1,0:T(8,128)(2,1)S(1)} collective-permute-done((bf16[128,512]{1,0:T(8,128)(2,1)S(1)}, bf16[128,512]{1,0:T(8,128)(2,1)S(1)}, u32[]{:S(2)}, u32[]{:S(2)}) %collective-permute-start.27) | collective-permute-done | bytes 131104 | tf_op jit(solution)/shard_map/ppermute | solution.py:26
  (72 shorter events, 12.0 us)
Async XLA Ops:
  6.5 122.4 %all-gather.2.cloned.1.call-start = ((), (), s32[]{:S(2)}) async-start(), calls=%async_computation | async-start | bytes 17571840 | tf_op jit(solution)/shard_map/all_gather | solution.py:377
  11.0 12.2 %collective-permute-start.4 = (bf16[256,512]{1,0:T(8,128)(2,1)S(1)}, bf16[256,512]{1,0:T(8,128)(2,1)S(1)}, u32[]{:S(2)}, u32[]{:S(2)}) collective-permute-start(bf16[256,512]{1,0:T(8,128)(2,1)S(1)} %constant_dynamic-update-slice_fusion.2.rest_0_), channel_id=1, source_target_pairs={{0,32},{32,64},{64,96},{96,128},{128,160},{160,192},{192,224},{224... | collective-permute-start | bytes 786440 | tf_op jit(solution)/shard_map/ppermute | solution.py:26
  13.0 10.2 %collective-permute-start.7 = (bf16[256,512]{1,0:T(8,128)(2,1)S(1)}, bf16[256,512]{1,0:T(8,128)(2,1)S(1)}, u32[]{:S(2)}, u32[]{:S(2)}) collective-permute-start(bf16[256,512]{1,0:T(8,128)(2,1)S(1)} %constant_dynamic-update-slice_fusion.2.rest_0_), channel_id=1, source_target_pairs={{0,224},{32,0},{64,32},{96,64},{128,96},{160,128},{192,160},{224,1... | collective-permute-start | bytes 786440 | tf_op jit(solution)/shard_map/ppermute | solution.py:26
  17.0 9.4 %collective-permute-start = (bf16[256,256]{1,0:T(8,128)(2,1)S(1)}, bf16[256,256]{1,0:T(8,128)(2,1)S(1)}, u32[]{:S(2)}, u32[]{:S(2)}) collective-permute-start(bf16[256,256]{1,0:T(8,128)(2,1)S(1)} %constant_dynamic-update-slice_fusion), channel_id=1, source_target_pairs={{0,8},{8,16},{16,24},{24,0},{1,9},{9,17},{17,25},{25,1},{2,10},{10... | collective-permute-start | bytes 393224 | tf_op jit(solution)/shard_map/ppermute | solution.py:26
  18.7 7.8 %collective-permute-start.1 = (bf16[256,256]{1,0:T(8,128)(2,1)S(1)}, bf16[256,256]{1,0:T(8,128)(2,1)S(1)}, u32[]{:S(2)}, u32[]{:S(2)}) collective-permute-start(bf16[256,256]{1,0:T(8,128)(2,1)S(1)} %constant_dynamic-update-slice_fusion), channel_id=1, source_target_pairs={{0,16},{8,24},{16,0},{24,8},{1,17},{9,25},{17,1},{25,9},{2,18},{10... | collective-permute-start | bytes 393224 | tf_op jit(solution)/shard_map/ppermute | solution.py:26
  19.6 7.4 %collective-permute-start.2 = (bf16[256,256]{1,0:T(8,128)(2,1)S(1)}, bf16[256,256]{1,0:T(8,128)(2,1)S(1)}, u32[]{:S(2)}, u32[]{:S(2)}) collective-permute-start(bf16[256,256]{1,0:T(8,128)(2,1)S(1)} %constant_dynamic-update-slice_fusion), channel_id=1, source_target_pairs={{0,24},{8,0},{16,8},{24,16},{1,25},{9,1},{17,9},{25,17},{2,26},{10... | collective-permute-start | bytes 393224 | tf_op jit(solution)/shard_map/ppermute | solution.py:26
  23.2 10.3 %collective-permute-start.5 = (bf16[256,512]{1,0:T(8,128)(2,1)S(1)}, bf16[256,512]{1,0:T(8,128)(2,1)S(1)}, u32[]{:S(2)}, u32[]{:S(2)}) collective-permute-start(bf16[256,512]{1,0:T(8,128)(2,1)S(1)} %collective-permute-done.4.rest_1_), channel_id=1, source_target_pairs={{0,32},{32,64},{64,96},{96,128},{128,160},{160,192},{192,224},{224... | collective-permute-start | bytes 786440 | tf_op jit(solution)/shard_map/ppermute | solution.py:26
  23.2 10.7 %collective-permute-start.8 = (bf16[256,512]{1,0:T(8,128)(2,1)S(1)}, bf16[256,512]{1,0:T(8,128)(2,1)S(1)}, u32[]{:S(2)}, u32[]{:S(2)}) collective-permute-start(bf16[256,512]{1,0:T(8,128)(2,1)S(1)} %collective-permute-done.7.rest_2_), channel_id=1, source_target_pairs={{0,224},{32,0},{64,32},{96,64},{128,96},{160,128},{192,160},{224,1... | collective-permute-start | bytes 786440 | tf_op jit(solution)/shard_map/ppermute | solution.py:26
  27.1 22.1 %collective-permute-start.3 = (bf16[4,256,256]{2,1,0:T(8,128)(2,1)S(1)}, bf16[4,256,256]{2,1,0:T(8,128)(2,1)S(1)}, u32[]{:S(2)}, u32[]{:S(2)}) collective-permute-start(bf16[4,256,256]{2,1,0:T(8,128)(2,1)S(1)} %pad_maximum_fusion.2.q_ref), channel_id=1, source_target_pairs={{0,4},{4,0},{1,5},{5,1},{2,6},{6,2},{3,7},{7,3},{8,12},{12,8},{9,1... | collective-permute-start | bytes 1572872 | tf_op jit(solution)/shard_map/ppermute | solution.py:26
  33.5 10.9 %collective-permute-start.6 = (bf16[256,512]{1,0:T(8,128)(2,1)S(1)}, bf16[256,512]{1,0:T(8,128)(2,1)S(1)}, u32[]{:S(2)}, u32[]{:S(2)}) collective-permute-start(bf16[256,512]{1,0:T(8,128)(2,1)S(1)} %collective-permute-done.5.rest_3_), channel_id=1, source_target_pairs={{0,32},{32,64},{64,96},{96,128},{128,160},{160,192},{192,224},{224... | collective-permute-start | bytes 786440 | tf_op jit(solution)/shard_map/ppermute | solution.py:26
  33.9 11.3 %collective-permute-start.9 = (bf16[256,512]{1,0:T(8,128)(2,1)S(1)}, bf16[256,512]{1,0:T(8,128)(2,1)S(1)}, u32[]{:S(2)}, u32[]{:S(2)}) collective-permute-start(bf16[256,512]{1,0:T(8,128)(2,1)S(1)} %collective-permute-done.8.rest_4_), channel_id=1, source_target_pairs={{0,224},{32,0},{64,32},{96,64},{128,96},{160,128},{192,160},{224,1... | collective-permute-start | bytes 786440 | tf_op jit(solution)/shard_map/ppermute | solution.py:26
  44.4 16.8 %collective-permute-start.10 = (bf16[128,512]{1,0:T(8,128)(2,1)S(1)}, bf16[128,512]{1,0:T(8,128)(2,1)S(1)}, u32[]{:S(2)}, u32[]{:S(2)}) collective-permute-start(bf16[128,512]{1,0:T(8,128)(2,1)S(1)} %slice.48), channel_id=1, source_target_pairs={{0,32},{32,64},{64,96},{96,128},{128,160},{160,192},{192,224},{224... | collective-permute-start | bytes 393224 | tf_op jit(solution)/shard_map/ppermute | solution.py:26
  45.1 16.1 %collective-permute-start.11 = (bf16[128,512]{1,0:T(8,128)(2,1)S(1)}, bf16[128,512]{1,0:T(8,128)(2,1)S(1)}, u32[]{:S(2)}, u32[]{:S(2)}) collective-permute-start(bf16[128,512]{1,0:T(8,128)(2,1)S(1)} %slice.49), channel_id=1, source_target_pairs={{0,224},{32,0},{64,32},{96,64},{128,96},{160,128},{192,160},{224,1... | collective-permute-start | bytes 393224 | tf_op jit(solution)/shard_map/ppermute | solution.py:26
  69.9 4.5 %collective-permute-start.12 = (bf16[4,272,512]{2,1,0:T(8,128)(2,1)S(1)}, bf16[4,272,512]{2,1,0:T(8,128)(2,1)S(1)}, u32[]{:S(2)}, u32[]{:S(2)}) collective-permute-start(bf16[4,272,512]{2,1,0:T(8,128)(2,1)S(1)} %get-tuple-element.23), channel_id=1, source_target_pairs={{0,4},{4,0},{1,5},{5,1},{2,6},{6,2},{3,7},{7,3},{8,12},{12,8},{9,1... | collective-permute-start | bytes 3342344 | tf_op jit(solution)/shard_map/ppermute | solution.py:26
  70.9 18.9 %collective-permute-start.19 = (bf16[128,2560]{1,0:T(8,128)(2,1)S(1)}, bf16[128,2560]{1,0:T(8,128)(2,1)S(1)}, u32[]{:S(2)}, u32[]{:S(2)}) collective-permute-start(bf16[128,2560]{1,0:T(8,128)(2,1)S(1)} %pad_maximum_fusion), channel_id=1, source_target_pairs={{0,1},{1,2},{2,3},{3,0},{4,5},{5,6},{6,7},{7,4},{8,9},{9,10},{10,1... | collective-permute-start | bytes 1966088 | tf_op jit(solution)/shard_map/ppermute | solution.py:26
  72.7 18.9 %collective-permute-start.22 = (bf16[128,2560]{1,0:T(8,128)(2,1)S(1)}, bf16[128,2560]{1,0:T(8,128)(2,1)S(1)}, u32[]{:S(2)}, u32[]{:S(2)}) collective-permute-start(bf16[128,2560]{1,0:T(8,128)(2,1)S(1)} %pad_maximum_fusion.1), channel_id=1, source_target_pairs={{0,3},{1,0},{2,1},{3,2},{4,7},{5,4},{6,5},{7,6},{8,11},{9,8},{10,9... | collective-permute-start | bytes 1966088 | tf_op jit(solution)/shard_map/ppermute | solution.py:26
  75.5 17.8 %collective-permute-start.13 = (bf16[272,512]{1,0:T(8,128)(2,1)S(1)}, bf16[272,512]{1,0:T(8,128)(2,1)S(1)}, u32[]{:S(2)}, u32[]{:S(2)}) collective-permute-start(bf16[272,512]{1,0:T(8,128)(2,1)S(1)} %get-tuple-element.25), channel_id=1, source_target_pairs={{0,24},{8,0},{16,8},{24,16},{1,25},{9,1},{17,9},{25,17},{2,26},{10... | collective-permute-start | bytes 835592 | tf_op jit(solution)/shard_map/ppermute | solution.py:26
  75.6 28.3 %collective-permute-start.14 = (bf16[272,512]{1,0:T(8,128)(2,1)S(1)}, bf16[272,512]{1,0:T(8,128)(2,1)S(1)}, u32[]{:S(2)}, u32[]{:S(2)}) collective-permute-start(bf16[272,512]{1,0:T(8,128)(2,1)S(1)} %get-tuple-element.26), channel_id=1, source_target_pairs={{0,16},{8,24},{16,0},{24,8},{1,17},{9,25},{17,1},{25,9},{2,18},{10... | collective-permute-start | bytes 835592 | tf_op jit(solution)/shard_map/ppermute | solution.py:26
  78.9 28.8 %collective-permute-start.20 = (bf16[128,2560]{1,0:T(8,128)(2,1)S(1)}, bf16[128,2560]{1,0:T(8,128)(2,1)S(1)}, u32[]{:S(2)}, u32[]{:S(2)}) collective-permute-start(bf16[128,2560]{1,0:T(8,128)(2,1)S(1)} %pad_maximum_fusion.1), channel_id=1, source_target_pairs={{0,1},{1,2},{2,3},{3,0},{4,5},{5,6},{6,7},{7,4},{8,9},{9,10},{10,1... | collective-permute-start | bytes 1966088 | tf_op jit(solution)/shard_map/ppermute | solution.py:26
  89.8 20.2 %collective-permute-start.24 = (bf16[128,2560]{1,0:T(8,128)(2,1)S(1)}, bf16[128,2560]{1,0:T(8,128)(2,1)S(1)}, u32[]{:S(2)}, u32[]{:S(2)}) collective-permute-start(bf16[128,2560]{1,0:T(8,128)(2,1)S(1)} %pad_maximum_fusion), channel_id=1, source_target_pairs={{0,3},{1,0},{2,1},{3,2},{4,7},{5,4},{6,5},{7,6},{8,11},{9,8},{10,9... | collective-permute-start | bytes 1966088 | tf_op jit(solution)/shard_map/ppermute | solution.py:26
  91.6 15.2 %collective-permute-start.15 = (bf16[272,512]{1,0:T(8,128)(2,1)S(1)}, bf16[272,512]{1,0:T(8,128)(2,1)S(1)}, u32[]{:S(2)}, u32[]{:S(2)}) collective-permute-start(bf16[272,512]{1,0:T(8,128)(2,1)S(1)} %get-tuple-element.27), channel_id=1, source_target_pairs={{0,8},{8,16},{16,24},{24,0},{1,9},{9,17},{17,25},{25,1},{2,10},{10... | collective-permute-start | bytes 835592 | tf_op jit(solution)/shard_map/ppermute | solution.py:26
  93.3 24.6 %collective-permute-start.21 = (bf16[128,2560]{1,0:T(8,128)(2,1)S(1)}, bf16[128,2560]{1,0:T(8,128)(2,1)S(1)}, u32[]{:S(2)}, u32[]{:S(2)}) collective-permute-start(bf16[128,2560]{1,0:T(8,128)(2,1)S(1)} %collective-permute-done.19.refs_6_), channel_id=1, source_target_pairs={{0,1},{1,2},{2,3},{3,0},{4,5},{5,6},{6,7},{7,4},{8,9},{9,10},{10,1... | collective-permute-start | bytes 1966088 | tf_op jit(solution)/shard_map/ppermute | solution.py:26
  103.9 20.2 %collective-permute-start.23 = (bf16[128,2560]{1,0:T(8,128)(2,1)S(1)}, bf16[128,2560]{1,0:T(8,128)(2,1)S(1)}, u32[]{:S(2)}, u32[]{:S(2)}) collective-permute-start(bf16[128,2560]{1,0:T(8,128)(2,1)S(1)} %collective-permute-done.22.refs_11_), channel_id=1, source_target_pairs={{0,3},{1,0},{2,1},{3,2},{4,7},{5,4},{6,5},{7,6},{8,11},{9,8},{10,9... | collective-permute-start | bytes 1966088 | tf_op jit(solution)/shard_map/ppermute | solution.py:26
  107.7 16.5 %collective-permute-start.16 = (bf16[256,256]{1,0:T(8,128)(2,1)S(1)}, bf16[256,256]{1,0:T(8,128)(2,1)S(1)}, u32[]{:S(2)}, u32[]{:S(2)}) collective-permute-start(bf16[256,256]{1,0:T(8,128)(2,1)S(1)} %finish_heads.1.refs_0_), channel_id=1, source_target_pairs={{0,1},{1,2},{2,3},{3,0},{4,5},{5,6},{6,7},{7,4},{8,9},{9,10},{10,1... | collective-permute-start | bytes 393224 | tf_op jit(solution)/shard_map/ppermute | solution.py:26
  107.8 16.4 %collective-permute-start.17 = (bf16[256,256]{1,0:T(8,128)(2,1)S(1)}, bf16[256,256]{1,0:T(8,128)(2,1)S(1)}, u32[]{:S(2)}, u32[]{:S(2)}) collective-permute-start(bf16[256,256]{1,0:T(8,128)(2,1)S(1)} %finish_heads.1.refs_0_), channel_id=1, source_target_pairs={{0,2},{1,3},{2,0},{3,1},{4,6},{5,7},{6,4},{7,5},{8,10},{9,11},{10,... | collective-permute-start | bytes 393224 | tf_op jit(solution)/shard_map/ppermute | solution.py:26
  110.0 15.6 %collective-permute-start.18 = (bf16[256,256]{1,0:T(8,128)(2,1)S(1)}, bf16[256,256]{1,0:T(8,128)(2,1)S(1)}, u32[]{:S(2)}, u32[]{:S(2)}) collective-permute-start(bf16[256,256]{1,0:T(8,128)(2,1)S(1)} %finish_heads.1.refs_0_), channel_id=1, source_target_pairs={{0,3},{1,0},{2,1},{3,2},{4,7},{5,4},{6,5},{7,6},{8,11},{9,8},{10,9... | collective-permute-start | bytes 393224 | tf_op jit(solution)/shard_map/ppermute | solution.py:26
  139.2 7.2 %collective-permute-start.29 = (bf16[128,512]{1,0:T(8,128)(2,1)S(1)}, bf16[128,512]{1,0:T(8,128)(2,1)S(1)}, u32[]{:S(2)}, u32[]{:S(2)}) collective-permute-start(bf16[128,512]{1,0:T(8,128)(2,1)S(1)} %get-tuple-element.34), channel_id=1, source_target_pairs={{0,3},{1,0},{2,1},{3,2},{4,7},{5,4},{6,5},{7,6},{8,11},{9,8},{10,9... | collective-permute-start | bytes 393224 | tf_op jit(solution)/shard_map/ppermute | solution.py:26
  143.0 7.2 %collective-permute-start.26 = (bf16[128,512]{1,0:T(8,128)(2,1)S(1)}, bf16[128,512]{1,0:T(8,128)(2,1)S(1)}, u32[]{:S(2)}, u32[]{:S(2)}) collective-permute-start(bf16[128,512]{1,0:T(8,128)(2,1)S(1)} %get-tuple-element.33), channel_id=1, source_target_pairs={{0,1},{1,2},{2,3},{3,0},{4,5},{5,6},{6,7},{7,4},{8,9},{9,10},{10,1... | collective-permute-start | bytes 393224 | tf_op jit(solution)/shard_map/ppermute | solution.py:26
  143.0 7.4 %collective-permute-start.25 = (bf16[128,512]{1,0:T(8,128)(2,1)S(1)}, bf16[128,512]{1,0:T(8,128)(2,1)S(1)}, u32[]{:S(2)}, u32[]{:S(2)}) collective-permute-start(bf16[128,512]{1,0:T(8,128)(2,1)S(1)} %slice.43), channel_id=1, source_target_pairs={{0,3},{1,0},{2,1},{3,2},{4,7},{5,4},{6,5},{7,6},{8,11},{9,8},{10,9... | collective-permute-start | bytes 393224 | tf_op jit(solution)/shard_map/ppermute | solution.py:26
  146.3 7.5 %collective-permute-start.28 = (bf16[128,512]{1,0:T(8,128)(2,1)S(1)}, bf16[128,512]{1,0:T(8,128)(2,1)S(1)}, u32[]{:S(2)}, u32[]{:S(2)}) collective-permute-start(bf16[128,512]{1,0:T(8,128)(2,1)S(1)} %slice.46), channel_id=1, source_target_pairs={{0,1},{1,2},{2,3},{3,0},{4,5},{5,6},{6,7},{7,4},{8,9},{9,10},{10,1... | collective-permute-start | bytes 393224 | tf_op jit(solution)/shard_map/ppermute | solution.py:26
  146.5 7.4 %collective-permute-start.30 = (bf16[128,512]{1,0:T(8,128)(2,1)S(1)}, bf16[128,512]{1,0:T(8,128)(2,1)S(1)}, u32[]{:S(2)}, u32[]{:S(2)}) collective-permute-start(bf16[128,512]{1,0:T(8,128)(2,1)S(1)} %add_convert_fusion), channel_id=1, source_target_pairs={{0,3},{1,0},{2,1},{3,2},{4,7},{5,4},{6,5},{7,6},{8,11},{9,8},{10,9... | collective-permute-start | bytes 393224 | tf_op jit(solution)/shard_map/ppermute | solution.py:26
  150.2 6.3 %collective-permute-start.27 = (bf16[128,512]{1,0:T(8,128)(2,1)S(1)}, bf16[128,512]{1,0:T(8,128)(2,1)S(1)}, u32[]{:S(2)}, u32[]{:S(2)}) collective-permute-start(bf16[128,512]{1,0:T(8,128)(2,1)S(1)} %add_convert_fusion.1), channel_id=1, source_target_pairs={{0,1},{1,2},{2,3},{3,0},{4,5},{5,6},{6,7},{7,4},{8,9},{9,10},{10,1... | collective-permute-start | bytes 393224 | tf_op jit(solution)/shard_map/ppermute | solution.py:26
  (6 other events, 81.9 us)
Sparse Core Ops, SparseCore 0:
  10.1 115.2 all-gather.1

commit v3 on v2

--- a/solution.py
+++ b/solution.py
@@ -15,7 +15,6 @@
 FLOOR = -1e20
 SCALE2 = HEAD**-0.5 * math.log2(math.e)
 STAT = 16
-AHEAD = 4
 
 
 VMEM = pl.BlockSpec(memory_space=pltpu.VMEM)
@@ -24,6 +23,10 @@
 
 def shift(a, axis, count, by):
     return lax.ppermute(a, axis, [(i, (i + by) % count) for i in range(count)])
+
+
+def down_hop(a, hop):
+    return lax.ppermute(a, "z", [((b + 1 - hop) % 8, (b - hop) % 8) for b in range(4)])
 
 
 def dot_nt(a, b):
@@ -296,42 +299,37 @@
             for n in range(2)
         ]
 
-    def down_copy(n):
-        row = pl.multiple_of(lax.rem(where_ref[3] + n, 4) * block, block)
+    def down_copy(n, s):
+        row = pl.multiple_of(lax.rem(where_ref[3] + s, 4) * block, block)
         return pltpu.make_async_copy(
             full_ref.at[pl.ds(row, block), pl.ds(2 * units, units)], d_ref.at[n], sems.at[0, count + n]
         )
 
-    for j in range(AHEAD):
+    @pl.loop(0, count)
+    def _(j):
         for c in copies(j):
             c.start()
+
+    ahead = (2, 1, 3, 0)
+    for n, s in enumerate(ahead):
+        down_copy(n, s).start()
 
     @pl.loop(0, count)
     def _(j):
         for c in copies(j):
             c.wait()
-
-        @pl.when(j + AHEAD < count)
-        def _():
-            for c in copies(j + AHEAD):
-                c.start()
-
-        @pl.when(j + AHEAD >= count)
-        def _():
-            down_copy(j + AHEAD - count).start()
-
         both = dot_nn(normed_ref[...], w_ref[j])
         gate, up = both[:, :lane], both[:, lane:]
         cols = pl.ds(pl.multiple_of(j * lane, lane), lane)
         h_ref[:, cols] = (gate / (1.0 + jnp.exp(-gate)) * up).astype(jnp.bfloat16)
 
-    for n in range(4):
-        down_copy(n).wait()
-    two = dot_nt(h_ref[...], d_ref[2]).astype(jnp.bfloat16)
+    for n, s in enumerate(ahead):
+        down_copy(n, s).wait()
+    two = dot_nt(h_ref[...], d_ref[0]).astype(jnp.bfloat16)
     lo_ref[...] = two[:half]
     hi_ref[...] = two[half:]
-    for n, ref in ((1, one_ref), (3, three_ref), (0, here_ref)):
-        ref[...] = dot_nt(h_ref[...], d_ref[n]).astype(jnp.bfloat16)
+    for n, ref in enumerate((one_ref, three_ref, here_ref)):
+        ref[...] = dot_nt(h_ref[...], d_ref[n + 1]).astype(jnp.bfloat16)
 
 
 def mixer(where, normed, full, block):
@@ -386,11 +384,11 @@
     kv = jnp.concatenate([k1, k2, v], axis=1)
     tok = kv.shape[0]
     up, down_ring = [kv], [kv]
-    for _ in range(3):
+    for n in range(3):
         up.append(shift(up[-1], "z", 8, 1))
-        down_ring.append(shift(down_ring[-1], "z", 8, -1))
+        down_ring.append(down_hop(down_ring[-1], n + 1))
     half_up = shift(up[3][: tok // 2], "z", 8, 1)
-    half_down = shift(down_ring[3][tok // 2 :], "z", 8, -1)
+    half_down = down_hop(down_ring[3][tok // 2 :], 4)
 
     half = tok // 2
     extra = both_ways(

time: 164 us -> 169 us (1.030)
  starting transfers between devices: 50.2 us -> 57.1 us
    ppermute x0 -> x4, starting transfers between devices: none -> 22.3 us  [down_hop(): lax.ppermute(a, 'z', [((b + 1 - hop) % 8, (b - hop) % 8) for b in range(4)])]
    ppermute x31 -> x27, starting transfers between devices: 50.2 us -> 34.8 us  [shift(): return lax.ppermute(a, axis, [(i, (i + by) % count) for i in range(count)])]
    ppermute x31 -> x27, waiting for transfers between devices: 56.9 us -> 45.9 us  [shift(): return lax.ppermute(a, axis, [(i, (i + by) % count) for i in range(count)])]
    ppermute x0 -> x4, waiting for transfers between devices: none -> 9.63 us  [down_hop(): lax.ppermute(a, 'z', [((b + 1 - hop) % 8, (b - hop) % 8) for b in range(4)])]
  transfers between devices with their start and end apart: 32 -> 32, of which waited for: 14 -> 13; matrix products, arithmetic and copies ran while one was open for 2% -> 2% of each run, Pallas kernels for 16% -> 15%
where the time goes in v3:
time: 169 us
  starting transfers between devices  57.1 us (34%)
  waiting for transfers between devices  55.6 us (33%)
  Pallas kernels  34.9 us (21%)
  between operations  14.4 us (9%)
  local copies, waits for them, and re-layouts  3.58 us (2%)
  other arithmetic  2.97 us (2%)
    ppermute x27, waiting for transfers between devices, shift(): return lax.ppermute(a, axis, [(i, (i + by) % count) for i in range(count)])  45.9 us
    ppermute x27, starting transfers between devices, shift(): return lax.ppermute(a, axis, [(i, (i + by) % count) for i in range(count)])  34.8 us
    ppermute x4, starting transfers between devices, down_hop(): lax.ppermute(a, 'z', [((b + 1 - hop) % 8, (b - hop) % 8) for b in range(4)])  22.3 us
    pallas_call x2, Pallas kernels, attention(): pl.pallas_call(functools.partial(attention_kernel, steps, bool(before)),...  20.6 us
    ppermute x4, waiting for transfers between devices, down_hop(): lax.ppermute(a, 'z', [((b + 1 - hop) % 8, (b - hop) % 8) for b in range(4)])  9.63 us
    pallas_call x1, Pallas kernels, mixer(): pl.pallas_call(mixer_kernel, out_shape=(part, part, whole, whole, whole),...  9.02 us
  transfers between devices with their start and end apart: 32, of which 13 were waited for; matrix products, arithmetic and copies ran while one was open for 2% of the time, Pallas kernels for 15%

profile of v3, /device:TPU:8, one launch (start us, length us, event | category | flops | bytes accessed | tf_op | source)
XLA Modules:
  0.0 168.6 jit_solution(9802988881912228245)
XLA Ops:
  6.5 1.8 %pad_maximum_fusion.3 = bf16[32,4224]{1,0:T(8,128)(2,1)} fusion(bf16[32,1408]{1,0:T(8,128)(2,1)} %bitcast.17, bf16[32,1408]{1,0:T(8,128)(2,1)} %param.24, bf16[32,1408]{1,0:T(8,128)(2,1)} %param.23), kind=kLoop, calls=%fused_computation.4 | loop fusion | flops 811008 | bytes 540672 | tf_op jit(solution)/shard_map/concatenate | solution.py:374
  11.0 2.0 %collective-permute-start.4 = (bf16[256,512]{1,0:T(8,128)(2,1)S(1)}, bf16[256,512]{1,0:T(8,128)(2,1)S(1)}, u32[]{:S(2)}, u32[]{:S(2)}) collective-permute-start(bf16[256,512]{1,0:T(8,128)(2,1)S(1)} %constant_dynamic-update-slice_fusion.2.rest_0_), channel_id=1, source_target_pairs={{0,32},{32,64},{64,96},{96,128},{128,160},{160,192},{192,224},{224... | collective-permute-start | bytes 786440 | tf_op jit(solution)/shard_map/ppermute | solution.py:25
  13.0 5.9 %collective-permute-start.7 = (bf16[256,512]{1,0:T(8,128)(2,1)S(1)}, bf16[256,512]{1,0:T(8,128)(2,1)S(1)}, u32[]{:S(2)}, u32[]{:S(2)}) collective-permute-start(bf16[256,512]{1,0:T(8,128)(2,1)S(1)} %constant_dynamic-update-slice_fusion.2.rest_0_), channel_id=1, source_target_pairs={{0,224},{32,0},{64,32},{96,64},{1,225},{33,1},{65,33},{97,65},{2,2... | collective-permute-start | bytes 786440 | tf_op jit(solution)/shard_map/ppermute | solution.py:29
  18.9 1.7 collective-permute-start
  21.5 2.4 %collective-permute-start.2 = (bf16[256,256]{1,0:T(8,128)(2,1)S(1)}, bf16[256,256]{1,0:T(8,128)(2,1)S(1)}, u32[]{:S(2)}, u32[]{:S(2)}) collective-permute-start(bf16[256,256]{1,0:T(8,128)(2,1)S(1)} %constant_dynamic-update-slice_fusion), channel_id=1, source_target_pairs={{0,24},{8,0},{16,8},{24,16},{1,25},{9,1},{17,9},{25,17},{2,26},{10... | collective-permute-start | bytes 393224 | tf_op jit(solution)/shard_map/ppermute | solution.py:25
  24.4 5.6 %collective-permute-start.8 = (bf16[256,512]{1,0:T(8,128)(2,1)S(1)}, bf16[256,512]{1,0:T(8,128)(2,1)S(1)}, u32[]{:S(2)}, u32[]{:S(2)}) collective-permute-start(bf16[256,512]{1,0:T(8,128)(2,1)S(1)} %collective-permute-done.7.rest_2_), channel_id=1, source_target_pairs={{224,192},{0,224},{32,0},{64,32},{225,193},{1,225},{33,1},{65,33},... | collective-permute-start | bytes 786440 | tf_op jit(solution)/shard_map/ppermute | solution.py:29
  30.2 3.5 %collective-permute-done.5.rest_3_ = bf16[256,512]{1,0:T(8,128)(2,1)S(1)} collective-permute-done((bf16[256,512]{1,0:T(8,128)(2,1)S(1)}, bf16[256,512]{1,0:T(8,128)(2,1)S(1)}, u32[]{:S(2)}, u32[]{:S(2)}) %collective-permute-start.5) | collective-permute-done | bytes 262176 | tf_op jit(solution)/shard_map/ppermute | solution.py:25
  33.7 4.0 %collective-permute-done.8.rest_4_ = bf16[256,512]{1,0:T(8,128)(2,1)S(1)} collective-permute-done((bf16[256,512]{1,0:T(8,128)(2,1)S(1)}, bf16[256,512]{1,0:T(8,128)(2,1)S(1)}, u32[]{:S(2)}, u32[]{:S(2)}) %collective-permute-start.8) | collective-permute-done | bytes 262176 | tf_op jit(solution)/shard_map/ppermute | solution.py:29
  37.7 5.6 %collective-permute-start.9 = (bf16[256,512]{1,0:T(8,128)(2,1)S(1)}, bf16[256,512]{1,0:T(8,128)(2,1)S(1)}, u32[]{:S(2)}, u32[]{:S(2)}) collective-permute-start(bf16[256,512]{1,0:T(8,128)(2,1)S(1)} %collective-permute-done.8.rest_4_), channel_id=1, source_target_pairs={{192,160},{224,192},{0,224},{32,0},{193,161},{225,193},{1,225},{33... | collective-permute-start | bytes 786440 | tf_op jit(solution)/shard_map/ppermute | solution.py:29
  44.8 5.1 %collective-permute-done.9.rest_1_ = bf16[256,512]{1,0:T(8,128)(2,1)S(1)} collective-permute-done((bf16[256,512]{1,0:T(8,128)(2,1)S(1)}, bf16[256,512]{1,0:T(8,128)(2,1)S(1)}, u32[]{:S(2)}, u32[]{:S(2)}) %collective-permute-start.9) | collective-permute-done | bytes 262176 | tf_op jit(solution)/shard_map/ppermute | solution.py:29
  50.0 5.3 %collective-permute-start.11 = (bf16[128,512]{1,0:T(8,128)(2,1)S(1)}, bf16[128,512]{1,0:T(8,128)(2,1)S(1)}, u32[]{:S(2)}, u32[]{:S(2)}) collective-permute-start(bf16[128,512]{1,0:T(8,128)(2,1)S(1)} %slice.49), channel_id=1, source_target_pairs={{160,128},{192,160},{224,192},{0,224},{161,129},{193,161},{225,193... | collective-permute-start | bytes 393224 | tf_op jit(solution)/shard_map/ppermute | solution.py:29
  55.3 12.0 %shard_map.127 = (bf16[4,272,512]{2,1,0:T(8,128)(2,1)S(1)}, bf16[4,272,512]{2,1,0:T(8,128)(2,1)S(1)}) custom-call(s32[4]{0:T(128)S(1)} %pad_add_fusion.where_ref, bf16[4,256,256]{2,1,0:T(8,128)(2,1)S(1)} %pad_maximum_fusion.2.q_ref, bf16[4,256,256]{2,1,0:T(8,128)(2,1)S(1)} %collective-permute-done.3.other_q_ref, ...), custom_call_target="tpu_custom_call" | custom-call | flops 4026531840 | bytes 4194304 | tf_op jit(solution)/shard_map/pallas_call | solution.py:151
  67.3 8.6 %shard_map.128 = (bf16[4,272,512]{2,1,0:T(8,128)(2,1)S(1)}, bf16[4,272,512]{2,1,0:T(8,128)(2,1)S(1)}) custom-call(s32[4]{0:T(128)S(1)} %pad_add_fusion.where_ref, bf16[4,256,256]{2,1,0:T(8,128)(2,1)S(1)} %pad_maximum_fusion.2.q_ref, bf16[4,256,256]{2,1,0:T(8,128)(2,1)S(1)} %collective-permute-done.3.other_q_ref, ...), custom_call_target="tpu_custom_call" | custom-call | flops 2415919104 | bytes 4194304 | tf_op jit(solution)/shard_map/pallas_call | solution.py:151
  77.0 1.7 %collective-permute-start.19 = (bf16[128,2560]{1,0:T(8,128)(2,1)S(1)}, bf16[128,2560]{1,0:T(8,128)(2,1)S(1)}, u32[]{:S(2)}, u32[]{:S(2)}) collective-permute-start(bf16[128,2560]{1,0:T(8,128)(2,1)S(1)} %pad_maximum_fusion), channel_id=1, source_target_pairs={{0,1},{1,2},{2,3},{3,0},{4,5},{5,6},{6,7},{7,4},{8,9},{9,10},{10,1... | collective-permute-start | bytes 1966088 | tf_op jit(solution)/shard_map/ppermute | solution.py:25
  78.8 1.8 %collective-permute-start.22 = (bf16[128,2560]{1,0:T(8,128)(2,1)S(1)}, bf16[128,2560]{1,0:T(8,128)(2,1)S(1)}, u32[]{:S(2)}, u32[]{:S(2)}) collective-permute-start(bf16[128,2560]{1,0:T(8,128)(2,1)S(1)} %pad_maximum_fusion.1), channel_id=1, source_target_pairs={{0,3},{1,0},{2,1},{3,2},{4,7},{5,4},{6,5},{7,6},{8,11},{9,8},{10,9... | collective-permute-start | bytes 1966088 | tf_op jit(solution)/shard_map/ppermute | solution.py:25
  81.9 3.1 %collective-permute-start.14 = (bf16[272,512]{1,0:T(8,128)(2,1)S(1)}, bf16[272,512]{1,0:T(8,128)(2,1)S(1)}, u32[]{:S(2)}, u32[]{:S(2)}) collective-permute-start(bf16[272,512]{1,0:T(8,128)(2,1)S(1)} %get-tuple-element.26), channel_id=1, source_target_pairs={{0,16},{8,24},{16,0},{24,8},{1,17},{9,25},{17,1},{25,9},{2,18},{10... | collective-permute-start | bytes 835592 | tf_op jit(solution)/shard_map/ppermute | solution.py:25
  85.5 10.6 %collective-permute-done.19.refs_6_ = bf16[128,2560]{1,0:T(8,128)(2,1)S(1)} collective-permute-done((bf16[128,2560]{1,0:T(8,128)(2,1)S(1)}, bf16[128,2560]{1,0:T(8,128)(2,1)S(1)}, u32[]{:S(2)}, u32[]{:S(2)}) %collective-permute-start.19) | collective-permute-done | bytes 655392 | tf_op jit(solution)/shard_map/ppermute | solution.py:25
  96.1 1.6 collective-permute-start.24
  97.6 1.6 collective-permute-start.15
  99.7 10.1 %collective-permute-done.14.refs_2_ = bf16[272,512]{1,0:T(8,128)(2,1)S(1)} collective-permute-done((bf16[272,512]{1,0:T(8,128)(2,1)S(1)}, bf16[272,512]{1,0:T(8,128)(2,1)S(1)}, u32[]{:S(2)}, u32[]{:S(2)}) %collective-permute-start.14) | collective-permute-done | bytes 278560 | tf_op jit(solution)/shard_map/ppermute | solution.py:25
  109.9 2.0 %collective-permute-start.23 = (bf16[128,2560]{1,0:T(8,128)(2,1)S(1)}, bf16[128,2560]{1,0:T(8,128)(2,1)S(1)}, u32[]{:S(2)}, u32[]{:S(2)}) collective-permute-start(bf16[128,2560]{1,0:T(8,128)(2,1)S(1)} %collective-permute-done.22.refs_11_), channel_id=1, source_target_pairs={{0,3},{1,0},{2,1},{3,2},{4,7},{5,4},{6,5},{7,6},{8,11},{9,8},{10,9... | collective-permute-start | bytes 1966088 | tf_op jit(solution)/shard_map/ppermute | solution.py:25
  113.6 2.1 %collective-permute-start.17 = (bf16[256,256]{1,0:T(8,128)(2,1)S(1)}, bf16[256,256]{1,0:T(8,128)(2,1)S(1)}, u32[]{:S(2)}, u32[]{:S(2)}) collective-permute-start(bf16[256,256]{1,0:T(8,128)(2,1)S(1)} %finish_heads.1.refs_0_), channel_id=1, source_target_pairs={{0,2},{1,3},{2,0},{3,1},{4,6},{5,7},{6,4},{7,5},{8,10},{9,11},{10,... | collective-permute-start | bytes 393224 | tf_op jit(solution)/shard_map/ppermute | solution.py:25
  117.0 7.2 %collective-permute-done.21.refs_8_ = bf16[128,2560]{1,0:T(8,128)(2,1)S(1)} collective-permute-done((bf16[128,2560]{1,0:T(8,128)(2,1)S(1)}, bf16[128,2560]{1,0:T(8,128)(2,1)S(1)}, u32[]{:S(2)}, u32[]{:S(2)}) %collective-permute-start.21) | collective-permute-done | bytes 655392 | tf_op jit(solution)/shard_map/ppermute | solution.py:25
  124.2 5.6 %collective-permute-done.23.refs_9_ = bf16[128,2560]{1,0:T(8,128)(2,1)S(1)} collective-permute-done((bf16[128,2560]{1,0:T(8,128)(2,1)S(1)}, bf16[128,2560]{1,0:T(8,128)(2,1)S(1)}, u32[]{:S(2)}, u32[]{:S(2)}) %collective-permute-start.23) | collective-permute-done | bytes 655392 | tf_op jit(solution)/shard_map/ppermute | solution.py:25
  129.8 1.4 collective-permute-done.18.refs_3_
  131.2 3.2 %project_norm.1 = (bf16[256,512]{1,0:T(8,128)(2,1)S(1)}, bf16[256,2048]{1,0:T(8,128)(2,1)S(1)}) custom-call(s32[4]{0:T(128)S(1)} %pad_add_fusion.where_ref, f32[1,2048]{1,0:T(1,128)S(1)} %bitcast.11, bf16[256,256]{1,0:T(8,128)(2,1)S(1)} %finish_heads.1.refs_0_, bf16[256,256]{1,0:T(8,128)(2,1)S(1)} %collective-permute-done.16.refs_1_, ...), custom_call_target="tpu_custom_call" | custom-call | flops 2000000000 | bytes 8000000 | tf_op jit(solution)/shard_map/project_norm/pallas_call | solution.py:270
  134.5 9.0 %mixer.1 = (bf16[128,512]{1,0:T(8,128)(2,1)S(1)}, bf16[128,512]{1,0:T(8,128)(2,1)S(1)}, bf16[256,512]{1,0:T(8,128)(2,1)S(1)}, bf16[256,512]{1,0:T(8,128)(2,1)S(1)}, bf16[256,512]{1,0:T(8,128)(2,1)S(1)}) custom-call(s32[4]{0:T(128)S(1)} %pad_add_fusion.where_ref, bf16[256,2048]{1,0:T(8,128)(2,1)S(1)} %get-tuple-element.29.normed_ref, ...), custom_call_target="tpu_custom_call" | custom-call | flops 4429185024 | bytes 18000000 | tf_op jit(solution)/shard_map/mixer/pallas_call | solution.py:342
  143.5 3.8 %collective-permute-start.29 = (bf16[128,512]{1,0:T(8,128)(2,1)S(1)}, bf16[128,512]{1,0:T(8,128)(2,1)S(1)}, u32[]{:S(2)}, u32[]{:S(2)}) collective-permute-start(bf16[128,512]{1,0:T(8,128)(2,1)S(1)} %get-tuple-element.34), channel_id=1, source_target_pairs={{0,3},{1,0},{2,1},{3,2},{4,7},{5,4},{6,5},{7,6},{8,11},{9,8},{10,9... | collective-permute-start | bytes 393224 | tf_op jit(solution)/shard_map/ppermute | solution.py:25
  147.3 3.3 %collective-permute-start.25 = (bf16[128,512]{1,0:T(8,128)(2,1)S(1)}, bf16[128,512]{1,0:T(8,128)(2,1)S(1)}, u32[]{:S(2)}, u32[]{:S(2)}) collective-permute-start(bf16[128,512]{1,0:T(8,128)(2,1)S(1)} %slice.43), channel_id=1, source_target_pairs={{0,3},{1,0},{2,1},{3,2},{4,7},{5,4},{6,5},{7,6},{8,11},{9,8},{10,9... | collective-permute-start | bytes 393224 | tf_op jit(solution)/shard_map/ppermute | solution.py:25
  150.8 3.8 %collective-permute-start.30 = (bf16[128,512]{1,0:T(8,128)(2,1)S(1)}, bf16[128,512]{1,0:T(8,128)(2,1)S(1)}, u32[]{:S(2)}, u32[]{:S(2)}) collective-permute-start(bf16[128,512]{1,0:T(8,128)(2,1)S(1)} %add_convert_fusion), channel_id=1, source_target_pairs={{0,3},{1,0},{2,1},{3,2},{4,7},{5,4},{6,5},{7,6},{8,11},{9,8},{10,9... | collective-permute-start | bytes 393224 | tf_op jit(solution)/shard_map/ppermute | solution.py:25
  154.8 3.2 %collective-permute-done.28 = bf16[128,512]{1,0:T(8,128)(2,1)S(1)} collective-permute-done((bf16[128,512]{1,0:T(8,128)(2,1)S(1)}, bf16[128,512]{1,0:T(8,128)(2,1)S(1)}, u32[]{:S(2)}, u32[]{:S(2)}) %collective-permute-start.28) | collective-permute-done | bytes 131104 | tf_op jit(solution)/shard_map/ppermute | solution.py:25
  158.0 2.9 %collective-permute-done.27 = bf16[128,512]{1,0:T(8,128)(2,1)S(1)} collective-permute-done((bf16[128,512]{1,0:T(8,128)(2,1)S(1)}, bf16[128,512]{1,0:T(8,128)(2,1)S(1)}, u32[]{:S(2)}, u32[]{:S(2)}) %collective-permute-start.27) | collective-permute-done | bytes 131104 | tf_op jit(solution)/shard_map/ppermute | solution.py:25
  (72 shorter events, 12.6 us)
Async XLA Ops:
  6.5 127.9 %all-gather.2.cloned.1.call-start = ((), (), s32[]{:S(2)}) async-start(), calls=%async_computation | async-start | bytes 17571840 | tf_op jit(solution)/shard_map/all_gather | solution.py:375
  11.0 12.9 %collective-permute-start.4 = (bf16[256,512]{1,0:T(8,128)(2,1)S(1)}, bf16[256,512]{1,0:T(8,128)(2,1)S(1)}, u32[]{:S(2)}, u32[]{:S(2)}) collective-permute-start(bf16[256,512]{1,0:T(8,128)(2,1)S(1)} %constant_dynamic-update-slice_fusion.2.rest_0_), channel_id=1, source_target_pairs={{0,32},{32,64},{64,96},{96,128},{128,160},{160,192},{192,224},{224... | collective-permute-start | bytes 786440 | tf_op jit(solution)/shard_map/ppermute | solution.py:25
  13.0 11.4 %collective-permute-start.7 = (bf16[256,512]{1,0:T(8,128)(2,1)S(1)}, bf16[256,512]{1,0:T(8,128)(2,1)S(1)}, u32[]{:S(2)}, u32[]{:S(2)}) collective-permute-start(bf16[256,512]{1,0:T(8,128)(2,1)S(1)} %constant_dynamic-update-slice_fusion.2.rest_0_), channel_id=1, source_target_pairs={{0,224},{32,0},{64,32},{96,64},{1,225},{33,1},{65,33},{97,65},{2,2... | collective-permute-start | bytes 786440 | tf_op jit(solution)/shard_map/ppermute | solution.py:29
  18.9 11.1 %collective-permute-start = (bf16[256,256]{1,0:T(8,128)(2,1)S(1)}, bf16[256,256]{1,0:T(8,128)(2,1)S(1)}, u32[]{:S(2)}, u32[]{:S(2)}) collective-permute-start(bf16[256,256]{1,0:T(8,128)(2,1)S(1)} %constant_dynamic-update-slice_fusion), channel_id=1, source_target_pairs={{0,8},{8,16},{16,24},{24,0},{1,9},{9,17},{17,25},{25,1},{2,10},{10... | collective-permute-start | bytes 393224 | tf_op jit(solution)/shard_map/ppermute | solution.py:25
  20.6 9.4 %collective-permute-start.1 = (bf16[256,256]{1,0:T(8,128)(2,1)S(1)}, bf16[256,256]{1,0:T(8,128)(2,1)S(1)}, u32[]{:S(2)}, u32[]{:S(2)}) collective-permute-start(bf16[256,256]{1,0:T(8,128)(2,1)S(1)} %constant_dynamic-update-slice_fusion), channel_id=1, source_target_pairs={{0,16},{8,24},{16,0},{24,8},{1,17},{9,25},{17,1},{25,9},{2,18},{10... | collective-permute-start | bytes 393224 | tf_op jit(solution)/shard_map/ppermute | solution.py:25
  21.5 8.5 %collective-permute-start.2 = (bf16[256,256]{1,0:T(8,128)(2,1)S(1)}, bf16[256,256]{1,0:T(8,128)(2,1)S(1)}, u32[]{:S(2)}, u32[]{:S(2)}) collective-permute-start(bf16[256,256]{1,0:T(8,128)(2,1)S(1)} %constant_dynamic-update-slice_fusion), channel_id=1, source_target_pairs={{0,24},{8,0},{16,8},{24,16},{1,25},{9,1},{17,9},{25,17},{2,26},{10... | collective-permute-start | bytes 393224 | tf_op jit(solution)/shard_map/ppermute | solution.py:25
  23.9 9.8 %collective-permute-start.5 = (bf16[256,512]{1,0:T(8,128)(2,1)S(1)}, bf16[256,512]{1,0:T(8,128)(2,1)S(1)}, u32[]{:S(2)}, u32[]{:S(2)}) collective-permute-start(bf16[256,512]{1,0:T(8,128)(2,1)S(1)} %collective-permute-done.4.rest_1_), channel_id=1, source_target_pairs={{0,32},{32,64},{64,96},{96,128},{128,160},{160,192},{192,224},{224... | collective-permute-start | bytes 786440 | tf_op jit(solution)/shard_map/ppermute | solution.py:25
  24.4 13.3 %collective-permute-start.8 = (bf16[256,512]{1,0:T(8,128)(2,1)S(1)}, bf16[256,512]{1,0:T(8,128)(2,1)S(1)}, u32[]{:S(2)}, u32[]{:S(2)}) collective-permute-start(bf16[256,512]{1,0:T(8,128)(2,1)S(1)} %collective-permute-done.7.rest_2_), channel_id=1, source_target_pairs={{224,192},{0,224},{32,0},{64,32},{225,193},{1,225},{33,1},{65,33},... | collective-permute-start | bytes 786440 | tf_op jit(solution)/shard_map/ppermute | solution.py:29
  30.1 25.2 %collective-permute-start.3 = (bf16[4,256,256]{2,1,0:T(8,128)(2,1)S(1)}, bf16[4,256,256]{2,1,0:T(8,128)(2,1)S(1)}, u32[]{:S(2)}, u32[]{:S(2)}) collective-permute-start(bf16[4,256,256]{2,1,0:T(8,128)(2,1)S(1)} %pad_maximum_fusion.2.q_ref), channel_id=1, source_target_pairs={{0,4},{4,0},{1,5},{5,1},{2,6},{6,2},{3,7},{7,3},{8,12},{12,8},{9,1... | collective-permute-start | bytes 1572872 | tf_op jit(solution)/shard_map/ppermute | solution.py:25
  33.7 11.0 %collective-permute-start.6 = (bf16[256,512]{1,0:T(8,128)(2,1)S(1)}, bf16[256,512]{1,0:T(8,128)(2,1)S(1)}, u32[]{:S(2)}, u32[]{:S(2)}) collective-permute-start(bf16[256,512]{1,0:T(8,128)(2,1)S(1)} %collective-permute-done.5.rest_3_), channel_id=1, source_target_pairs={{0,32},{32,64},{64,96},{96,128},{128,160},{160,192},{192,224},{224... | collective-permute-start | bytes 786440 | tf_op jit(solution)/shard_map/ppermute | solution.py:25
  37.7 12.2 %collective-permute-start.9 = (bf16[256,512]{1,0:T(8,128)(2,1)S(1)}, bf16[256,512]{1,0:T(8,128)(2,1)S(1)}, u32[]{:S(2)}, u32[]{:S(2)}) collective-permute-start(bf16[256,512]{1,0:T(8,128)(2,1)S(1)} %collective-permute-done.8.rest_4_), channel_id=1, source_target_pairs={{192,160},{224,192},{0,224},{32,0},{193,161},{225,193},{1,225},{33... | collective-permute-start | bytes 786440 | tf_op jit(solution)/shard_map/ppermute | solution.py:29
  44.7 22.6 %collective-permute-start.10 = (bf16[128,512]{1,0:T(8,128)(2,1)S(1)}, bf16[128,512]{1,0:T(8,128)(2,1)S(1)}, u32[]{:S(2)}, u32[]{:S(2)}) collective-permute-start(bf16[128,512]{1,0:T(8,128)(2,1)S(1)} %slice.48), channel_id=1, source_target_pairs={{0,32},{32,64},{64,96},{96,128},{128,160},{160,192},{192,224},{224... | collective-permute-start | bytes 393224 | tf_op jit(solution)/shard_map/ppermute | solution.py:25
  50.0 17.4 %collective-permute-start.11 = (bf16[128,512]{1,0:T(8,128)(2,1)S(1)}, bf16[128,512]{1,0:T(8,128)(2,1)S(1)}, u32[]{:S(2)}, u32[]{:S(2)}) collective-permute-start(bf16[128,512]{1,0:T(8,128)(2,1)S(1)} %slice.49), channel_id=1, source_target_pairs={{160,128},{192,160},{224,192},{0,224},{161,129},{193,161},{225,193... | collective-permute-start | bytes 393224 | tf_op jit(solution)/shard_map/ppermute | solution.py:29
  76.0 4.7 %collective-permute-start.12 = (bf16[4,272,512]{2,1,0:T(8,128)(2,1)S(1)}, bf16[4,272,512]{2,1,0:T(8,128)(2,1)S(1)}, u32[]{:S(2)}, u32[]{:S(2)}) collective-permute-start(bf16[4,272,512]{2,1,0:T(8,128)(2,1)S(1)} %get-tuple-element.23), channel_id=1, source_target_pairs={{0,4},{4,0},{1,5},{5,1},{2,6},{6,2},{3,7},{7,3},{8,12},{12,8},{9,1... | collective-permute-start | bytes 3342344 | tf_op jit(solution)/shard_map/ppermute | solution.py:25
  77.0 19.1 %collective-permute-start.19 = (bf16[128,2560]{1,0:T(8,128)(2,1)S(1)}, bf16[128,2560]{1,0:T(8,128)(2,1)S(1)}, u32[]{:S(2)}, u32[]{:S(2)}) collective-permute-start(bf16[128,2560]{1,0:T(8,128)(2,1)S(1)} %pad_maximum_fusion), channel_id=1, source_target_pairs={{0,1},{1,2},{2,3},{3,0},{4,5},{5,6},{6,7},{7,4},{8,9},{9,10},{10,1... | collective-permute-start | bytes 1966088 | tf_op jit(solution)/shard_map/ppermute | solution.py:25
  78.8 18.9 %collective-permute-start.22 = (bf16[128,2560]{1,0:T(8,128)(2,1)S(1)}, bf16[128,2560]{1,0:T(8,128)(2,1)S(1)}, u32[]{:S(2)}, u32[]{:S(2)}) collective-permute-start(bf16[128,2560]{1,0:T(8,128)(2,1)S(1)} %pad_maximum_fusion.1), channel_id=1, source_target_pairs={{0,3},{1,0},{2,1},{3,2},{4,7},{5,4},{6,5},{7,6},{8,11},{9,8},{10,9... | collective-permute-start | bytes 1966088 | tf_op jit(solution)/shard_map/ppermute | solution.py:25
  81.8 17.4 %collective-permute-start.13 = (bf16[272,512]{1,0:T(8,128)(2,1)S(1)}, bf16[272,512]{1,0:T(8,128)(2,1)S(1)}, u32[]{:S(2)}, u32[]{:S(2)}) collective-permute-start(bf16[272,512]{1,0:T(8,128)(2,1)S(1)} %get-tuple-element.25), channel_id=1, source_target_pairs={{0,24},{8,0},{16,8},{24,16},{1,25},{9,1},{17,9},{25,17},{2,26},{10... | collective-permute-start | bytes 835592 | tf_op jit(solution)/shard_map/ppermute | solution.py:25
  81.9 27.9 %collective-permute-start.14 = (bf16[272,512]{1,0:T(8,128)(2,1)S(1)}, bf16[272,512]{1,0:T(8,128)(2,1)S(1)}, u32[]{:S(2)}, u32[]{:S(2)}) collective-permute-start(bf16[272,512]{1,0:T(8,128)(2,1)S(1)} %get-tuple-element.26), channel_id=1, source_target_pairs={{0,16},{8,24},{16,0},{24,8},{1,17},{9,25},{17,1},{25,9},{2,18},{10... | collective-permute-start | bytes 835592 | tf_op jit(solution)/shard_map/ppermute | solution.py:25
  85.0 28.6 %collective-permute-start.20 = (bf16[128,2560]{1,0:T(8,128)(2,1)S(1)}, bf16[128,2560]{1,0:T(8,128)(2,1)S(1)}, u32[]{:S(2)}, u32[]{:S(2)}) collective-permute-start(bf16[128,2560]{1,0:T(8,128)(2,1)S(1)} %pad_maximum_fusion.1), channel_id=1, source_target_pairs={{0,1},{1,2},{2,3},{3,0},{4,5},{5,6},{6,7},{7,4},{8,9},{9,10},{10,1... | collective-permute-start | bytes 1966088 | tf_op jit(solution)/shard_map/ppermute | solution.py:25
  96.1 19.7 %collective-permute-start.24 = (bf16[128,2560]{1,0:T(8,128)(2,1)S(1)}, bf16[128,2560]{1,0:T(8,128)(2,1)S(1)}, u32[]{:S(2)}, u32[]{:S(2)}) collective-permute-start(bf16[128,2560]{1,0:T(8,128)(2,1)S(1)} %pad_maximum_fusion), channel_id=1, source_target_pairs={{0,3},{1,0},{2,1},{3,2},{4,7},{5,4},{6,5},{7,6},{8,11},{9,8},{10,9... | collective-permute-start | bytes 1966088 | tf_op jit(solution)/shard_map/ppermute | solution.py:25
  97.6 14.9 %collective-permute-start.15 = (bf16[272,512]{1,0:T(8,128)(2,1)S(1)}, bf16[272,512]{1,0:T(8,128)(2,1)S(1)}, u32[]{:S(2)}, u32[]{:S(2)}) collective-permute-start(bf16[272,512]{1,0:T(8,128)(2,1)S(1)} %get-tuple-element.27), channel_id=1, source_target_pairs={{0,8},{8,16},{16,24},{24,0},{1,9},{9,17},{17,25},{25,1},{2,10},{10... | collective-permute-start | bytes 835592 | tf_op jit(solution)/shard_map/ppermute | solution.py:25
  99.2 24.9 %collective-permute-start.21 = (bf16[128,2560]{1,0:T(8,128)(2,1)S(1)}, bf16[128,2560]{1,0:T(8,128)(2,1)S(1)}, u32[]{:S(2)}, u32[]{:S(2)}) collective-permute-start(bf16[128,2560]{1,0:T(8,128)(2,1)S(1)} %collective-permute-done.19.refs_6_), channel_id=1, source_target_pairs={{0,1},{1,2},{2,3},{3,0},{4,5},{5,6},{6,7},{7,4},{8,9},{9,10},{10,1... | collective-permute-start | bytes 1966088 | tf_op jit(solution)/shard_map/ppermute | solution.py:25
  109.9 19.9 %collective-permute-start.23 = (bf16[128,2560]{1,0:T(8,128)(2,1)S(1)}, bf16[128,2560]{1,0:T(8,128)(2,1)S(1)}, u32[]{:S(2)}, u32[]{:S(2)}) collective-permute-start(bf16[128,2560]{1,0:T(8,128)(2,1)S(1)} %collective-permute-done.22.refs_11_), channel_id=1, source_target_pairs={{0,3},{1,0},{2,1},{3,2},{4,7},{5,4},{6,5},{7,6},{8,11},{9,8},{10,9... | collective-permute-start | bytes 1966088 | tf_op jit(solution)/shard_map/ppermute | solution.py:25
  113.4 16.4 %collective-permute-start.16 = (bf16[256,256]{1,0:T(8,128)(2,1)S(1)}, bf16[256,256]{1,0:T(8,128)(2,1)S(1)}, u32[]{:S(2)}, u32[]{:S(2)}) collective-permute-start(bf16[256,256]{1,0:T(8,128)(2,1)S(1)} %finish_heads.1.refs_0_), channel_id=1, source_target_pairs={{0,1},{1,2},{2,3},{3,0},{4,5},{5,6},{6,7},{7,4},{8,9},{9,10},{10,1... | collective-permute-start | bytes 393224 | tf_op jit(solution)/shard_map/ppermute | solution.py:25
  113.6 16.2 %collective-permute-start.17 = (bf16[256,256]{1,0:T(8,128)(2,1)S(1)}, bf16[256,256]{1,0:T(8,128)(2,1)S(1)}, u32[]{:S(2)}, u32[]{:S(2)}) collective-permute-start(bf16[256,256]{1,0:T(8,128)(2,1)S(1)} %finish_heads.1.refs_0_), channel_id=1, source_target_pairs={{0,2},{1,3},{2,0},{3,1},{4,6},{5,7},{6,4},{7,5},{8,10},{9,11},{10,... | collective-permute-start | bytes 393224 | tf_op jit(solution)/shard_map/ppermute | solution.py:25
  115.8 15.4 %collective-permute-start.18 = (bf16[256,256]{1,0:T(8,128)(2,1)S(1)}, bf16[256,256]{1,0:T(8,128)(2,1)S(1)}, u32[]{:S(2)}, u32[]{:S(2)}) collective-permute-start(bf16[256,256]{1,0:T(8,128)(2,1)S(1)} %finish_heads.1.refs_0_), channel_id=1, source_target_pairs={{0,3},{1,0},{2,1},{3,2},{4,7},{5,4},{6,5},{7,6},{8,11},{9,8},{10,9... | collective-permute-start | bytes 393224 | tf_op jit(solution)/shard_map/ppermute | solution.py:25
  143.5 7.2 %collective-permute-start.29 = (bf16[128,512]{1,0:T(8,128)(2,1)S(1)}, bf16[128,512]{1,0:T(8,128)(2,1)S(1)}, u32[]{:S(2)}, u32[]{:S(2)}) collective-permute-start(bf16[128,512]{1,0:T(8,128)(2,1)S(1)} %get-tuple-element.34), channel_id=1, source_target_pairs={{0,3},{1,0},{2,1},{3,2},{4,7},{5,4},{6,5},{7,6},{8,11},{9,8},{10,9... | collective-permute-start | bytes 393224 | tf_op jit(solution)/shard_map/ppermute | solution.py:25
  147.3 7.3 %collective-permute-start.26 = (bf16[128,512]{1,0:T(8,128)(2,1)S(1)}, bf16[128,512]{1,0:T(8,128)(2,1)S(1)}, u32[]{:S(2)}, u32[]{:S(2)}) collective-permute-start(bf16[128,512]{1,0:T(8,128)(2,1)S(1)} %get-tuple-element.33), channel_id=1, source_target_pairs={{0,1},{1,2},{2,3},{3,0},{4,5},{5,6},{6,7},{7,4},{8,9},{9,10},{10,1... | collective-permute-start | bytes 393224 | tf_op jit(solution)/shard_map/ppermute | solution.py:25
  147.3 7.5 %collective-permute-start.25 = (bf16[128,512]{1,0:T(8,128)(2,1)S(1)}, bf16[128,512]{1,0:T(8,128)(2,1)S(1)}, u32[]{:S(2)}, u32[]{:S(2)}) collective-permute-start(bf16[128,512]{1,0:T(8,128)(2,1)S(1)} %slice.43), channel_id=1, source_target_pairs={{0,3},{1,0},{2,1},{3,2},{4,7},{5,4},{6,5},{7,6},{8,11},{9,8},{10,9... | collective-permute-start | bytes 393224 | tf_op jit(solution)/shard_map/ppermute | solution.py:25
  150.6 7.4 %collective-permute-start.28 = (bf16[128,512]{1,0:T(8,128)(2,1)S(1)}, bf16[128,512]{1,0:T(8,128)(2,1)S(1)}, u32[]{:S(2)}, u32[]{:S(2)}) collective-permute-start(bf16[128,512]{1,0:T(8,128)(2,1)S(1)} %slice.46), channel_id=1, source_target_pairs={{0,1},{1,2},{2,3},{3,0},{4,5},{5,6},{6,7},{7,4},{8,9},{9,10},{10,1... | collective-permute-start | bytes 393224 | tf_op jit(solution)/shard_map/ppermute | solution.py:25
  150.8 7.3 %collective-permute-start.30 = (bf16[128,512]{1,0:T(8,128)(2,1)S(1)}, bf16[128,512]{1,0:T(8,128)(2,1)S(1)}, u32[]{:S(2)}, u32[]{:S(2)}) collective-permute-start(bf16[128,512]{1,0:T(8,128)(2,1)S(1)} %add_convert_fusion), channel_id=1, source_target_pairs={{0,3},{1,0},{2,1},{3,2},{4,7},{5,4},{6,5},{7,6},{8,11},{9,8},{10,9... | collective-permute-start | bytes 393224 | tf_op jit(solution)/shard_map/ppermute | solution.py:25
  154.6 6.3 %collective-permute-start.27 = (bf16[128,512]{1,0:T(8,128)(2,1)S(1)}, bf16[128,512]{1,0:T(8,128)(2,1)S(1)}, u32[]{:S(2)}, u32[]{:S(2)}) collective-permute-start(bf16[128,512]{1,0:T(8,128)(2,1)S(1)} %add_convert_fusion.1), channel_id=1, source_target_pairs={{0,1},{1,2},{2,3},{3,0},{4,5},{5,6},{6,7},{7,4},{8,9},{9,10},{10,1... | collective-permute-start | bytes 393224 | tf_op jit(solution)/shard_map/ppermute | solution.py:25
  (6 other events, 84.9 us)
Sparse Core Ops, SparseCore 0:
  10.1 114.5 all-gather.1

commit v4 on v3

--- a/solution.py
+++ b/solution.py
@@ -23,10 +23,6 @@
 
 def shift(a, axis, count, by):
     return lax.ppermute(a, axis, [(i, (i + by) % count) for i in range(count)])
-
-
-def down_hop(a, hop):
-    return lax.ppermute(a, "z", [((b + 1 - hop) % 8, (b - hop) % 8) for b in range(4)])
 
 
 def dot_nt(a, b):
@@ -323,12 +319,12 @@
         cols = pl.ds(pl.multiple_of(j * lane, lane), lane)
         h_ref[:, cols] = (gate / (1.0 + jnp.exp(-gate)) * up).astype(jnp.bfloat16)
 
-    for n, s in enumerate(ahead):
-        down_copy(n, s).wait()
+    down_copy(0, ahead[0]).wait()
     two = dot_nt(h_ref[...], d_ref[0]).astype(jnp.bfloat16)
     lo_ref[...] = two[:half]
     hi_ref[...] = two[half:]
     for n, ref in enumerate((one_ref, three_ref, here_ref)):
+        down_copy(n + 1, ahead[n + 1]).wait()
         ref[...] = dot_nt(h_ref[...], d_ref[n + 1]).astype(jnp.bfloat16)
 
 
@@ -384,11 +380,11 @@
     kv = jnp.concatenate([k1, k2, v], axis=1)
     tok = kv.shape[0]
     up, down_ring = [kv], [kv]
-    for n in range(3):
+    for _ in range(3):
         up.append(shift(up[-1], "z", 8, 1))
-        down_ring.append(down_hop(down_ring[-1], n + 1))
+        down_ring.append(shift(down_ring[-1], "z", 8, -1))
     half_up = shift(up[3][: tok // 2], "z", 8, 1)
-    half_down = down_hop(down_ring[3][tok // 2 :], 4)
+    half_down = shift(down_ring[3][tok // 2 :], "z", 8, -1)
 
     half = tok // 2
     extra = both_ways(

time: 169 us -> 164 us (0.970)
  starting transfers between devices: 57.1 us -> 50.2 us
    ppermute x4 -> x0, starting transfers between devices: 22.3 us -> none  [down_hop(): lax.ppermute(a, 'z', [((b + 1 - hop) % 8, (b - hop) % 8) for b in range(4)])]
    ppermute x27 -> x31, starting transfers between devices: 34.8 us -> 50.2 us  [shift(): return lax.ppermute(a, axis, [(i, (i + by) % count) for i in range(count)])]
    ppermute x27 -> x31, waiting for transfers between devices: 45.9 us -> 56.9 us  [shift(): return lax.ppermute(a, axis, [(i, (i + by) % count) for i in range(count)])]
    ppermute x4 -> x0, waiting for transfers between devices: 9.63 us -> none  [down_hop(): lax.ppermute(a, 'z', [((b + 1 - hop) % 8, (b - hop) % 8) for b in range(4)])]
  transfers between devices with their start and end apart: 32 -> 32, of which waited for: 13 -> 14; matrix products, arithmetic and copies ran while one was open for 2% -> 2% of each run, Pallas kernels for 15% -> 16%
where the time goes in v4:
time: 164 us; the launch traced here: 163 us
  waiting for transfers between devices  56.9 us (35%)
  starting transfers between devices  50.2 us (31%)
  Pallas kernels  35.4 us (22%)
  between operations  14.4 us (9%)
  local copies, waits for them, and re-layouts  3.57 us (2%)
  other arithmetic  2.96 us (2%)
    ppermute x31, waiting for transfers between devices, shift(): return lax.ppermute(a, axis, [(i, (i + by) % count) for i in range(count)])  56.9 us
    ppermute x31, starting transfers between devices, shift(): return lax.ppermute(a, axis, [(i, (i + by) % count) for i in range(count)])  50.2 us
    pallas_call x2, Pallas kernels, attention(): pl.pallas_call(functools.partial(attention_kernel, steps, bool(before)),...  20.6 us
    pallas_call x1, Pallas kernels, mixer(): pl.pallas_call(mixer_kernel, out_shape=(part, part, whole, whole, whole),...  9.53 us
  transfers between devices with their start and end apart: 32, of which 14 were waited for; matrix products, arithmetic and copies ran while one was open for 2% of the time, Pallas kernels for 16%

profile of v4, /device:TPU:8, one launch (start us, length us, event | category | flops | bytes accessed | tf_op | source)
XLA Modules:
  0.0 163.4 jit_solution(3887792326394167747)
XLA Ops:
  6.5 1.8 %pad_maximum_fusion.3 = bf16[32,4224]{1,0:T(8,128)(2,1)} fusion(bf16[32,1408]{1,0:T(8,128)(2,1)} %bitcast.17, bf16[32,1408]{1,0:T(8,128)(2,1)} %param.24, bf16[32,1408]{1,0:T(8,128)(2,1)} %param.23), kind=kLoop, calls=%fused_computation.4 | loop fusion | flops 811008 | bytes 540672 | tf_op jit(solution)/shard_map/concatenate | solution.py:370
  11.0 2.0 %collective-permute-start.4 = (bf16[256,512]{1,0:T(8,128)(2,1)S(1)}, bf16[256,512]{1,0:T(8,128)(2,1)S(1)}, u32[]{:S(2)}, u32[]{:S(2)}) collective-permute-start(bf16[256,512]{1,0:T(8,128)(2,1)S(1)} %constant_dynamic-update-slice_fusion.2.rest_0_), channel_id=1, source_target_pairs={{0,32},{32,64},{64,96},{96,128},{128,160},{160,192},{192,224},{224... | collective-permute-start | bytes 786440 | tf_op jit(solution)/shard_map/ppermute | solution.py:25
  13.0 4.0 %collective-permute-start.7 = (bf16[256,512]{1,0:T(8,128)(2,1)S(1)}, bf16[256,512]{1,0:T(8,128)(2,1)S(1)}, u32[]{:S(2)}, u32[]{:S(2)}) collective-permute-start(bf16[256,512]{1,0:T(8,128)(2,1)S(1)} %constant_dynamic-update-slice_fusion.2.rest_0_), channel_id=1, source_target_pairs={{0,224},{32,0},{64,32},{96,64},{128,96},{160,128},{192,160},{224,1... | collective-permute-start | bytes 786440 | tf_op jit(solution)/shard_map/ppermute | solution.py:25
  17.0 1.7 %collective-permute-start = (bf16[256,256]{1,0:T(8,128)(2,1)S(1)}, bf16[256,256]{1,0:T(8,128)(2,1)S(1)}, u32[]{:S(2)}, u32[]{:S(2)}) collective-permute-start(bf16[256,256]{1,0:T(8,128)(2,1)S(1)} %constant_dynamic-update-slice_fusion), channel_id=1, source_target_pairs={{0,8},{8,16},{16,24},{24,0},{1,9},{9,17},{17,25},{25,1},{2,10},{10... | collective-permute-start | bytes 393224 | tf_op jit(solution)/shard_map/ppermute | solution.py:25
  19.6 2.4 %collective-permute-start.2 = (bf16[256,256]{1,0:T(8,128)(2,1)S(1)}, bf16[256,256]{1,0:T(8,128)(2,1)S(1)}, u32[]{:S(2)}, u32[]{:S(2)}) collective-permute-start(bf16[256,256]{1,0:T(8,128)(2,1)S(1)} %constant_dynamic-update-slice_fusion), channel_id=1, source_target_pairs={{0,24},{8,0},{16,8},{24,16},{1,25},{9,1},{17,9},{25,17},{2,26},{10... | collective-permute-start | bytes 393224 | tf_op jit(solution)/shard_map/ppermute | solution.py:25
  23.2 3.2 %collective-permute-start.8 = (bf16[256,512]{1,0:T(8,128)(2,1)S(1)}, bf16[256,512]{1,0:T(8,128)(2,1)S(1)}, u32[]{:S(2)}, u32[]{:S(2)}) collective-permute-start(bf16[256,512]{1,0:T(8,128)(2,1)S(1)} %collective-permute-done.7.rest_2_), channel_id=1, source_target_pairs={{0,224},{32,0},{64,32},{96,64},{128,96},{160,128},{192,160},{224,1... | collective-permute-start | bytes 786440 | tf_op jit(solution)/shard_map/ppermute | solution.py:25
  27.2 6.3 %collective-permute-done.5.rest_3_ = bf16[256,512]{1,0:T(8,128)(2,1)S(1)} collective-permute-done((bf16[256,512]{1,0:T(8,128)(2,1)S(1)}, bf16[256,512]{1,0:T(8,128)(2,1)S(1)}, u32[]{:S(2)}, u32[]{:S(2)}) %collective-permute-start.5) | collective-permute-done | bytes 262176 | tf_op jit(solution)/shard_map/ppermute | solution.py:25
  33.9 3.8 %collective-permute-start.9 = (bf16[256,512]{1,0:T(8,128)(2,1)S(1)}, bf16[256,512]{1,0:T(8,128)(2,1)S(1)}, u32[]{:S(2)}, u32[]{:S(2)}) collective-permute-start(bf16[256,512]{1,0:T(8,128)(2,1)S(1)} %collective-permute-done.8.rest_4_), channel_id=1, source_target_pairs={{0,224},{32,0},{64,32},{96,64},{128,96},{160,128},{192,160},{224,1... | collective-permute-start | bytes 786440 | tf_op jit(solution)/shard_map/ppermute | solution.py:25
  37.7 6.7 %collective-permute-done.6.rest_0_ = bf16[256,512]{1,0:T(8,128)(2,1)S(1)} collective-permute-done((bf16[256,512]{1,0:T(8,128)(2,1)S(1)}, bf16[256,512]{1,0:T(8,128)(2,1)S(1)}, u32[]{:S(2)}, u32[]{:S(2)}) %collective-permute-start.6) | collective-permute-done | bytes 262176 | tf_op jit(solution)/shard_map/ppermute | solution.py:25
  45.1 4.0 %collective-permute-start.11 = (bf16[128,512]{1,0:T(8,128)(2,1)S(1)}, bf16[128,512]{1,0:T(8,128)(2,1)S(1)}, u32[]{:S(2)}, u32[]{:S(2)}) collective-permute-start(bf16[128,512]{1,0:T(8,128)(2,1)S(1)} %slice.49), channel_id=1, source_target_pairs={{0,224},{32,0},{64,32},{96,64},{128,96},{160,128},{192,160},{224,1... | collective-permute-start | bytes 393224 | tf_op jit(solution)/shard_map/ppermute | solution.py:25
  49.2 12.0 %shard_map.127 = (bf16[4,272,512]{2,1,0:T(8,128)(2,1)S(1)}, bf16[4,272,512]{2,1,0:T(8,128)(2,1)S(1)}) custom-call(s32[4]{0:T(128)S(1)} %pad_add_fusion.where_ref, bf16[4,256,256]{2,1,0:T(8,128)(2,1)S(1)} %pad_maximum_fusion.2.q_ref, bf16[4,256,256]{2,1,0:T(8,128)(2,1)S(1)} %collective-permute-done.3.other_q_ref, ...), custom_call_target="tpu_custom_call" | custom-call | flops 4026531840 | bytes 4194304 | tf_op jit(solution)/shard_map/pallas_call | solution.py:147
  61.2 8.6 %shard_map.128 = (bf16[4,272,512]{2,1,0:T(8,128)(2,1)S(1)}, bf16[4,272,512]{2,1,0:T(8,128)(2,1)S(1)}) custom-call(s32[4]{0:T(128)S(1)} %pad_add_fusion.where_ref, bf16[4,256,256]{2,1,0:T(8,128)(2,1)S(1)} %pad_maximum_fusion.2.q_ref, bf16[4,256,256]{2,1,0:T(8,128)(2,1)S(1)} %collective-permute-done.3.other_q_ref, ...), custom_call_target="tpu_custom_call" | custom-call | flops 2415919104 | bytes 4194304 | tf_op jit(solution)/shard_map/pallas_call | solution.py:147
  70.9 1.8 %collective-permute-start.19 = (bf16[128,2560]{1,0:T(8,128)(2,1)S(1)}, bf16[128,2560]{1,0:T(8,128)(2,1)S(1)}, u32[]{:S(2)}, u32[]{:S(2)}) collective-permute-start(bf16[128,2560]{1,0:T(8,128)(2,1)S(1)} %pad_maximum_fusion), channel_id=1, source_target_pairs={{0,1},{1,2},{2,3},{3,0},{4,5},{5,6},{6,7},{7,4},{8,9},{9,10},{10,1... | collective-permute-start | bytes 1966088 | tf_op jit(solution)/shard_map/ppermute | solution.py:25
  72.7 1.6 collective-permute-start.22
  74.3 1.2 merge_cores.1
  75.6 3.3 %collective-permute-start.14 = (bf16[272,512]{1,0:T(8,128)(2,1)S(1)}, bf16[272,512]{1,0:T(8,128)(2,1)S(1)}, u32[]{:S(2)}, u32[]{:S(2)}) collective-permute-start(bf16[272,512]{1,0:T(8,128)(2,1)S(1)} %get-tuple-element.26), channel_id=1, source_target_pairs={{0,16},{8,24},{16,0},{24,8},{1,17},{9,25},{17,1},{25,9},{2,18},{10... | collective-permute-start | bytes 835592 | tf_op jit(solution)/shard_map/ppermute | solution.py:25
  79.6 10.2 %collective-permute-done.19.refs_6_ = bf16[128,2560]{1,0:T(8,128)(2,1)S(1)} collective-permute-done((bf16[128,2560]{1,0:T(8,128)(2,1)S(1)}, bf16[128,2560]{1,0:T(8,128)(2,1)S(1)}, u32[]{:S(2)}, u32[]{:S(2)}) %collective-permute-start.19) | collective-permute-done | bytes 655392 | tf_op jit(solution)/shard_map/ppermute | solution.py:25
  89.8 1.9 %collective-permute-start.24 = (bf16[128,2560]{1,0:T(8,128)(2,1)S(1)}, bf16[128,2560]{1,0:T(8,128)(2,1)S(1)}, u32[]{:S(2)}, u32[]{:S(2)}) collective-permute-start(bf16[128,2560]{1,0:T(8,128)(2,1)S(1)} %pad_maximum_fusion), channel_id=1, source_target_pairs={{0,3},{1,0},{2,1},{3,2},{4,7},{5,4},{6,5},{7,6},{8,11},{9,8},{10,9... | collective-permute-start | bytes 1966088 | tf_op jit(solution)/shard_map/ppermute | solution.py:25
  91.6 1.7 %collective-permute-start.15 = (bf16[272,512]{1,0:T(8,128)(2,1)S(1)}, bf16[272,512]{1,0:T(8,128)(2,1)S(1)}, u32[]{:S(2)}, u32[]{:S(2)}) collective-permute-start(bf16[272,512]{1,0:T(8,128)(2,1)S(1)} %get-tuple-element.27), channel_id=1, source_target_pairs={{0,8},{8,16},{16,24},{24,0},{1,9},{9,17},{17,25},{25,1},{2,10},{10... | collective-permute-start | bytes 835592 | tf_op jit(solution)/shard_map/ppermute | solution.py:25
  93.7 10.2 %collective-permute-done.14.refs_2_ = bf16[272,512]{1,0:T(8,128)(2,1)S(1)} collective-permute-done((bf16[272,512]{1,0:T(8,128)(2,1)S(1)}, bf16[272,512]{1,0:T(8,128)(2,1)S(1)}, u32[]{:S(2)}, u32[]{:S(2)}) %collective-permute-start.14) | collective-permute-done | bytes 278560 | tf_op jit(solution)/shard_map/ppermute | solution.py:25
  103.9 2.3 %collective-permute-start.23 = (bf16[128,2560]{1,0:T(8,128)(2,1)S(1)}, bf16[128,2560]{1,0:T(8,128)(2,1)S(1)}, u32[]{:S(2)}, u32[]{:S(2)}) collective-permute-start(bf16[128,2560]{1,0:T(8,128)(2,1)S(1)} %collective-permute-done.22.refs_11_), channel_id=1, source_target_pairs={{0,3},{1,0},{2,1},{3,2},{4,7},{5,4},{6,5},{7,6},{8,11},{9,8},{10,9... | collective-permute-start | bytes 1966088 | tf_op jit(solution)/shard_map/ppermute | solution.py:25
  107.8 2.2 %collective-permute-start.17 = (bf16[256,256]{1,0:T(8,128)(2,1)S(1)}, bf16[256,256]{1,0:T(8,128)(2,1)S(1)}, u32[]{:S(2)}, u32[]{:S(2)}) collective-permute-start(bf16[256,256]{1,0:T(8,128)(2,1)S(1)} %finish_heads.1.refs_0_), channel_id=1, source_target_pairs={{0,2},{1,3},{2,0},{3,1},{4,6},{5,7},{6,4},{7,5},{8,10},{9,11},{10,... | collective-permute-start | bytes 393224 | tf_op jit(solution)/shard_map/ppermute | solution.py:25
  111.1 6.8 %collective-permute-done.21.refs_8_ = bf16[128,2560]{1,0:T(8,128)(2,1)S(1)} collective-permute-done((bf16[128,2560]{1,0:T(8,128)(2,1)S(1)}, bf16[128,2560]{1,0:T(8,128)(2,1)S(1)}, u32[]{:S(2)}, u32[]{:S(2)}) %collective-permute-start.21) | collective-permute-done | bytes 655392 | tf_op jit(solution)/shard_map/ppermute | solution.py:25
  117.9 6.3 %collective-permute-done.23.refs_9_ = bf16[128,2560]{1,0:T(8,128)(2,1)S(1)} collective-permute-done((bf16[128,2560]{1,0:T(8,128)(2,1)S(1)}, bf16[128,2560]{1,0:T(8,128)(2,1)S(1)}, u32[]{:S(2)}, u32[]{:S(2)}) %collective-permute-start.23) | collective-permute-done | bytes 655392 | tf_op jit(solution)/shard_map/ppermute | solution.py:25
  124.2 1.5 collective-permute-done.18.refs_3_
  125.6 3.2 %project_norm.1 = (bf16[256,512]{1,0:T(8,128)(2,1)S(1)}, bf16[256,2048]{1,0:T(8,128)(2,1)S(1)}) custom-call(s32[4]{0:T(128)S(1)} %pad_add_fusion.where_ref, f32[1,2048]{1,0:T(1,128)S(1)} %bitcast.11, bf16[256,256]{1,0:T(8,128)(2,1)S(1)} %finish_heads.1.refs_0_, bf16[256,256]{1,0:T(8,128)(2,1)S(1)} %collective-permute-done.16.refs_1_, ...), custom_call_target="tpu_custom_call" | custom-call | flops 2000000000 | bytes 8000000 | tf_op jit(solution)/shard_map/project_norm/pallas_call | solution.py:266
  128.9 9.5 %mixer.1 = (bf16[128,512]{1,0:T(8,128)(2,1)S(1)}, bf16[128,512]{1,0:T(8,128)(2,1)S(1)}, bf16[256,512]{1,0:T(8,128)(2,1)S(1)}, bf16[256,512]{1,0:T(8,128)(2,1)S(1)}, bf16[256,512]{1,0:T(8,128)(2,1)S(1)}) custom-call(s32[4]{0:T(128)S(1)} %pad_add_fusion.where_ref, bf16[256,2048]{1,0:T(8,128)(2,1)S(1)} %get-tuple-element.29.normed_ref, ...), custom_call_target="tpu_custom_call" | custom-call | flops 4429185024 | bytes 18000000 | tf_op jit(solution)/shard_map/mixer/pallas_call | solution.py:338
  138.4 3.8 %collective-permute-start.29 = (bf16[128,512]{1,0:T(8,128)(2,1)S(1)}, bf16[128,512]{1,0:T(8,128)(2,1)S(1)}, u32[]{:S(2)}, u32[]{:S(2)}) collective-permute-start(bf16[128,512]{1,0:T(8,128)(2,1)S(1)} %get-tuple-element.34), channel_id=1, source_target_pairs={{0,3},{1,0},{2,1},{3,2},{4,7},{5,4},{6,5},{7,6},{8,11},{9,8},{10,9... | collective-permute-start | bytes 393224 | tf_op jit(solution)/shard_map/ppermute | solution.py:25
  142.2 3.3 %collective-permute-start.25 = (bf16[128,512]{1,0:T(8,128)(2,1)S(1)}, bf16[128,512]{1,0:T(8,128)(2,1)S(1)}, u32[]{:S(2)}, u32[]{:S(2)}) collective-permute-start(bf16[128,512]{1,0:T(8,128)(2,1)S(1)} %slice.43), channel_id=1, source_target_pairs={{0,3},{1,0},{2,1},{3,2},{4,7},{5,4},{6,5},{7,6},{8,11},{9,8},{10,9... | collective-permute-start | bytes 393224 | tf_op jit(solution)/shard_map/ppermute | solution.py:25
  145.7 3.6 %collective-permute-start.30 = (bf16[128,512]{1,0:T(8,128)(2,1)S(1)}, bf16[128,512]{1,0:T(8,128)(2,1)S(1)}, u32[]{:S(2)}, u32[]{:S(2)}) collective-permute-start(bf16[128,512]{1,0:T(8,128)(2,1)S(1)} %add_convert_fusion), channel_id=1, source_target_pairs={{0,3},{1,0},{2,1},{3,2},{4,7},{5,4},{6,5},{7,6},{8,11},{9,8},{10,9... | collective-permute-start | bytes 393224 | tf_op jit(solution)/shard_map/ppermute | solution.py:25
  149.6 3.5 %collective-permute-done.28 = bf16[128,512]{1,0:T(8,128)(2,1)S(1)} collective-permute-done((bf16[128,512]{1,0:T(8,128)(2,1)S(1)}, bf16[128,512]{1,0:T(8,128)(2,1)S(1)}, u32[]{:S(2)}, u32[]{:S(2)}) %collective-permute-start.28) | collective-permute-done | bytes 131104 | tf_op jit(solution)/shard_map/ppermute | solution.py:25
  153.1 2.6 %collective-permute-done.27 = bf16[128,512]{1,0:T(8,128)(2,1)S(1)} collective-permute-done((bf16[128,512]{1,0:T(8,128)(2,1)S(1)}, bf16[128,512]{1,0:T(8,128)(2,1)S(1)}, u32[]{:S(2)}, u32[]{:S(2)}) %collective-permute-start.27) | collective-permute-done | bytes 131104 | tf_op jit(solution)/shard_map/ppermute | solution.py:25
  (72 shorter events, 12.0 us)
Async XLA Ops:
  6.5 122.4 %all-gather.2.cloned.1.call-start = ((), (), s32[]{:S(2)}) async-start(), calls=%async_computation | async-start | bytes 17571840 | tf_op jit(solution)/shard_map/all_gather | solution.py:371
  11.0 12.2 %collective-permute-start.4 = (bf16[256,512]{1,0:T(8,128)(2,1)S(1)}, bf16[256,512]{1,0:T(8,128)(2,1)S(1)}, u32[]{:S(2)}, u32[]{:S(2)}) collective-permute-start(bf16[256,512]{1,0:T(8,128)(2,1)S(1)} %constant_dynamic-update-slice_fusion.2.rest_0_), channel_id=1, source_target_pairs={{0,32},{32,64},{64,96},{96,128},{128,160},{160,192},{192,224},{224... | collective-permute-start | bytes 786440 | tf_op jit(solution)/shard_map/ppermute | solution.py:25
  13.0 10.2 %collective-permute-start.7 = (bf16[256,512]{1,0:T(8,128)(2,1)S(1)}, bf16[256,512]{1,0:T(8,128)(2,1)S(1)}, u32[]{:S(2)}, u32[]{:S(2)}) collective-permute-start(bf16[256,512]{1,0:T(8,128)(2,1)S(1)} %constant_dynamic-update-slice_fusion.2.rest_0_), channel_id=1, source_target_pairs={{0,224},{32,0},{64,32},{96,64},{128,96},{160,128},{192,160},{224,1... | collective-permute-start | bytes 786440 | tf_op jit(solution)/shard_map/ppermute | solution.py:25
  17.0 9.4 %collective-permute-start = (bf16[256,256]{1,0:T(8,128)(2,1)S(1)}, bf16[256,256]{1,0:T(8,128)(2,1)S(1)}, u32[]{:S(2)}, u32[]{:S(2)}) collective-permute-start(bf16[256,256]{1,0:T(8,128)(2,1)S(1)} %constant_dynamic-update-slice_fusion), channel_id=1, source_target_pairs={{0,8},{8,16},{16,24},{24,0},{1,9},{9,17},{17,25},{25,1},{2,10},{10... | collective-permute-start | bytes 393224 | tf_op jit(solution)/shard_map/ppermute | solution.py:25
  18.7 7.8 %collective-permute-start.1 = (bf16[256,256]{1,0:T(8,128)(2,1)S(1)}, bf16[256,256]{1,0:T(8,128)(2,1)S(1)}, u32[]{:S(2)}, u32[]{:S(2)}) collective-permute-start(bf16[256,256]{1,0:T(8,128)(2,1)S(1)} %constant_dynamic-update-slice_fusion), channel_id=1, source_target_pairs={{0,16},{8,24},{16,0},{24,8},{1,17},{9,25},{17,1},{25,9},{2,18},{10... | collective-permute-start | bytes 393224 | tf_op jit(solution)/shard_map/ppermute | solution.py:25
  19.6 7.4 %collective-permute-start.2 = (bf16[256,256]{1,0:T(8,128)(2,1)S(1)}, bf16[256,256]{1,0:T(8,128)(2,1)S(1)}, u32[]{:S(2)}, u32[]{:S(2)}) collective-permute-start(bf16[256,256]{1,0:T(8,128)(2,1)S(1)} %constant_dynamic-update-slice_fusion), channel_id=1, source_target_pairs={{0,24},{8,0},{16,8},{24,16},{1,25},{9,1},{17,9},{25,17},{2,26},{10... | collective-permute-start | bytes 393224 | tf_op jit(solution)/shard_map/ppermute | solution.py:25
  23.2 10.3 %collective-permute-start.5 = (bf16[256,512]{1,0:T(8,128)(2,1)S(1)}, bf16[256,512]{1,0:T(8,128)(2,1)S(1)}, u32[]{:S(2)}, u32[]{:S(2)}) collective-permute-start(bf16[256,512]{1,0:T(8,128)(2,1)S(1)} %collective-permute-done.4.rest_1_), channel_id=1, source_target_pairs={{0,32},{32,64},{64,96},{96,128},{128,160},{160,192},{192,224},{224... | collective-permute-start | bytes 786440 | tf_op jit(solution)/shard_map/ppermute | solution.py:25
  23.2 10.7 %collective-permute-start.8 = (bf16[256,512]{1,0:T(8,128)(2,1)S(1)}, bf16[256,512]{1,0:T(8,128)(2,1)S(1)}, u32[]{:S(2)}, u32[]{:S(2)}) collective-permute-start(bf16[256,512]{1,0:T(8,128)(2,1)S(1)} %collective-permute-done.7.rest_2_), channel_id=1, source_target_pairs={{0,224},{32,0},{64,32},{96,64},{128,96},{160,128},{192,160},{224,1... | collective-permute-start | bytes 786440 | tf_op jit(solution)/shard_map/ppermute | solution.py:25
  27.1 22.1 %collective-permute-start.3 = (bf16[4,256,256]{2,1,0:T(8,128)(2,1)S(1)}, bf16[4,256,256]{2,1,0:T(8,128)(2,1)S(1)}, u32[]{:S(2)}, u32[]{:S(2)}) collective-permute-start(bf16[4,256,256]{2,1,0:T(8,128)(2,1)S(1)} %pad_maximum_fusion.2.q_ref), channel_id=1, source_target_pairs={{0,4},{4,0},{1,5},{5,1},{2,6},{6,2},{3,7},{7,3},{8,12},{12,8},{9,1... | collective-permute-start | bytes 1572872 | tf_op jit(solution)/shard_map/ppermute | solution.py:25
  33.5 10.9 %collective-permute-start.6 = (bf16[256,512]{1,0:T(8,128)(2,1)S(1)}, bf16[256,512]{1,0:T(8,128)(2,1)S(1)}, u32[]{:S(2)}, u32[]{:S(2)}) collective-permute-start(bf16[256,512]{1,0:T(8,128)(2,1)S(1)} %collective-permute-done.5.rest_3_), channel_id=1, source_target_pairs={{0,32},{32,64},{64,96},{96,128},{128,160},{160,192},{192,224},{224... | collective-permute-start | bytes 786440 | tf_op jit(solution)/shard_map/ppermute | solution.py:25
  33.9 11.3 %collective-permute-start.9 = (bf16[256,512]{1,0:T(8,128)(2,1)S(1)}, bf16[256,512]{1,0:T(8,128)(2,1)S(1)}, u32[]{:S(2)}, u32[]{:S(2)}) collective-permute-start(bf16[256,512]{1,0:T(8,128)(2,1)S(1)} %collective-permute-done.8.rest_4_), channel_id=1, source_target_pairs={{0,224},{32,0},{64,32},{96,64},{128,96},{160,128},{192,160},{224,1... | collective-permute-start | bytes 786440 | tf_op jit(solution)/shard_map/ppermute | solution.py:25
  44.4 16.8 %collective-permute-start.10 = (bf16[128,512]{1,0:T(8,128)(2,1)S(1)}, bf16[128,512]{1,0:T(8,128)(2,1)S(1)}, u32[]{:S(2)}, u32[]{:S(2)}) collective-permute-start(bf16[128,512]{1,0:T(8,128)(2,1)S(1)} %slice.48), channel_id=1, source_target_pairs={{0,32},{32,64},{64,96},{96,128},{128,160},{160,192},{192,224},{224... | collective-permute-start | bytes 393224 | tf_op jit(solution)/shard_map/ppermute | solution.py:25
  45.1 16.1 %collective-permute-start.11 = (bf16[128,512]{1,0:T(8,128)(2,1)S(1)}, bf16[128,512]{1,0:T(8,128)(2,1)S(1)}, u32[]{:S(2)}, u32[]{:S(2)}) collective-permute-start(bf16[128,512]{1,0:T(8,128)(2,1)S(1)} %slice.49), channel_id=1, source_target_pairs={{0,224},{32,0},{64,32},{96,64},{128,96},{160,128},{192,160},{224,1... | collective-permute-start | bytes 393224 | tf_op jit(solution)/shard_map/ppermute | solution.py:25
  69.9 4.5 %collective-permute-start.12 = (bf16[4,272,512]{2,1,0:T(8,128)(2,1)S(1)}, bf16[4,272,512]{2,1,0:T(8,128)(2,1)S(1)}, u32[]{:S(2)}, u32[]{:S(2)}) collective-permute-start(bf16[4,272,512]{2,1,0:T(8,128)(2,1)S(1)} %get-tuple-element.23), channel_id=1, source_target_pairs={{0,4},{4,0},{1,5},{5,1},{2,6},{6,2},{3,7},{7,3},{8,12},{12,8},{9,1... | collective-permute-start | bytes 3342344 | tf_op jit(solution)/shard_map/ppermute | solution.py:25
  70.9 18.9 %collective-permute-start.19 = (bf16[128,2560]{1,0:T(8,128)(2,1)S(1)}, bf16[128,2560]{1,0:T(8,128)(2,1)S(1)}, u32[]{:S(2)}, u32[]{:S(2)}) collective-permute-start(bf16[128,2560]{1,0:T(8,128)(2,1)S(1)} %pad_maximum_fusion), channel_id=1, source_target_pairs={{0,1},{1,2},{2,3},{3,0},{4,5},{5,6},{6,7},{7,4},{8,9},{9,10},{10,1... | collective-permute-start | bytes 1966088 | tf_op jit(solution)/shard_map/ppermute | solution.py:25
  72.7 18.9 %collective-permute-start.22 = (bf16[128,2560]{1,0:T(8,128)(2,1)S(1)}, bf16[128,2560]{1,0:T(8,128)(2,1)S(1)}, u32[]{:S(2)}, u32[]{:S(2)}) collective-permute-start(bf16[128,2560]{1,0:T(8,128)(2,1)S(1)} %pad_maximum_fusion.1), channel_id=1, source_target_pairs={{0,3},{1,0},{2,1},{3,2},{4,7},{5,4},{6,5},{7,6},{8,11},{9,8},{10,9... | collective-permute-start | bytes 1966088 | tf_op jit(solution)/shard_map/ppermute | solution.py:25
  75.5 17.8 %collective-permute-start.13 = (bf16[272,512]{1,0:T(8,128)(2,1)S(1)}, bf16[272,512]{1,0:T(8,128)(2,1)S(1)}, u32[]{:S(2)}, u32[]{:S(2)}) collective-permute-start(bf16[272,512]{1,0:T(8,128)(2,1)S(1)} %get-tuple-element.25), channel_id=1, source_target_pairs={{0,24},{8,0},{16,8},{24,16},{1,25},{9,1},{17,9},{25,17},{2,26},{10... | collective-permute-start | bytes 835592 | tf_op jit(solution)/shard_map/ppermute | solution.py:25
  75.6 28.3 %collective-permute-start.14 = (bf16[272,512]{1,0:T(8,128)(2,1)S(1)}, bf16[272,512]{1,0:T(8,128)(2,1)S(1)}, u32[]{:S(2)}, u32[]{:S(2)}) collective-permute-start(bf16[272,512]{1,0:T(8,128)(2,1)S(1)} %get-tuple-element.26), channel_id=1, source_target_pairs={{0,16},{8,24},{16,0},{24,8},{1,17},{9,25},{17,1},{25,9},{2,18},{10... | collective-permute-start | bytes 835592 | tf_op jit(solution)/shard_map/ppermute | solution.py:25
  78.9 28.8 %collective-permute-start.20 = (bf16[128,2560]{1,0:T(8,128)(2,1)S(1)}, bf16[128,2560]{1,0:T(8,128)(2,1)S(1)}, u32[]{:S(2)}, u32[]{:S(2)}) collective-permute-start(bf16[128,2560]{1,0:T(8,128)(2,1)S(1)} %pad_maximum_fusion.1), channel_id=1, source_target_pairs={{0,1},{1,2},{2,3},{3,0},{4,5},{5,6},{6,7},{7,4},{8,9},{9,10},{10,1... | collective-permute-start | bytes 1966088 | tf_op jit(solution)/shard_map/ppermute | solution.py:25
  89.8 20.2 %collective-permute-start.24 = (bf16[128,2560]{1,0:T(8,128)(2,1)S(1)}, bf16[128,2560]{1,0:T(8,128)(2,1)S(1)}, u32[]{:S(2)}, u32[]{:S(2)}) collective-permute-start(bf16[128,2560]{1,0:T(8,128)(2,1)S(1)} %pad_maximum_fusion), channel_id=1, source_target_pairs={{0,3},{1,0},{2,1},{3,2},{4,7},{5,4},{6,5},{7,6},{8,11},{9,8},{10,9... | collective-permute-start | bytes 1966088 | tf_op jit(solution)/shard_map/ppermute | solution.py:25
  91.6 15.2 %collective-permute-start.15 = (bf16[272,512]{1,0:T(8,128)(2,1)S(1)}, bf16[272,512]{1,0:T(8,128)(2,1)S(1)}, u32[]{:S(2)}, u32[]{:S(2)}) collective-permute-start(bf16[272,512]{1,0:T(8,128)(2,1)S(1)} %get-tuple-element.27), channel_id=1, source_target_pairs={{0,8},{8,16},{16,24},{24,0},{1,9},{9,17},{17,25},{25,1},{2,10},{10... | collective-permute-start | bytes 835592 | tf_op jit(solution)/shard_map/ppermute | solution.py:25
  93.3 24.6 %collective-permute-start.21 = (bf16[128,2560]{1,0:T(8,128)(2,1)S(1)}, bf16[128,2560]{1,0:T(8,128)(2,1)S(1)}, u32[]{:S(2)}, u32[]{:S(2)}) collective-permute-start(bf16[128,2560]{1,0:T(8,128)(2,1)S(1)} %collective-permute-done.19.refs_6_), channel_id=1, source_target_pairs={{0,1},{1,2},{2,3},{3,0},{4,5},{5,6},{6,7},{7,4},{8,9},{9,10},{10,1... | collective-permute-start | bytes 1966088 | tf_op jit(solution)/shard_map/ppermute | solution.py:25
  103.9 20.2 %collective-permute-start.23 = (bf16[128,2560]{1,0:T(8,128)(2,1)S(1)}, bf16[128,2560]{1,0:T(8,128)(2,1)S(1)}, u32[]{:S(2)}, u32[]{:S(2)}) collective-permute-start(bf16[128,2560]{1,0:T(8,128)(2,1)S(1)} %collective-permute-done.22.refs_11_), channel_id=1, source_target_pairs={{0,3},{1,0},{2,1},{3,2},{4,7},{5,4},{6,5},{7,6},{8,11},{9,8},{10,9... | collective-permute-start | bytes 1966088 | tf_op jit(solution)/shard_map/ppermute | solution.py:25
  107.7 16.5 %collective-permute-start.16 = (bf16[256,256]{1,0:T(8,128)(2,1)S(1)}, bf16[256,256]{1,0:T(8,128)(2,1)S(1)}, u32[]{:S(2)}, u32[]{:S(2)}) collective-permute-start(bf16[256,256]{1,0:T(8,128)(2,1)S(1)} %finish_heads.1.refs_0_), channel_id=1, source_target_pairs={{0,1},{1,2},{2,3},{3,0},{4,5},{5,6},{6,7},{7,4},{8,9},{9,10},{10,1... | collective-permute-start | bytes 393224 | tf_op jit(solution)/shard_map/ppermute | solution.py:25
  107.8 16.4 %collective-permute-start.17 = (bf16[256,256]{1,0:T(8,128)(2,1)S(1)}, bf16[256,256]{1,0:T(8,128)(2,1)S(1)}, u32[]{:S(2)}, u32[]{:S(2)}) collective-permute-start(bf16[256,256]{1,0:T(8,128)(2,1)S(1)} %finish_heads.1.refs_0_), channel_id=1, source_target_pairs={{0,2},{1,3},{2,0},{3,1},{4,6},{5,7},{6,4},{7,5},{8,10},{9,11},{10,... | collective-permute-start | bytes 393224 | tf_op jit(solution)/shard_map/ppermute | solution.py:25
  110.0 15.6 %collective-permute-start.18 = (bf16[256,256]{1,0:T(8,128)(2,1)S(1)}, bf16[256,256]{1,0:T(8,128)(2,1)S(1)}, u32[]{:S(2)}, u32[]{:S(2)}) collective-permute-start(bf16[256,256]{1,0:T(8,128)(2,1)S(1)} %finish_heads.1.refs_0_), channel_id=1, source_target_pairs={{0,3},{1,0},{2,1},{3,2},{4,7},{5,4},{6,5},{7,6},{8,11},{9,8},{10,9... | collective-permute-start | bytes 393224 | tf_op jit(solution)/shard_map/ppermute | solution.py:25
  138.4 7.2 %collective-permute-start.29 = (bf16[128,512]{1,0:T(8,128)(2,1)S(1)}, bf16[128,512]{1,0:T(8,128)(2,1)S(1)}, u32[]{:S(2)}, u32[]{:S(2)}) collective-permute-start(bf16[128,512]{1,0:T(8,128)(2,1)S(1)} %get-tuple-element.34), channel_id=1, source_target_pairs={{0,3},{1,0},{2,1},{3,2},{4,7},{5,4},{6,5},{7,6},{8,11},{9,8},{10,9... | collective-permute-start | bytes 393224 | tf_op jit(solution)/shard_map/ppermute | solution.py:25
  142.2 7.2 %collective-permute-start.26 = (bf16[128,512]{1,0:T(8,128)(2,1)S(1)}, bf16[128,512]{1,0:T(8,128)(2,1)S(1)}, u32[]{:S(2)}, u32[]{:S(2)}) collective-permute-start(bf16[128,512]{1,0:T(8,128)(2,1)S(1)} %get-tuple-element.33), channel_id=1, source_target_pairs={{0,1},{1,2},{2,3},{3,0},{4,5},{5,6},{6,7},{7,4},{8,9},{9,10},{10,1... | collective-permute-start | bytes 393224 | tf_op jit(solution)/shard_map/ppermute | solution.py:25
  142.2 7.4 %collective-permute-start.25 = (bf16[128,512]{1,0:T(8,128)(2,1)S(1)}, bf16[128,512]{1,0:T(8,128)(2,1)S(1)}, u32[]{:S(2)}, u32[]{:S(2)}) collective-permute-start(bf16[128,512]{1,0:T(8,128)(2,1)S(1)} %slice.43), channel_id=1, source_target_pairs={{0,3},{1,0},{2,1},{3,2},{4,7},{5,4},{6,5},{7,6},{8,11},{9,8},{10,9... | collective-permute-start | bytes 393224 | tf_op jit(solution)/shard_map/ppermute | solution.py:25
  145.6 7.5 %collective-permute-start.28 = (bf16[128,512]{1,0:T(8,128)(2,1)S(1)}, bf16[128,512]{1,0:T(8,128)(2,1)S(1)}, u32[]{:S(2)}, u32[]{:S(2)}) collective-permute-start(bf16[128,512]{1,0:T(8,128)(2,1)S(1)} %slice.46), channel_id=1, source_target_pairs={{0,1},{1,2},{2,3},{3,0},{4,5},{5,6},{6,7},{7,4},{8,9},{9,10},{10,1... | collective-permute-start | bytes 393224 | tf_op jit(solution)/shard_map/ppermute | solution.py:25
  145.7 7.4 %collective-permute-start.30 = (bf16[128,512]{1,0:T(8,128)(2,1)S(1)}, bf16[128,512]{1,0:T(8,128)(2,1)S(1)}, u32[]{:S(2)}, u32[]{:S(2)}) collective-permute-start(bf16[128,512]{1,0:T(8,128)(2,1)S(1)} %add_convert_fusion), channel_id=1, source_target_pairs={{0,3},{1,0},{2,1},{3,2},{4,7},{5,4},{6,5},{7,6},{8,11},{9,8},{10,9... | collective-permute-start | bytes 393224 | tf_op jit(solution)/shard_map/ppermute | solution.py:25
  149.5 6.3 %collective-permute-start.27 = (bf16[128,512]{1,0:T(8,128)(2,1)S(1)}, bf16[128,512]{1,0:T(8,128)(2,1)S(1)}, u32[]{:S(2)}, u32[]{:S(2)}) collective-permute-start(bf16[128,512]{1,0:T(8,128)(2,1)S(1)} %add_convert_fusion.1), channel_id=1, source_target_pairs={{0,1},{1,2},{2,3},{3,0},{4,5},{5,6},{6,7},{7,4},{8,9},{9,10},{10,1... | collective-permute-start | bytes 393224 | tf_op jit(solution)/shard_map/ppermute | solution.py:25
  (6 other events, 81.9 us)
Sparse Core Ops, SparseCore 0:
  10.1 115.2 all-gather.1

commit v5 on v4

--- a/solution.py
+++ b/solution.py
@@ -285,15 +285,8 @@
     half = lo_ref.shape[0]
 
     def copies(j):
-        at = pl.multiple_of(j * lane, lane)
-        return [
-            pltpu.make_async_copy(
-                full_ref.at[:, pl.ds(at + n * units, lane)],
-                w_ref.at[j, :, pl.ds(n * lane, lane)],
-                sems.at[n, j],
-            )
-            for n in range(2)
-        ]
+        at = pl.multiple_of(j * width, width)
+        return [pltpu.make_async_copy(full_ref.at[:, pl.ds(at, width)], w_ref.at[j], sems.at[0, j])]
 
     def down_copy(n, s):
         row = pl.multiple_of(lax.rem(where_ref[3] + s, 4) * block, block)
@@ -367,7 +360,10 @@
     z, y, c, x = (lax.axis_index(n).astype(jnp.int32) for n in ("z", "y", "c", "x"))
     where = jnp.stack([z, y, c, x])
 
-    both = jnp.concatenate([gw, uw, dw.T], axis=1)
+    lane = 128
+    blocks = [w.reshape(w.shape[0], -1, lane) for w in (gw, uw)]
+    turns = jnp.stack(blocks, axis=2).reshape(gw.shape[0], -1)
+    both = jnp.concatenate([turns, dw.T], axis=1)
     full = lax.all_gather(both, ("z", "y", "c"), axis=0, tiled=True)
 
     q = jnp.concatenate([q1, q2], axis=1)

time: 164 us -> 159 us (0.970)
  the two profiles are of different devices: /device:TPU:8 before, /device:TPU:1 now
where the time goes in v5:
time: 159 us
  starting transfers between devices  53.3 us (34%)
  waiting for transfers between devices  51.3 us (32%)
  Pallas kernels  35.3 us (22%)
  between operations  14.4 us (9%)
  local copies, waits for them, and re-layouts  2.53 us (2%)
  other arithmetic  1.99 us (1%)
    ppermute x31, starting transfers between devices, shift(): return lax.ppermute(a, axis, [(i, (i + by) % count) for i in range(count)])  53.3 us
    ppermute x31, waiting for transfers between devices, shift(): return lax.ppermute(a, axis, [(i, (i + by) % count) for i in range(count)])  47 us
    pallas_call x2, Pallas kernels, attention(): pl.pallas_call(functools.partial(attention_kernel, steps, bool(before)),...  20.6 us
    pallas_call x1, Pallas kernels, mixer(): pl.pallas_call(mixer_kernel, out_shape=(part, part, whole, whole, whole),...  9.5 us
    all_gather x1, waiting for transfers between devices, per_device(): full = lax.all_gather(both, ('z', 'y', 'c'), axis=0, tiled=True)  4.32 us
    pallas_call x1, Pallas kernels, project(): pl.pallas_call(project_kernel, out_shape=(jax.ShapeDtypeStruct((tok, bloc...  3.24 us
  transfers between devices with their start and end apart: 32, of which 17 were waited for; matrix products, arithmetic and copies ran while one was open for 0% of the time, Pallas kernels for 16%

profile of v5, /device:TPU:1, one launch (start us, length us, event | category | flops | bytes accessed | tf_op | source)
XLA Modules:
  0.0 158.8 jit_solution(15500015720712055215)
XLA Ops:
  9.8 2.5 %collective-permute-start.4 = (bf16[256,512]{1,0:T(8,128)(2,1)S(1)}, bf16[256,512]{1,0:T(8,128)(2,1)S(1)}, u32[]{:S(2)}, u32[]{:S(2)}) collective-permute-start(bf16[256,512]{1,0:T(8,128)(2,1)S(1)} %constant_dynamic-update-slice_fusion.2.rest_0_), channel_id=1, source_target_pairs={{0,32},{32,64},{64,96},{96,128},{128,160},{160,192},{192,224},{224... | collective-permute-start | bytes 786440 | tf_op jit(solution)/shard_map/ppermute | solution.py:25
  12.3 4.0 %collective-permute-start.7 = (bf16[256,512]{1,0:T(8,128)(2,1)S(1)}, bf16[256,512]{1,0:T(8,128)(2,1)S(1)}, u32[]{:S(2)}, u32[]{:S(2)}) collective-permute-start(bf16[256,512]{1,0:T(8,128)(2,1)S(1)} %constant_dynamic-update-slice_fusion.2.rest_0_), channel_id=1, source_target_pairs={{0,224},{32,0},{64,32},{96,64},{128,96},{160,128},{192,160},{224,1... | collective-permute-start | bytes 786440 | tf_op jit(solution)/shard_map/ppermute | solution.py:25
  17.8 2.6 %collective-permute-start.1 = (bf16[256,256]{1,0:T(8,128)(2,1)S(1)}, bf16[256,256]{1,0:T(8,128)(2,1)S(1)}, u32[]{:S(2)}, u32[]{:S(2)}) collective-permute-start(bf16[256,256]{1,0:T(8,128)(2,1)S(1)} %constant_dynamic-update-slice_fusion), channel_id=1, source_target_pairs={{0,16},{8,24},{16,0},{24,8},{1,17},{9,25},{17,1},{25,9},{2,18},{10... | collective-permute-start | bytes 393224 | tf_op jit(solution)/shard_map/ppermute | solution.py:25
  22.3 2.7 %collective-permute-start.8 = (bf16[256,512]{1,0:T(8,128)(2,1)S(1)}, bf16[256,512]{1,0:T(8,128)(2,1)S(1)}, u32[]{:S(2)}, u32[]{:S(2)}) collective-permute-start(bf16[256,512]{1,0:T(8,128)(2,1)S(1)} %collective-permute-done.7.rest_2_), channel_id=1, source_target_pairs={{0,224},{32,0},{64,32},{96,64},{128,96},{160,128},{192,160},{224,1... | collective-permute-start | bytes 786440 | tf_op jit(solution)/shard_map/ppermute | solution.py:25
  26.0 1.9 %collective-permute-start.3 = (bf16[4,256,256]{2,1,0:T(8,128)(2,1)S(1)}, bf16[4,256,256]{2,1,0:T(8,128)(2,1)S(1)}, u32[]{:S(2)}, u32[]{:S(2)}) collective-permute-start(bf16[4,256,256]{2,1,0:T(8,128)(2,1)S(1)} %pad_maximum_fusion.2.q_ref), channel_id=1, source_target_pairs={{0,4},{4,0},{1,5},{5,1},{2,6},{6,2},{3,7},{7,3},{8,12},{12,8},{9,1... | collective-permute-start | bytes 1572872 | tf_op jit(solution)/shard_map/ppermute | solution.py:25
  27.8 2.3 %collective-permute-done.5.rest_3_ = bf16[256,512]{1,0:T(8,128)(2,1)S(1)} collective-permute-done((bf16[256,512]{1,0:T(8,128)(2,1)S(1)}, bf16[256,512]{1,0:T(8,128)(2,1)S(1)}, u32[]{:S(2)}, u32[]{:S(2)}) %collective-permute-start.5) | collective-permute-done | bytes 262176 | tf_op jit(solution)/shard_map/ppermute | solution.py:25
  30.4 3.5 %collective-permute-start.9 = (bf16[256,512]{1,0:T(8,128)(2,1)S(1)}, bf16[256,512]{1,0:T(8,128)(2,1)S(1)}, u32[]{:S(2)}, u32[]{:S(2)}) collective-permute-start(bf16[256,512]{1,0:T(8,128)(2,1)S(1)} %collective-permute-done.8.rest_4_), channel_id=1, source_target_pairs={{0,224},{32,0},{64,32},{96,64},{128,96},{160,128},{192,160},{224,1... | collective-permute-start | bytes 786440 | tf_op jit(solution)/shard_map/ppermute | solution.py:25
  34.0 5.0 %collective-permute-done.6.rest_0_ = bf16[256,512]{1,0:T(8,128)(2,1)S(1)} collective-permute-done((bf16[256,512]{1,0:T(8,128)(2,1)S(1)}, bf16[256,512]{1,0:T(8,128)(2,1)S(1)}, u32[]{:S(2)}, u32[]{:S(2)}) %collective-permute-start.6) | collective-permute-done | bytes 262176 | tf_op jit(solution)/shard_map/ppermute | solution.py:25
  39.7 3.6 %collective-permute-start.11 = (bf16[128,512]{1,0:T(8,128)(2,1)S(1)}, bf16[128,512]{1,0:T(8,128)(2,1)S(1)}, u32[]{:S(2)}, u32[]{:S(2)}) collective-permute-start(bf16[128,512]{1,0:T(8,128)(2,1)S(1)} %slice.49), channel_id=1, source_target_pairs={{0,224},{32,0},{64,32},{96,64},{128,96},{160,128},{192,160},{224,1... | collective-permute-start | bytes 393224 | tf_op jit(solution)/shard_map/ppermute | solution.py:25
  43.3 12.0 %shard_map.127 = (bf16[4,272,512]{2,1,0:T(8,128)(2,1)S(1)}, bf16[4,272,512]{2,1,0:T(8,128)(2,1)S(1)}) custom-call(s32[4]{0:T(128)S(1)} %pad_add_fusion.where_ref, bf16[4,256,256]{2,1,0:T(8,128)(2,1)S(1)} %pad_maximum_fusion.2.q_ref, bf16[4,256,256]{2,1,0:T(8,128)(2,1)S(1)} %collective-permute-done.3.other_q_ref, ...), custom_call_target="tpu_custom_call" | custom-call | flops 4026531840 | bytes 4194304 | tf_op jit(solution)/shard_map/pallas_call | solution.py:147
  55.4 8.6 %shard_map.128 = (bf16[4,272,512]{2,1,0:T(8,128)(2,1)S(1)}, bf16[4,272,512]{2,1,0:T(8,128)(2,1)S(1)}) custom-call(s32[4]{0:T(128)S(1)} %pad_add_fusion.where_ref, bf16[4,256,256]{2,1,0:T(8,128)(2,1)S(1)} %pad_maximum_fusion.2.q_ref, bf16[4,256,256]{2,1,0:T(8,128)(2,1)S(1)} %collective-permute-done.3.other_q_ref, ...), custom_call_target="tpu_custom_call" | custom-call | flops 2415919104 | bytes 4194304 | tf_op jit(solution)/shard_map/pallas_call | solution.py:147
  64.0 4.4 %collective-permute-start.12 = (bf16[4,272,512]{2,1,0:T(8,128)(2,1)S(1)}, bf16[4,272,512]{2,1,0:T(8,128)(2,1)S(1)}, u32[]{:S(2)}, u32[]{:S(2)}) collective-permute-start(bf16[4,272,512]{2,1,0:T(8,128)(2,1)S(1)} %get-tuple-element.23), channel_id=1, source_target_pairs={{0,4},{4,0},{1,5},{5,1},{2,6},{6,2},{3,7},{7,3},{8,12},{12,8},{9,1... | collective-permute-start | bytes 3342344 | tf_op jit(solution)/shard_map/ppermute | solution.py:25
  69.9 1.6 collective-permute-start.22
  72.7 3.5 %collective-permute-start.13 = (bf16[272,512]{1,0:T(8,128)(2,1)S(1)}, bf16[272,512]{1,0:T(8,128)(2,1)S(1)}, u32[]{:S(2)}, u32[]{:S(2)}) collective-permute-start(bf16[272,512]{1,0:T(8,128)(2,1)S(1)} %get-tuple-element.25), channel_id=1, source_target_pairs={{0,24},{8,0},{16,8},{24,16},{1,25},{9,1},{17,9},{25,17},{2,26},{10... | collective-permute-start | bytes 835592 | tf_op jit(solution)/shard_map/ppermute | solution.py:25
  77.1 8.4 %collective-permute-done.19.refs_6_ = bf16[128,2560]{1,0:T(8,128)(2,1)S(1)} collective-permute-done((bf16[128,2560]{1,0:T(8,128)(2,1)S(1)}, bf16[128,2560]{1,0:T(8,128)(2,1)S(1)}, u32[]{:S(2)}, u32[]{:S(2)}) %collective-permute-start.19) | collective-permute-done | bytes 655392 | tf_op jit(solution)/shard_map/ppermute | solution.py:25
  85.5 1.4 collective-permute-start.24
  87.0 1.8 %collective-permute-start.15 = (bf16[272,512]{1,0:T(8,128)(2,1)S(1)}, bf16[272,512]{1,0:T(8,128)(2,1)S(1)}, u32[]{:S(2)}, u32[]{:S(2)}) collective-permute-start(bf16[272,512]{1,0:T(8,128)(2,1)S(1)} %get-tuple-element.27), channel_id=1, source_target_pairs={{0,8},{8,16},{16,24},{24,0},{1,9},{9,17},{17,25},{25,1},{2,10},{10... | collective-permute-start | bytes 835592 | tf_op jit(solution)/shard_map/ppermute | solution.py:25
  89.1 2.7 %collective-permute-done.14.refs_2_ = bf16[272,512]{1,0:T(8,128)(2,1)S(1)} collective-permute-done((bf16[272,512]{1,0:T(8,128)(2,1)S(1)}, bf16[272,512]{1,0:T(8,128)(2,1)S(1)}, u32[]{:S(2)}, u32[]{:S(2)}) %collective-permute-start.14) | collective-permute-done | bytes 278560 | tf_op jit(solution)/shard_map/ppermute | solution.py:25
  91.8 2.1 %collective-permute-start.23 = (bf16[128,2560]{1,0:T(8,128)(2,1)S(1)}, bf16[128,2560]{1,0:T(8,128)(2,1)S(1)}, u32[]{:S(2)}, u32[]{:S(2)}) collective-permute-start(bf16[128,2560]{1,0:T(8,128)(2,1)S(1)} %collective-permute-done.22.refs_11_), channel_id=1, source_target_pairs={{0,3},{1,0},{2,1},{3,2},{4,7},{5,4},{6,5},{7,6},{8,11},{9,8},{10,9... | collective-permute-start | bytes 1966088 | tf_op jit(solution)/shard_map/ppermute | solution.py:25
  94.6 9.1 %collective-permute-done.15.refs_3_ = bf16[272,512]{1,0:T(8,128)(2,1)S(1)} collective-permute-done((bf16[272,512]{1,0:T(8,128)(2,1)S(1)}, bf16[272,512]{1,0:T(8,128)(2,1)S(1)}, u32[]{:S(2)}, u32[]{:S(2)}) %collective-permute-start.15) | collective-permute-done | bytes 278560 | tf_op jit(solution)/shard_map/ppermute | solution.py:25
  105.0 2.6 %collective-permute-start.17 = (bf16[256,256]{1,0:T(8,128)(2,1)S(1)}, bf16[256,256]{1,0:T(8,128)(2,1)S(1)}, u32[]{:S(2)}, u32[]{:S(2)}) collective-permute-start(bf16[256,256]{1,0:T(8,128)(2,1)S(1)} %finish_heads.1.refs_0_), channel_id=1, source_target_pairs={{0,2},{1,3},{2,0},{3,1},{4,6},{5,7},{6,4},{7,5},{8,10},{9,11},{10,... | collective-permute-start | bytes 393224 | tf_op jit(solution)/shard_map/ppermute | solution.py:25
  108.4 5.2 %collective-permute-done.21.refs_8_ = bf16[128,2560]{1,0:T(8,128)(2,1)S(1)} collective-permute-done((bf16[128,2560]{1,0:T(8,128)(2,1)S(1)}, bf16[128,2560]{1,0:T(8,128)(2,1)S(1)}, u32[]{:S(2)}, u32[]{:S(2)}) %collective-permute-start.21) | collective-permute-done | bytes 655392 | tf_op jit(solution)/shard_map/ppermute | solution.py:25
  113.6 2.8 %collective-permute-done.16.refs_1_ = bf16[256,256]{1,0:T(8,128)(2,1)S(1)} collective-permute-done((bf16[256,256]{1,0:T(8,128)(2,1)S(1)}, bf16[256,256]{1,0:T(8,128)(2,1)S(1)}, u32[]{:S(2)}, u32[]{:S(2)}) %collective-permute-start.16) | collective-permute-done | bytes 131104 | tf_op jit(solution)/shard_map/ppermute | solution.py:25
  116.4 3.9 %collective-permute-done.17.refs_2_ = bf16[256,256]{1,0:T(8,128)(2,1)S(1)} collective-permute-done((bf16[256,256]{1,0:T(8,128)(2,1)S(1)}, bf16[256,256]{1,0:T(8,128)(2,1)S(1)}, u32[]{:S(2)}, u32[]{:S(2)}) %collective-permute-start.17) | collective-permute-done | bytes 131104 | tf_op jit(solution)/shard_map/ppermute | solution.py:25
  120.3 3.2 %project_norm.1 = (bf16[256,512]{1,0:T(8,128)(2,1)S(1)}, bf16[256,2048]{1,0:T(8,128)(2,1)S(1)}) custom-call(s32[4]{0:T(128)S(1)} %pad_add_fusion.where_ref, f32[1,2048]{1,0:T(1,128)S(1)} %bitcast.11, bf16[256,256]{1,0:T(8,128)(2,1)S(1)} %finish_heads.1.refs_0_, bf16[256,256]{1,0:T(8,128)(2,1)S(1)} %collective-permute-done.16.refs_1_, ...), custom_call_target="tpu_custom_call" | custom-call | flops 2000000000 | bytes 8000000 | tf_op jit(solution)/shard_map/project_norm/pallas_call | solution.py:266
  123.6 4.3 %all-gather.2.cloned.1.call-done.full_ref = bf16[2048,4224]{1,0:T(8,128)(2,1)} async-done(((bf16[32,4224]{1,0:T(8,128)(2,1)}), bf16[2048,4224]{1,0:T(8,128)(2,1)}) %all-gather.2.cloned.1.call-update) | async-done | bytes 17301520 | tf_op jit(solution)/shard_map/all_gather | solution.py:367
  127.9 9.5 %mixer.1 = (bf16[128,512]{1,0:T(8,128)(2,1)S(1)}, bf16[128,512]{1,0:T(8,128)(2,1)S(1)}, bf16[256,512]{1,0:T(8,128)(2,1)S(1)}, bf16[256,512]{1,0:T(8,128)(2,1)S(1)}, bf16[256,512]{1,0:T(8,128)(2,1)S(1)}) custom-call(s32[4]{0:T(128)S(1)} %pad_add_fusion.where_ref, bf16[256,2048]{1,0:T(8,128)(2,1)S(1)} %get-tuple-element.29.normed_ref, ...), custom_call_target="tpu_custom_call" | custom-call | flops 4429185024 | bytes 18000000 | tf_op jit(solution)/shard_map/mixer/pallas_call | solution.py:331
  137.4 2.5 %collective-permute-start.29 = (bf16[128,512]{1,0:T(8,128)(2,1)S(1)}, bf16[128,512]{1,0:T(8,128)(2,1)S(1)}, u32[]{:S(2)}, u32[]{:S(2)}) collective-permute-start(bf16[128,512]{1,0:T(8,128)(2,1)S(1)} %get-tuple-element.34), channel_id=1, source_target_pairs={{0,3},{1,0},{2,1},{3,2},{4,7},{5,4},{6,5},{7,6},{8,11},{9,8},{10,9... | collective-permute-start | bytes 393224 | tf_op jit(solution)/shard_map/ppermute | solution.py:25
  139.9 2.8 %collective-permute-start.25 = (bf16[128,512]{1,0:T(8,128)(2,1)S(1)}, bf16[128,512]{1,0:T(8,128)(2,1)S(1)}, u32[]{:S(2)}, u32[]{:S(2)}) collective-permute-start(bf16[128,512]{1,0:T(8,128)(2,1)S(1)} %slice.43), channel_id=1, source_target_pairs={{0,3},{1,0},{2,1},{3,2},{4,7},{5,4},{6,5},{7,6},{8,11},{9,8},{10,9... | collective-permute-start | bytes 393224 | tf_op jit(solution)/shard_map/ppermute | solution.py:25
  142.8 3.2 %collective-permute-start.30 = (bf16[128,512]{1,0:T(8,128)(2,1)S(1)}, bf16[128,512]{1,0:T(8,128)(2,1)S(1)}, u32[]{:S(2)}, u32[]{:S(2)}) collective-permute-start(bf16[128,512]{1,0:T(8,128)(2,1)S(1)} %add_convert_fusion), channel_id=1, source_target_pairs={{0,3},{1,0},{2,1},{3,2},{4,7},{5,4},{6,5},{7,6},{8,11},{9,8},{10,9... | collective-permute-start | bytes 393224 | tf_op jit(solution)/shard_map/ppermute | solution.py:25
  146.2 1.5 collective-permute-done.28
  148.0 3.2 %collective-permute-done.27 = bf16[128,512]{1,0:T(8,128)(2,1)S(1)} collective-permute-done((bf16[128,512]{1,0:T(8,128)(2,1)S(1)}, bf16[128,512]{1,0:T(8,128)(2,1)S(1)}, u32[]{:S(2)}, u32[]{:S(2)}) %collective-permute-start.27) | collective-permute-done | bytes 131104 | tf_op jit(solution)/shard_map/ppermute | solution.py:25
  (85 shorter events, 15.9 us)
Async XLA Ops:
  6.5 121.3 %all-gather.2.cloned.1.call-start = ((), (), s32[]{:S(2)}) async-start(), calls=%async_computation | async-start | bytes 17571840 | tf_op jit(solution)/shard_map/all_gather | solution.py:367
  9.8 12.5 %collective-permute-start.4 = (bf16[256,512]{1,0:T(8,128)(2,1)S(1)}, bf16[256,512]{1,0:T(8,128)(2,1)S(1)}, u32[]{:S(2)}, u32[]{:S(2)}) collective-permute-start(bf16[256,512]{1,0:T(8,128)(2,1)S(1)} %constant_dynamic-update-slice_fusion.2.rest_0_), channel_id=1, source_target_pairs={{0,32},{32,64},{64,96},{96,128},{128,160},{160,192},{192,224},{224... | collective-permute-start | bytes 786440 | tf_op jit(solution)/shard_map/ppermute | solution.py:25
  12.3 10.0 %collective-permute-start.7 = (bf16[256,512]{1,0:T(8,128)(2,1)S(1)}, bf16[256,512]{1,0:T(8,128)(2,1)S(1)}, u32[]{:S(2)}, u32[]{:S(2)}) collective-permute-start(bf16[256,512]{1,0:T(8,128)(2,1)S(1)} %constant_dynamic-update-slice_fusion.2.rest_0_), channel_id=1, source_target_pairs={{0,224},{32,0},{64,32},{96,64},{128,96},{160,128},{192,160},{224,1... | collective-permute-start | bytes 786440 | tf_op jit(solution)/shard_map/ppermute | solution.py:25
  16.4 8.6 %collective-permute-start = (bf16[256,256]{1,0:T(8,128)(2,1)S(1)}, bf16[256,256]{1,0:T(8,128)(2,1)S(1)}, u32[]{:S(2)}, u32[]{:S(2)}) collective-permute-start(bf16[256,256]{1,0:T(8,128)(2,1)S(1)} %constant_dynamic-update-slice_fusion), channel_id=1, source_target_pairs={{0,8},{8,16},{16,24},{24,0},{1,9},{9,17},{17,25},{25,1},{2,10},{10... | collective-permute-start | bytes 393224 | tf_op jit(solution)/shard_map/ppermute | solution.py:25
  17.8 7.8 %collective-permute-start.1 = (bf16[256,256]{1,0:T(8,128)(2,1)S(1)}, bf16[256,256]{1,0:T(8,128)(2,1)S(1)}, u32[]{:S(2)}, u32[]{:S(2)}) collective-permute-start(bf16[256,256]{1,0:T(8,128)(2,1)S(1)} %constant_dynamic-update-slice_fusion), channel_id=1, source_target_pairs={{0,16},{8,24},{16,0},{24,8},{1,17},{9,25},{17,1},{25,9},{2,18},{10... | collective-permute-start | bytes 393224 | tf_op jit(solution)/shard_map/ppermute | solution.py:25
  20.4 5.5 %collective-permute-start.2 = (bf16[256,256]{1,0:T(8,128)(2,1)S(1)}, bf16[256,256]{1,0:T(8,128)(2,1)S(1)}, u32[]{:S(2)}, u32[]{:S(2)}) collective-permute-start(bf16[256,256]{1,0:T(8,128)(2,1)S(1)} %constant_dynamic-update-slice_fusion), channel_id=1, source_target_pairs={{0,24},{8,0},{16,8},{24,16},{1,25},{9,1},{17,9},{25,17},{2,26},{10... | collective-permute-start | bytes 393224 | tf_op jit(solution)/shard_map/ppermute | solution.py:25
  22.3 7.8 %collective-permute-start.5 = (bf16[256,512]{1,0:T(8,128)(2,1)S(1)}, bf16[256,512]{1,0:T(8,128)(2,1)S(1)}, u32[]{:S(2)}, u32[]{:S(2)}) collective-permute-start(bf16[256,512]{1,0:T(8,128)(2,1)S(1)} %collective-permute-done.4.rest_1_), channel_id=1, source_target_pairs={{0,32},{32,64},{64,96},{96,128},{128,160},{160,192},{192,224},{224... | collective-permute-start | bytes 786440 | tf_op jit(solution)/shard_map/ppermute | solution.py:25
  22.3 8.2 %collective-permute-start.8 = (bf16[256,512]{1,0:T(8,128)(2,1)S(1)}, bf16[256,512]{1,0:T(8,128)(2,1)S(1)}, u32[]{:S(2)}, u32[]{:S(2)}) collective-permute-start(bf16[256,512]{1,0:T(8,128)(2,1)S(1)} %collective-permute-done.7.rest_2_), channel_id=1, source_target_pairs={{0,224},{32,0},{64,32},{96,64},{128,96},{160,128},{192,160},{224,1... | collective-permute-start | bytes 786440 | tf_op jit(solution)/shard_map/ppermute | solution.py:25
  26.0 17.4 %collective-permute-start.3 = (bf16[4,256,256]{2,1,0:T(8,128)(2,1)S(1)}, bf16[4,256,256]{2,1,0:T(8,128)(2,1)S(1)}, u32[]{:S(2)}, u32[]{:S(2)}) collective-permute-start(bf16[4,256,256]{2,1,0:T(8,128)(2,1)S(1)} %pad_maximum_fusion.2.q_ref), channel_id=1, source_target_pairs={{0,4},{4,0},{1,5},{5,1},{2,6},{6,2},{3,7},{7,3},{8,12},{12,8},{9,1... | collective-permute-start | bytes 1572872 | tf_op jit(solution)/shard_map/ppermute | solution.py:25
  30.1 8.9 %collective-permute-start.6 = (bf16[256,512]{1,0:T(8,128)(2,1)S(1)}, bf16[256,512]{1,0:T(8,128)(2,1)S(1)}, u32[]{:S(2)}, u32[]{:S(2)}) collective-permute-start(bf16[256,512]{1,0:T(8,128)(2,1)S(1)} %collective-permute-done.5.rest_3_), channel_id=1, source_target_pairs={{0,32},{32,64},{64,96},{96,128},{128,160},{160,192},{192,224},{224... | collective-permute-start | bytes 786440 | tf_op jit(solution)/shard_map/ppermute | solution.py:25
  30.4 9.3 %collective-permute-start.9 = (bf16[256,512]{1,0:T(8,128)(2,1)S(1)}, bf16[256,512]{1,0:T(8,128)(2,1)S(1)}, u32[]{:S(2)}, u32[]{:S(2)}) collective-permute-start(bf16[256,512]{1,0:T(8,128)(2,1)S(1)} %collective-permute-done.8.rest_4_), channel_id=1, source_target_pairs={{0,224},{32,0},{64,32},{96,64},{128,96},{160,128},{192,160},{224,1... | collective-permute-start | bytes 786440 | tf_op jit(solution)/shard_map/ppermute | solution.py:25
  39.0 16.3 %collective-permute-start.10 = (bf16[128,512]{1,0:T(8,128)(2,1)S(1)}, bf16[128,512]{1,0:T(8,128)(2,1)S(1)}, u32[]{:S(2)}, u32[]{:S(2)}) collective-permute-start(bf16[128,512]{1,0:T(8,128)(2,1)S(1)} %slice.48), channel_id=1, source_target_pairs={{0,32},{32,64},{64,96},{96,128},{128,160},{160,192},{192,224},{224... | collective-permute-start | bytes 393224 | tf_op jit(solution)/shard_map/ppermute | solution.py:25
  39.7 15.7 %collective-permute-start.11 = (bf16[128,512]{1,0:T(8,128)(2,1)S(1)}, bf16[128,512]{1,0:T(8,128)(2,1)S(1)}, u32[]{:S(2)}, u32[]{:S(2)}) collective-permute-start(bf16[128,512]{1,0:T(8,128)(2,1)S(1)} %slice.49), channel_id=1, source_target_pairs={{0,224},{32,0},{64,32},{96,64},{128,96},{160,128},{192,160},{224,1... | collective-permute-start | bytes 393224 | tf_op jit(solution)/shard_map/ppermute | solution.py:25
  64.0 7.5 %collective-permute-start.12 = (bf16[4,272,512]{2,1,0:T(8,128)(2,1)S(1)}, bf16[4,272,512]{2,1,0:T(8,128)(2,1)S(1)}, u32[]{:S(2)}, u32[]{:S(2)}) collective-permute-start(bf16[4,272,512]{2,1,0:T(8,128)(2,1)S(1)} %get-tuple-element.23), channel_id=1, source_target_pairs={{0,4},{4,0},{1,5},{5,1},{2,6},{6,2},{3,7},{7,3},{8,12},{12,8},{9,1... | collective-permute-start | bytes 3342344 | tf_op jit(solution)/shard_map/ppermute | solution.py:25
  68.6 17.0 %collective-permute-start.19 = (bf16[128,2560]{1,0:T(8,128)(2,1)S(1)}, bf16[128,2560]{1,0:T(8,128)(2,1)S(1)}, u32[]{:S(2)}, u32[]{:S(2)}) collective-permute-start(bf16[128,2560]{1,0:T(8,128)(2,1)S(1)} %pad_maximum_fusion), channel_id=1, source_target_pairs={{0,1},{1,2},{2,3},{3,0},{4,5},{5,6},{6,7},{7,4},{8,9},{9,10},{10,1... | collective-permute-start | bytes 1966088 | tf_op jit(solution)/shard_map/ppermute | solution.py:25
  69.9 17.1 %collective-permute-start.22 = (bf16[128,2560]{1,0:T(8,128)(2,1)S(1)}, bf16[128,2560]{1,0:T(8,128)(2,1)S(1)}, u32[]{:S(2)}, u32[]{:S(2)}) collective-permute-start(bf16[128,2560]{1,0:T(8,128)(2,1)S(1)} %pad_maximum_fusion.1), channel_id=1, source_target_pairs={{0,3},{1,0},{2,1},{3,2},{4,7},{5,4},{6,5},{7,6},{8,11},{9,8},{10,9... | collective-permute-start | bytes 1966088 | tf_op jit(solution)/shard_map/ppermute | solution.py:25
  72.7 16.1 %collective-permute-start.13 = (bf16[272,512]{1,0:T(8,128)(2,1)S(1)}, bf16[272,512]{1,0:T(8,128)(2,1)S(1)}, u32[]{:S(2)}, u32[]{:S(2)}) collective-permute-start(bf16[272,512]{1,0:T(8,128)(2,1)S(1)} %get-tuple-element.25), channel_id=1, source_target_pairs={{0,24},{8,0},{16,8},{24,16},{1,25},{9,1},{17,9},{25,17},{2,26},{10... | collective-permute-start | bytes 835592 | tf_op jit(solution)/shard_map/ppermute | solution.py:25
  76.2 15.6 %collective-permute-start.14 = (bf16[272,512]{1,0:T(8,128)(2,1)S(1)}, bf16[272,512]{1,0:T(8,128)(2,1)S(1)}, u32[]{:S(2)}, u32[]{:S(2)}) collective-permute-start(bf16[272,512]{1,0:T(8,128)(2,1)S(1)} %get-tuple-element.26), channel_id=1, source_target_pairs={{0,16},{8,24},{16,0},{24,8},{1,17},{9,25},{17,1},{25,9},{2,18},{10... | collective-permute-start | bytes 835592 | tf_op jit(solution)/shard_map/ppermute | solution.py:25
  76.6 28.4 %collective-permute-start.20 = (bf16[128,2560]{1,0:T(8,128)(2,1)S(1)}, bf16[128,2560]{1,0:T(8,128)(2,1)S(1)}, u32[]{:S(2)}, u32[]{:S(2)}) collective-permute-start(bf16[128,2560]{1,0:T(8,128)(2,1)S(1)} %pad_maximum_fusion.1), channel_id=1, source_target_pairs={{0,1},{1,2},{2,3},{3,0},{4,5},{5,6},{6,7},{7,4},{8,9},{9,10},{10,1... | collective-permute-start | bytes 1966088 | tf_op jit(solution)/shard_map/ppermute | solution.py:25
  85.5 22.0 %collective-permute-start.24 = (bf16[128,2560]{1,0:T(8,128)(2,1)S(1)}, bf16[128,2560]{1,0:T(8,128)(2,1)S(1)}, u32[]{:S(2)}, u32[]{:S(2)}) collective-permute-start(bf16[128,2560]{1,0:T(8,128)(2,1)S(1)} %pad_maximum_fusion), channel_id=1, source_target_pairs={{0,3},{1,0},{2,1},{3,2},{4,7},{5,4},{6,5},{7,6},{8,11},{9,8},{10,9... | collective-permute-start | bytes 1966088 | tf_op jit(solution)/shard_map/ppermute | solution.py:25
  87.0 16.7 %collective-permute-start.15 = (bf16[272,512]{1,0:T(8,128)(2,1)S(1)}, bf16[272,512]{1,0:T(8,128)(2,1)S(1)}, u32[]{:S(2)}, u32[]{:S(2)}) collective-permute-start(bf16[272,512]{1,0:T(8,128)(2,1)S(1)} %get-tuple-element.27), channel_id=1, source_target_pairs={{0,8},{8,16},{16,24},{24,0},{1,9},{9,17},{17,25},{25,1},{2,10},{10... | collective-permute-start | bytes 835592 | tf_op jit(solution)/shard_map/ppermute | solution.py:25
  88.8 24.8 %collective-permute-start.21 = (bf16[128,2560]{1,0:T(8,128)(2,1)S(1)}, bf16[128,2560]{1,0:T(8,128)(2,1)S(1)}, u32[]{:S(2)}, u32[]{:S(2)}) collective-permute-start(bf16[128,2560]{1,0:T(8,128)(2,1)S(1)} %collective-permute-done.19.refs_6_), channel_id=1, source_target_pairs={{0,1},{1,2},{2,3},{3,0},{4,5},{5,6},{6,7},{7,4},{8,9},{9,10},{10,1... | collective-permute-start | bytes 1966088 | tf_op jit(solution)/shard_map/ppermute | solution.py:25
  91.8 21.8 %collective-permute-start.23 = (bf16[128,2560]{1,0:T(8,128)(2,1)S(1)}, bf16[128,2560]{1,0:T(8,128)(2,1)S(1)}, u32[]{:S(2)}, u32[]{:S(2)}) collective-permute-start(bf16[128,2560]{1,0:T(8,128)(2,1)S(1)} %collective-permute-done.22.refs_11_), channel_id=1, source_target_pairs={{0,3},{1,0},{2,1},{3,2},{4,7},{5,4},{6,5},{7,6},{8,11},{9,8},{10,9... | collective-permute-start | bytes 1966088 | tf_op jit(solution)/shard_map/ppermute | solution.py:25
  104.5 11.9 %collective-permute-start.16 = (bf16[256,256]{1,0:T(8,128)(2,1)S(1)}, bf16[256,256]{1,0:T(8,128)(2,1)S(1)}, u32[]{:S(2)}, u32[]{:S(2)}) collective-permute-start(bf16[256,256]{1,0:T(8,128)(2,1)S(1)} %finish_heads.1.refs_0_), channel_id=1, source_target_pairs={{0,1},{1,2},{2,3},{3,0},{4,5},{5,6},{6,7},{7,4},{8,9},{9,10},{10,1... | collective-permute-start | bytes 393224 | tf_op jit(solution)/shard_map/ppermute | solution.py:25
  105.0 15.3 %collective-permute-start.17 = (bf16[256,256]{1,0:T(8,128)(2,1)S(1)}, bf16[256,256]{1,0:T(8,128)(2,1)S(1)}, u32[]{:S(2)}, u32[]{:S(2)}) collective-permute-start(bf16[256,256]{1,0:T(8,128)(2,1)S(1)} %finish_heads.1.refs_0_), channel_id=1, source_target_pairs={{0,2},{1,3},{2,0},{3,1},{4,6},{5,7},{6,4},{7,5},{8,10},{9,11},{10,... | collective-permute-start | bytes 393224 | tf_op jit(solution)/shard_map/ppermute | solution.py:25
  107.5 12.8 %collective-permute-start.18 = (bf16[256,256]{1,0:T(8,128)(2,1)S(1)}, bf16[256,256]{1,0:T(8,128)(2,1)S(1)}, u32[]{:S(2)}, u32[]{:S(2)}) collective-permute-start(bf16[256,256]{1,0:T(8,128)(2,1)S(1)} %finish_heads.1.refs_0_), channel_id=1, source_target_pairs={{0,3},{1,0},{2,1},{3,2},{4,7},{5,4},{6,5},{7,6},{8,11},{9,8},{10,9... | collective-permute-start | bytes 393224 | tf_op jit(solution)/shard_map/ppermute | solution.py:25
  137.4 5.4 %collective-permute-start.29 = (bf16[128,512]{1,0:T(8,128)(2,1)S(1)}, bf16[128,512]{1,0:T(8,128)(2,1)S(1)}, u32[]{:S(2)}, u32[]{:S(2)}) collective-permute-start(bf16[128,512]{1,0:T(8,128)(2,1)S(1)} %get-tuple-element.34), channel_id=1, source_target_pairs={{0,3},{1,0},{2,1},{3,2},{4,7},{5,4},{6,5},{7,6},{8,11},{9,8},{10,9... | collective-permute-start | bytes 393224 | tf_op jit(solution)/shard_map/ppermute | solution.py:25
  139.9 6.1 %collective-permute-start.26 = (bf16[128,512]{1,0:T(8,128)(2,1)S(1)}, bf16[128,512]{1,0:T(8,128)(2,1)S(1)}, u32[]{:S(2)}, u32[]{:S(2)}) collective-permute-start(bf16[128,512]{1,0:T(8,128)(2,1)S(1)} %get-tuple-element.33), channel_id=1, source_target_pairs={{0,1},{1,2},{2,3},{3,0},{4,5},{5,6},{6,7},{7,4},{8,9},{9,10},{10,1... | collective-permute-start | bytes 393224 | tf_op jit(solution)/shard_map/ppermute | solution.py:25
  139.9 6.3 %collective-permute-start.25 = (bf16[128,512]{1,0:T(8,128)(2,1)S(1)}, bf16[128,512]{1,0:T(8,128)(2,1)S(1)}, u32[]{:S(2)}, u32[]{:S(2)}) collective-permute-start(bf16[128,512]{1,0:T(8,128)(2,1)S(1)} %slice.43), channel_id=1, source_target_pairs={{0,3},{1,0},{2,1},{3,2},{4,7},{5,4},{6,5},{7,6},{8,11},{9,8},{10,9... | collective-permute-start | bytes 393224 | tf_op jit(solution)/shard_map/ppermute | solution.py:25
  142.7 5.1 %collective-permute-start.28 = (bf16[128,512]{1,0:T(8,128)(2,1)S(1)}, bf16[128,512]{1,0:T(8,128)(2,1)S(1)}, u32[]{:S(2)}, u32[]{:S(2)}) collective-permute-start(bf16[128,512]{1,0:T(8,128)(2,1)S(1)} %slice.46), channel_id=1, source_target_pairs={{0,1},{1,2},{2,3},{3,0},{4,5},{5,6},{6,7},{7,4},{8,9},{9,10},{10,1... | collective-permute-start | bytes 393224 | tf_op jit(solution)/shard_map/ppermute | solution.py:25
  142.8 5.1 %collective-permute-start.30 = (bf16[128,512]{1,0:T(8,128)(2,1)S(1)}, bf16[128,512]{1,0:T(8,128)(2,1)S(1)}, u32[]{:S(2)}, u32[]{:S(2)}) collective-permute-start(bf16[128,512]{1,0:T(8,128)(2,1)S(1)} %add_convert_fusion), channel_id=1, source_target_pairs={{0,3},{1,0},{2,1},{3,2},{4,7},{5,4},{6,5},{7,6},{8,11},{9,8},{10,9... | collective-permute-start | bytes 393224 | tf_op jit(solution)/shard_map/ppermute | solution.py:25
  146.0 5.1 %collective-permute-start.27 = (bf16[128,512]{1,0:T(8,128)(2,1)S(1)}, bf16[128,512]{1,0:T(8,128)(2,1)S(1)}, u32[]{:S(2)}, u32[]{:S(2)}) collective-permute-start(bf16[128,512]{1,0:T(8,128)(2,1)S(1)} %add_convert_fusion.1), channel_id=1, source_target_pairs={{0,1},{1,2},{2,3},{3,0},{4,5},{5,6},{6,7},{7,4},{8,9},{9,10},{10,1... | collective-permute-start | bytes 393224 | tf_op jit(solution)/shard_map/ppermute | solution.py:25
  (10 other events, 92.9 us)
Sparse Core Ops, SparseCore 0:
  10.1 117.7 all-gather.1
